TPU v7x, 256 devices: a 4x2x16 block of a 4x16x16 slice. The times are simulated.
256 devices in a mesh: grp: 2 (over y), sp: 32 (over z, core), tp: 4 (over x).
Axes of the slice: x: 4, y: 2, z: 16, core: 2. Of those that a mesh axis runs over, the one named last changes fastest.
The devices are a block of a 4x16x16 slice.
Arguments:
- resid_in: bfloat16 [8, 2048, 2048], P(('grp', 'tp'), 'sp'), parts along dimension 0, may hold values from -6 to 6
- query_one: bfloat16 [8, 2048, 1024], P('grp', 'sp', 'tp'), parts along dimension 0, may hold values from -624 to 624
- key_one: bfloat16 [8, 2048, 256], P('grp', 'sp', 'tp'), parts along dimension 0, may hold values from -7.78125 to 7.78125
- query_two: bfloat16 [8, 2048, 1024], P('grp', 'sp', 'tp'), parts along dimension 0, may hold values from -624 to 624
- key_two: bfloat16 [8, 2048, 256], P('grp', 'sp', 'tp'), parts along dimension 0, may hold values from -7.78125 to 7.78125
- value: bfloat16 [8, 2048, 512], P('grp', 'sp', 'tp'), parts along dimension 0, may hold values from -6 to 6
- lam: float32 [32], P('tp'), may hold values from 0.3 to 0.8
- head_gain: float32 [64], replicated, may hold values from 0.1 to 1.9
- doc_ids: int32 [8, 2048], P('grp', 'sp'), parts along dimension 0, may hold values from 0 to 3, never falling along the last dimension, each value on 1 to 1024 neighbouring positions
- out_weight: bfloat16 [2048, 2048], P('tp'), may hold values from -0.125 to 0.125
- norm_gain: float32 [2048], replicated, may hold values from 0.1 to 1.9
- gate_weight: bfloat16 [2048, 5632], P('sp', 'tp'), may hold values from -0.125 to 0.125
- value_weight: bfloat16 [2048, 5632], P('sp', 'tp'), may hold values from -0.125 to 0.125
- conv_gate: float32 [3, 5632], P(None, 'tp'), may hold values from -3.5 to 3.5
- conv_value: float32 [3, 5632], P(None, 'tp'), may hold values from -3.5 to 3.5
- down_weight: bfloat16 [5632, 2048], P('tp', 'sp'), may hold values from -0.078125 to 0.078125
Outputs:
- resid_out: bfloat16 [8, 2048, 2048], P(('grp', 'tp'), 'sp'), parts along dimension 0
There are 2 independent parts, one for each index of `grp`. A program takes and returns all parts, laid end to end along the dimension named above; an argument that names none is the same for every part. Nothing has to cross between parts.
All inputs are finite; a program needn't handle non-finite values.
Results may differ from a plain program's by a relative error of at most 0.014.
Values may be sent and summed in bfloat16 or wider, within the bound.
No kernel may reach another device: no remote copies, remote signals or barrier semaphores. Data moves between devices by JAX's collectives and lax.ppermute only.
A program may use at most 128 MiB of HBM per device.

v0:
```python
import math

import jax
import jax.numpy as jnp
from jax import lax
from jax.sharding import PartitionSpec as P

NEG_BIG = -1e30
NORM_EPS = 1e-06
ROPE_BASE = 500000.0


def turned_gather(arrays, axis, dims):
    turned = [jnp.moveaxis(a, dim, 0) for a, dim in zip(arrays, dims)]
    widths = [t[0].size for t in turned]
    both = jnp.concatenate([t.reshape(-1, w) for t, w in zip(turned, widths)], axis=1)
    result = lax.all_gather(both, axis, axis=0, tiled=True)
    tiles = jnp.split(result, [sum(widths[:k]) for k in range(1, len(widths))], axis=1)
    return tuple(
        (
            jnp.moveaxis(b.reshape(-1, *t.shape[1:]), 0, dim)
            for b, t, dim in zip(tiles, turned, dims)
        )
    )


def sent_together(arrays, axis, dim, along):
    ends, at = ([], 0)
    for a in arrays[:-1]:
        at += a.shape[along]
        ends.append(at)
    both = jnp.concatenate(arrays, axis=along)
    return tuple(jnp.split(lax.all_gather(both, axis, axis=dim, tiled=True), ends, axis=along))


def split_up(array, dim, length):
    before, after = (array.shape[:dim], array.shape[dim + 1 :])
    return jnp.moveaxis(array.reshape(*before, length, -1, *after), dim, 0)


def sum_at_owner(array, axis, dim):
    length = lax.axis_size(axis)
    tiles = lax.all_to_all(split_up(array, dim, length), axis, 0, 0, tiled=True)
    return jnp.sum(tiles.astype(jnp.float32), axis=0)


def joined_along(tiles, dim):
    dims = list(tiles.shape[1:])
    dims[dim] *= tiles.shape[0]
    return jnp.moveaxis(tiles, 0, dim).reshape(dims)


def from_everyone(array, axis):
    copies = jnp.broadcast_to(array, (lax.axis_size(axis), *array.shape))
    return lax.all_to_all(copies, axis, split_axis=0, concat_axis=0, tiled=True)


def collect(array, axis, dim):
    return joined_along(from_everyone(array, axis), dim)


def from_behind(array, axis, by):
    length = lax.axis_size(axis)
    pairs = [(i, i + by) for i in range(length) if 0 <= i + by < length]
    return lax.ppermute(array, axis, pairs)


def rotate(block, positions, heads):
    entries = block.astype(jnp.float32).reshape(block.shape[:-1] + (heads, -1))
    width = entries.shape[-1]
    half = width // 2
    freqs = ROPE_BASE ** (-jnp.arange(half, dtype=jnp.float32) * 2.0 / width)
    angles = positions.astype(jnp.float32)[:, None] * freqs[None, :]
    cosine = jnp.cos(angles)[:, None, :]
    sine = jnp.sin(angles)[:, None, :]
    first = entries[..., :half]
    second = entries[..., half:]
    turned = jnp.concatenate(
        [first * cosine - second * sine, second * cosine + first * sine], axis=-1
    )
    return turned.astype(jnp.bfloat16)


def depthwise(edge, current, taps, edge_docs, docs):
    count = current.shape[0]
    extended = jnp.concatenate([edge, current], axis=0).astype(jnp.float32)
    ext_docs = jnp.concatenate([edge_docs, docs], axis=0)
    total = taps[2][None, :] * extended[2:]
    for shift_k in range(2):
        same = (ext_docs[shift_k : shift_k + count] == docs)[:, None]
        total = total + jnp.where(
            same, taps[shift_k][None, :] * extended[shift_k : shift_k + count], 0.0
        )
    return total


def online_step(state, queries, keys, vals, allowed, scale):
    peak, total, accum = state
    scores = (
        jnp.einsum("sqhgd,skhd->shgqk", queries, keys, preferred_element_type=jnp.float32) * scale
    )
    mask = allowed[:, None, None]
    scores = jnp.where(mask, scores, NEG_BIG)
    new_peak = jnp.maximum(peak, jnp.max(scores, axis=-1))
    expd = jnp.where(mask, jnp.exp(scores - new_peak[..., None]), 0.0)
    fade = jnp.exp(peak - new_peak)
    new_total = total * fade + jnp.sum(expd, axis=-1)
    update = jnp.einsum(
        "shgqk,skhd->shgqd", expd.astype(jnp.bfloat16), vals, preferred_element_type=jnp.float32
    )
    return (new_peak, new_total, accum * fade[..., None] + update)


def per_device(
    resid_in,
    query_one,
    key_one,
    query_two,
    key_two,
    value,
    lam,
    head_gain,
    doc_ids,
    out_weight,
    norm_gain,
    gate_weight,
    value_weight,
    conv_gate,
    conv_value,
    down_weight,
):
    gate_full, value_full, down_full = turned_gather(
        (gate_weight, value_weight, down_weight), "sp", (0, 0, 1)
    )
    seqs = query_one.shape[0]
    rows = query_one.shape[1]
    heads = lam.shape[0]
    key_width = query_one.shape[2] // heads
    kv_local = key_one.shape[2] // key_width
    group = heads // kv_local
    head_width = value.shape[2] // kv_local
    scale = key_width ** (-0.5)
    positions = lax.axis_index("sp") * rows + jnp.arange(rows, dtype=jnp.int32)
    q_first = rotate(query_one, positions, heads).reshape(seqs, rows, kv_local, group, key_width)
    q_second = rotate(query_two, positions, heads).reshape(seqs, rows, kv_local, group, key_width)
    k_first = rotate(key_one, positions, kv_local).reshape(seqs, rows, kv_local * key_width)
    k_second = rotate(key_two, positions, kv_local).reshape(seqs, rows, kv_local * key_width)
    start_state = (
        jnp.full((seqs, kv_local, group, rows), NEG_BIG, jnp.float32),
        jnp.zeros((seqs, kv_local, group, rows), jnp.float32),
        jnp.zeros((seqs, kv_local, group, rows, head_width), jnp.float32),
    )
    keys_one, keys_two, vals, docs = (
        *sent_together((k_first, k_second, value), "sp", 1, 2),
        lax.all_gather(doc_ids, "sp", axis=1, tiled=True),
    )
    count = keys_one.shape[1]
    step_len = math.gcd(count, 512)

    def inner(state, index):
        offset = index * step_len
        ka = lax.dynamic_slice_in_dim(keys_one, offset, step_len, 1).reshape(
            seqs, step_len, kv_local, key_width
        )
        kb = lax.dynamic_slice_in_dim(keys_two, offset, step_len, 1).reshape(
            seqs, step_len, kv_local, key_width
        )
        va = lax.dynamic_slice_in_dim(vals, offset, step_len, 1).reshape(
            seqs, step_len, kv_local, head_width
        )
        dpiece = lax.dynamic_slice_in_dim(docs, offset, step_len, 1)
        key_pos = offset + jnp.arange(step_len, dtype=jnp.int32)
        allowed = (key_pos[None, None, :] <= positions[None, :, None]) & (
            dpiece[:, None, :] == doc_ids[:, :, None]
        )
        first = online_step(state[0], q_first, ka, va, allowed, scale)
        second = online_step(state[1], q_second, kb, va, allowed, scale)
        return ((first, second), None)

    def run(state):
        return lax.scan(inner, state, jnp.arange(count // step_len))[0]

    first, second = lax.cond(
        jnp.int32(0) <= positions[rows - 1], run, lambda state: state, (start_state, start_state)
    )
    weights = lam.reshape(kv_local, group)[None, :, :, None, None]
    mixed = first[2] / first[1][..., None] - weights * (second[2] / second[1][..., None])
    meansq = jnp.mean(mixed * mixed, axis=-1, keepdims=True)
    normed_heads = mixed * lax.rsqrt(meansq + NORM_EPS) * head_gain
    heads_out = jnp.transpose(normed_heads, (0, 3, 1, 2, 4)).reshape(
        seqs * rows, heads * head_width
    )
    heads_out = heads_out.astype(jnp.bfloat16)
    proj = sum_at_owner(
        jnp.dot(heads_out, out_weight, preferred_element_type=jnp.float32).astype(jnp.bfloat16),
        "tp",
        0,
    )
    mid = resid_in.astype(jnp.float32) + proj.reshape(resid_in.shape)
    meansq_mid = jnp.mean(mid * mid, axis=-1, keepdims=True)
    normed = (mid * lax.rsqrt(meansq_mid + NORM_EPS) * norm_gain).astype(jnp.bfloat16)
    gathered = collect(normed, "tp", 0)
    full_rows = gathered.reshape(seqs * rows, gathered.shape[2])
    gate_sum = jnp.dot(full_rows, gate_full, preferred_element_type=jnp.float32)
    value_sum = jnp.dot(full_rows, value_full, preferred_element_type=jnp.float32)
    hidden_width = gate_weight.shape[1]
    up_gate = gate_sum.astype(jnp.bfloat16).reshape(seqs, rows, hidden_width)
    up_value = value_sum.astype(jnp.bfloat16).reshape(seqs, rows, hidden_width)
    tails = jnp.stack([up_gate[:, rows - 2 :], up_value[:, rows - 2 :]], axis=0)
    edges, edge_docs = from_behind((tails, doc_ids[:, rows - 2 :]), "sp", 1)
    sweep = jax.vmap(depthwise, in_axes=(0, 0, None, 0, 0))
    conv_g = sweep(edges[0], up_gate, conv_gate, edge_docs, doc_ids)
    conv_v = sweep(edges[1], up_value, conv_value, edge_docs, doc_ids)
    hidden = (jax.nn.silu(conv_g) * conv_v).astype(jnp.bfloat16).reshape(seqs * rows, hidden_width)
    partial_down = jnp.dot(hidden, down_full, preferred_element_type=jnp.float32)
    down = sum_at_owner(partial_down.astype(jnp.bfloat16), "tp", 0)
    return (mid + down.reshape(mid.shape)).astype(jnp.bfloat16)


def solution(mesh):
    placed = (
        P(("grp", "tp"), "sp", None),
        P("grp", "sp", "tp"),
        P("grp", "sp", "tp"),
        P("grp", "sp", "tp"),
        P("grp", "sp", "tp"),
        P("grp", "sp", "tp"),
        P("tp"),
        P(),
        P("grp", "sp"),
        P("tp", None),
        P(),
        P("sp", "tp"),
        P("sp", "tp"),
        P(None, "tp"),
        P(None, "tp"),
        P("tp", "sp"),
    )
    return jax.shard_map(
        per_device,
        mesh=mesh,
        in_specs=placed,
        out_specs=P(("grp", "tp"), "sp", None),
        check_vma=False,
    )
```

profile of v0, /device:TPU:33, one launch (start us, length us, event | category | flops | bytes accessed | tf_op | source)
XLA Modules:
  0.0 286.9 jit_solution(15549829019060020416)
XLA Ops:
  6.7 1.1 copy.43
  7.8 0.9 copy.44
  9.2 0.9 copy.47
  10.1 0.8 pad_maximum_fusion.3
  11.1 0.8 pad_maximum_fusion
  12.5 50.6 %all-gather = s32[32,64,4]{1,2,0:T(4,128)S(1)} all-gather(s32[1,64,4]{1,2,0:T(4,128)S(1)} %bitcast.155), channel_id=1, replica_groups=mesh['grp'=2,'sp'=32,'tp'=4] {'sp'}, dimensions={0}, use_global_device_ids=true | all-gather | bytes 33792 | tf_op jit(solution)/shard_map/all_gather | solution.py:155
  64.8 33.1 %all-gather.4.cloned.1.call-done = bf16[4,2048,256]{2,0,1:T(4,128)(2,1)} async-done(((bf16[4,64,256]{2,0,1:T(4,128)(2,1)}), bf16[4,2048,256]{2,0,1:T(4,128)(2,1)}) %all-gather.4.cloned.1.call-update) | async-done | bytes 4194320 | tf_op jit(solution)/shard_map/all_gather | solution.py:33
  97.9 99.5 %conditional.1 = (f32[4,2,4,64]{3,2,1,0:T(4,128)}, f32[4,2,4,64,64]{4,3,2,1,0:T(8,128)}, f32[4,2,4,64]{3,2,1,0:T(4,128)}, f32[4,2,4,64,64]{4,3,2,1,0:T(8,128)}) conditional(s32[]{:T(128)} %bitcast, () %tuple.17, (bf16[4,2048,256]{2,0,1:T(4,128)(2,1)}, s32[64]{0:T(128)S(1)}, s32[4,2048]{1,0:T(4,128)S(1)}, s32[4,64]{1,0:T(4,128)S(1)}, ...), branch_computations={%region_0.0_spmd, %region_1.8_spmd} | conditional | flops 431018496 | bytes 120289104 | solution.py:183
  97.9 7.6 %copy.51 = bf16[4,2048,256]{1,2,0:T(8,128)(2,1)} copy(bf16[4,2048,256]{2,0,1:T(4,128)(2,1)} %get-tuple-element.178) | data formatting | bytes 8388608 | tf_op jit(solution)/shard_map
  105.4 3.3 %fusion.55 = (bf16[4,2048,64]{1,2,0:T(8,128)(2,1)}, bf16[4,2048,64]{1,2,0:T(8,128)(2,1)}) fusion(bf16[4,2048,256]{1,2,0:T(8,128)(2,1)} %copy.51), kind=kLoop, calls=%fused_computation.114 | loop fusion | bytes 4194304 | tf_op jit(solution)/shard_map/split | solution.py:33
  108.7 1.5 split.25
  110.2 87.2 %while.20 = (s32[]{:T(128)}, f32[4,2,4,64]{3,2,1,0:T(4,128)S(1)}, f32[4,2,4,64]{3,2,1,0:T(4,128)}, f32[4,2,4,64,64]{4,3,2,1,0:T(8,128)}, f32[4,2,4,64]{3,2,1,0:T...) while((s32[]{:T(128)}, f32[4,2,4,64]{3,2,1,0:T(4,128)S(1)}, ...), condition=%wide.region_7.7_spmd.clone, body=%wide.region_2.6_spmd.clone.sunk | while | flops 431018496 | bytes 86734432 | solution.py:181
  111.6 1.0 constant_dynamic-slice_fusion.9
  112.6 0.7 fusion.90
  113.4 1.2 constant_dynamic-slice_fusion.10
  114.5 3.5 %fusion.91 = (f32[4,2,4,64]{3,2,1,0:T(4,128)S(1)}, f32[4,2,4,64]{3,2,1,0:T(4,128)S(1)}, f32[4,2,512,64,4]{2,3,4,1,0:T(8,128)}) fusion(pred[4,64,512]{2,1,0:T(8,128)(4,1)S(1)} %compare_and_fusion.2, f32[4,2,512,64,4]{2,3,4,1,0:T(8,128)S(1)} %fusion.90, bf16[4,512,2,32,1]{1,3,4,2,0:T(8,128)(2,1)S(1)} %bitcast.133, ...), kind=kOutput, calls=%fused_computation.5.clone.1 | convolution fusion | flops 73396224 | bytes 8929280 | tf_op jit(solution)/shard_map/cond/branch_1_fun/while/body/eval_jaxpr/sqhgd,skhd->shgqk/dot_general | solution.py:100
  118.1 5.1 %fusion.92 = (f32[4,2,4,64]{3,2,1,0:T(4,128)S(1)}, f32[4,2,4,64]{3,2,1,0:T(4,128)S(1)}) fusion(f32[4,2,512,64,4]{2,3,4,1,0:T(8,128)} %get-tuple-element.369, f32[4,2,4,64]{3,2,1,0:T(4,128)S(1)} %select_maximum_fusion.5, pred[4,64,512]{2,1,0:T(8,128)(4,1)S(1)} %compare_and_fusion.2, f32[4,2,4,64]{3,2,1,0:T(4,128)S(1)} %select_maximum_fusion.4, ...), kind=kLoop, calls=%fused_computation.9.clone.1 | loop fusion | flops 10481664 | bytes 8552448 | tf_op jit(solution)/shard_map/cond/branch_1_fun/while/body/eval_jaxpr/reduce_sum | solution.py:107
  123.2 0.7 fusion.93
  123.9 1.1 constant_dynamic-slice_fusion.11
  125.0 2.4 fusion.95
  127.4 2.3 fusion.94
  131.2 1.0 constant_dynamic-slice_fusion.9
  132.2 0.7 fusion.90
  133.0 1.2 constant_dynamic-slice_fusion.10
  134.1 3.5 %fusion.91 = (f32[4,2,4,64]{3,2,1,0:T(4,128)S(1)}, f32[4,2,4,64]{3,2,1,0:T(4,128)S(1)}, f32[4,2,512,64,4]{2,3,4,1,0:T(8,128)}) fusion(pred[4,64,512]{2,1,0:T(8,128)(4,1)S(1)} %compare_and_fusion.2, f32[4,2,512,64,4]{2,3,4,1,0:T(8,128)S(1)} %fusion.90, bf16[4,512,2,32,1]{1,3,4,2,0:T(8,128)(2,1)S(1)} %bitcast.133, ...), kind=kOutput, calls=%fused_computation.5.clone.1 | convolution fusion | flops 73396224 | bytes 8929280 | tf_op jit(solution)/shard_map/cond/branch_1_fun/while/body/eval_jaxpr/sqhgd,skhd->shgqk/dot_general | solution.py:100
  137.7 5.1 %fusion.92 = (f32[4,2,4,64]{3,2,1,0:T(4,128)S(1)}, f32[4,2,4,64]{3,2,1,0:T(4,128)S(1)}) fusion(f32[4,2,512,64,4]{2,3,4,1,0:T(8,128)} %get-tuple-element.369, f32[4,2,4,64]{3,2,1,0:T(4,128)S(1)} %select_maximum_fusion.5, pred[4,64,512]{2,1,0:T(8,128)(4,1)S(1)} %compare_and_fusion.2, f32[4,2,4,64]{3,2,1,0:T(4,128)S(1)} %select_maximum_fusion.4, ...), kind=kLoop, calls=%fused_computation.9.clone.1 | loop fusion | flops 10481664 | bytes 8552448 | tf_op jit(solution)/shard_map/cond/branch_1_fun/while/body/eval_jaxpr/reduce_sum | solution.py:107
  142.8 1.4 fusion.93
  144.2 1.1 constant_dynamic-slice_fusion.11
  145.4 3.6 %fusion.95 = f32[4,2,4,64,64]{4,3,2,1,0:T(8,128)} fusion(bf16[4,512,2,64,1]{1,3,4,2,0:T(8,128)(2,1)S(1)} %bitcast.135, f32[4,2,512,64,4]{2,3,4,1,0:T(8,128)S(1)} %copy-done.3, f32[4,2,4,64]{3,2,1,0:T(4,128)S(1)} %select_maximum_fusion.5, pred[4,64,512]{2,1,0:T(8,128)(4,1)S(1)} %compare_and_fusion.2, f32[4,2,4,64,64]{4,3,2,1,0:T(8,128)} %get-tuple-element.403, ...), kind=kOutput, calls=%fused_computation.15.clone.1 | convolution fusion | flops 139853824 | bytes 5914625 | tf_op jit(solution)/shard_map/cond/branch_1_fun/while/body/eval_jaxpr/shgqk,skhd->shgqd/dot_general | solution.py:108
  148.9 3.4 %fusion.94 = f32[4,2,4,64,64]{4,3,2,1,0:T(8,128)} fusion(bf16[4,512,2,64,1]{1,3,4,2,0:T(8,128)(2,1)S(1)} %bitcast.136, f32[4,2,512,64,4]{2,3,4,1,0:T(8,128)S(1)} %copy-done.2, f32[4,2,4,64]{3,2,1,0:T(4,128)S(1)} %select_maximum_fusion.4, pred[4,64,512]{2,1,0:T(8,128)(4,1)S(1)} %compare_and_fusion.2, f32[4,2,4,64,64]{4,3,2,1,0:T(8,128)} %get-tuple-element.400, ...), kind=kOutput, calls=%fused_computation.14.clone.1 | convolution fusion | flops 139853824 | bytes 5914625 | tf_op jit(solution)/shard_map/cond/branch_1_fun/while/body/eval_jaxpr/shgqk,skhd->shgqd/dot_general | solution.py:108
  153.8 1.0 constant_dynamic-slice_fusion.9
  154.7 0.7 fusion.90
  155.5 1.2 constant_dynamic-slice_fusion.10
  156.7 3.5 %fusion.91 = (f32[4,2,4,64]{3,2,1,0:T(4,128)S(1)}, f32[4,2,4,64]{3,2,1,0:T(4,128)S(1)}, f32[4,2,512,64,4]{2,3,4,1,0:T(8,128)}) fusion(pred[4,64,512]{2,1,0:T(8,128)(4,1)S(1)} %compare_and_fusion.2, f32[4,2,512,64,4]{2,3,4,1,0:T(8,128)S(1)} %fusion.90, bf16[4,512,2,32,1]{1,3,4,2,0:T(8,128)(2,1)S(1)} %bitcast.133, ...), kind=kOutput, calls=%fused_computation.5.clone.1 | convolution fusion | flops 73396224 | bytes 8929280 | tf_op jit(solution)/shard_map/cond/branch_1_fun/while/body/eval_jaxpr/sqhgd,skhd->shgqk/dot_general | solution.py:100
  160.2 5.1 %fusion.92 = (f32[4,2,4,64]{3,2,1,0:T(4,128)S(1)}, f32[4,2,4,64]{3,2,1,0:T(4,128)S(1)}) fusion(f32[4,2,512,64,4]{2,3,4,1,0:T(8,128)} %get-tuple-element.369, f32[4,2,4,64]{3,2,1,0:T(4,128)S(1)} %select_maximum_fusion.5, pred[4,64,512]{2,1,0:T(8,128)(4,1)S(1)} %compare_and_fusion.2, f32[4,2,4,64]{3,2,1,0:T(4,128)S(1)} %select_maximum_fusion.4, ...), kind=kLoop, calls=%fused_computation.9.clone.1 | loop fusion | flops 10481664 | bytes 8552448 | tf_op jit(solution)/shard_map/cond/branch_1_fun/while/body/eval_jaxpr/reduce_sum | solution.py:107
  165.3 1.4 fusion.93
  166.7 1.1 constant_dynamic-slice_fusion.11
  167.8 3.6 %fusion.95 = f32[4,2,4,64,64]{4,3,2,1,0:T(8,128)} fusion(bf16[4,512,2,64,1]{1,3,4,2,0:T(8,128)(2,1)S(1)} %bitcast.135, f32[4,2,512,64,4]{2,3,4,1,0:T(8,128)S(1)} %copy-done.3, f32[4,2,4,64]{3,2,1,0:T(4,128)S(1)} %select_maximum_fusion.5, pred[4,64,512]{2,1,0:T(8,128)(4,1)S(1)} %compare_and_fusion.2, f32[4,2,4,64,64]{4,3,2,1,0:T(8,128)} %get-tuple-element.403, ...), kind=kOutput, calls=%fused_computation.15.clone.1 | convolution fusion | flops 139853824 | bytes 5914625 | tf_op jit(solution)/shard_map/cond/branch_1_fun/while/body/eval_jaxpr/shgqk,skhd->shgqd/dot_general | solution.py:108
  171.4 3.4 %fusion.94 = f32[4,2,4,64,64]{4,3,2,1,0:T(8,128)} fusion(bf16[4,512,2,64,1]{1,3,4,2,0:T(8,128)(2,1)S(1)} %bitcast.136, f32[4,2,512,64,4]{2,3,4,1,0:T(8,128)S(1)} %copy-done.2, f32[4,2,4,64]{3,2,1,0:T(4,128)S(1)} %select_maximum_fusion.4, pred[4,64,512]{2,1,0:T(8,128)(4,1)S(1)} %compare_and_fusion.2, f32[4,2,4,64,64]{4,3,2,1,0:T(8,128)} %get-tuple-element.400, ...), kind=kOutput, calls=%fused_computation.14.clone.1 | convolution fusion | flops 139853824 | bytes 5914625 | tf_op jit(solution)/shard_map/cond/branch_1_fun/while/body/eval_jaxpr/shgqk,skhd->shgqd/dot_general | solution.py:108
  176.2 1.0 constant_dynamic-slice_fusion.9
  177.2 0.7 fusion.90
  177.9 1.2 constant_dynamic-slice_fusion.10
  179.1 3.5 %fusion.91 = (f32[4,2,4,64]{3,2,1,0:T(4,128)S(1)}, f32[4,2,4,64]{3,2,1,0:T(4,128)S(1)}, f32[4,2,512,64,4]{2,3,4,1,0:T(8,128)}) fusion(pred[4,64,512]{2,1,0:T(8,128)(4,1)S(1)} %compare_and_fusion.2, f32[4,2,512,64,4]{2,3,4,1,0:T(8,128)S(1)} %fusion.90, bf16[4,512,2,32,1]{1,3,4,2,0:T(8,128)(2,1)S(1)} %bitcast.133, ...), kind=kOutput, calls=%fused_computation.5.clone.1 | convolution fusion | flops 73396224 | bytes 8929280 | tf_op jit(solution)/shard_map/cond/branch_1_fun/while/body/eval_jaxpr/sqhgd,skhd->shgqk/dot_general | solution.py:100
  182.7 5.1 %fusion.92 = (f32[4,2,4,64]{3,2,1,0:T(4,128)S(1)}, f32[4,2,4,64]{3,2,1,0:T(4,128)S(1)}) fusion(f32[4,2,512,64,4]{2,3,4,1,0:T(8,128)} %get-tuple-element.369, f32[4,2,4,64]{3,2,1,0:T(4,128)S(1)} %select_maximum_fusion.5, pred[4,64,512]{2,1,0:T(8,128)(4,1)S(1)} %compare_and_fusion.2, f32[4,2,4,64]{3,2,1,0:T(4,128)S(1)} %select_maximum_fusion.4, ...), kind=kLoop, calls=%fused_computation.9.clone.1 | loop fusion | flops 10481664 | bytes 8552448 | tf_op jit(solution)/shard_map/cond/branch_1_fun/while/body/eval_jaxpr/reduce_sum | solution.py:107
  187.8 1.4 fusion.93
  189.2 1.1 constant_dynamic-slice_fusion.11
  190.3 3.6 %fusion.95 = f32[4,2,4,64,64]{4,3,2,1,0:T(8,128)} fusion(bf16[4,512,2,64,1]{1,3,4,2,0:T(8,128)(2,1)S(1)} %bitcast.135, f32[4,2,512,64,4]{2,3,4,1,0:T(8,128)S(1)} %copy-done.3, f32[4,2,4,64]{3,2,1,0:T(4,128)S(1)} %select_maximum_fusion.5, pred[4,64,512]{2,1,0:T(8,128)(4,1)S(1)} %compare_and_fusion.2, f32[4,2,4,64,64]{4,3,2,1,0:T(8,128)} %get-tuple-element.403, ...), kind=kOutput, calls=%fused_computation.15.clone.1 | convolution fusion | flops 139853824 | bytes 5914625 | tf_op jit(solution)/shard_map/cond/branch_1_fun/while/body/eval_jaxpr/shgqk,skhd->shgqd/dot_general | solution.py:108
  194.0 3.4 %fusion.94 = f32[4,2,4,64,64]{4,3,2,1,0:T(8,128)} fusion(bf16[4,512,2,64,1]{1,3,4,2,0:T(8,128)(2,1)S(1)} %bitcast.136, f32[4,2,512,64,4]{2,3,4,1,0:T(8,128)S(1)} %copy-done.2, f32[4,2,4,64]{3,2,1,0:T(4,128)S(1)} %select_maximum_fusion.4, pred[4,64,512]{2,1,0:T(8,128)(4,1)S(1)} %compare_and_fusion.2, f32[4,2,4,64,64]{4,3,2,1,0:T(8,128)} %get-tuple-element.400, ...), kind=kOutput, calls=%fused_computation.14.clone.1 | convolution fusion | flops 139853824 | bytes 5914625 | tf_op jit(solution)/shard_map/cond/branch_1_fun/while/body/eval_jaxpr/shgqk,skhd->shgqd/dot_general | solution.py:108
  197.3 2.3 multiply_reduce_fusion
  200.8 0.7 convolution_convert_fusion
  201.6 18.8 %all_to_all.15 = bf16[4,64,2048]{2,1,0:T(8,128)(2,1)S(1)} all-to-all(bf16[4,64,2048]{2,1,0:T(8,128)(2,1)S(1)} %bitcast.137), channel_id=1, replica_groups=mesh['grp'=2,'sp'=32,'tp'=4] {'tp'}, dimensions={0} | all-to-all | bytes 2097152 | tf_op jit(solution)/shard_map/all_to_all | solution.py:43
  220.9 1.1 broadcast_in_dim.98
  222.0 4.5 %all-to-all-start.1 = ((bf16[4,1,64,2048]{3,2,1,0:T(8,128)(2,1)}), bf16[4,1,64,2048]{3,2,1,0:T(8,128)(2,1)}, u32[]{:S(2)}, u32[]{:S(2)}) async-start(bf16[4,1,64,2048]{3,2,1,0:T(8,128)(2,1)} %broadcast_in_dim.98), calls=%async_computation.1 | async-start | bytes 2097152 | tf_op jit(solution)/shard_map/all_to_all | solution.py:55
  226.5 4.4 %collective-permute-start.1 = (s32[4,2]{1,0:T(4,128)S(1)}, s32[4,2]{1,0:T(4,128)S(1)}, u32[]{:S(2)}, u32[]{:S(2)}) collective-permute-start(s32[4,2]{1,0:T(4,128)S(1)} %slice.100), channel_id=1, source_target_pairs={{0,4},{4,8},{8,12},{12,16},{16,20},{20,24},{24,28},{28,32},{32,36}... | collective-permute-start | bytes 104 | tf_op jit(solution)/shard_map/ppermute | solution.py:65
  231.0 0.6 collective-permute-done.1
  231.7 8.6 %all-to-all-done.1 = bf16[4,1,64,2048]{3,2,1,0:T(8,128)(2,1)} async-done(((bf16[4,1,64,2048]{3,2,1,0:T(8,128)(2,1)}), bf16[4,1,64,2048]{3,2,1,0:T(8,128)(2,1)}, u32[]{:S(2)}, u32[]{:S(2)}) %all-to-all-start.1) | async-done | bytes 1048608 | tf_op jit(solution)/shard_map/all_to_all | solution.py:55
  240.3 4.8 %fusion.35 = bf16[256,1408]{1,0:T(8,128)(2,1)S(1)} fusion(bf16[256,2048]{1,0:T(8,128)(2,1)} %bitcast.22, bf16[2048,4224]{1,0:T(8,128)(2,1)} %all-gather.6.cloned.1.call-done), kind=kOutput, calls=%fused_computation.47 | convolution fusion | flops 1476755456 | bytes 7536640 | tf_op jit(solution)/shard_map/dot_general | solution.py:205
  245.1 4.8 %fusion.32 = bf16[256,1408]{1,0:T(8,128)(2,1)S(1)} fusion(bf16[256,2048]{1,0:T(8,128)(2,1)} %bitcast.22, bf16[2048,4224]{1,0:T(8,128)(2,1)} %all-gather.6.cloned.1.call-done), kind=kOutput, calls=%fused_computation.46 | convolution fusion | flops 1476755456 | bytes 7536640 | tf_op jit(solution)/shard_map/dot_general | solution.py:204
  250.0 4.8 %collective-permute-start = (bf16[2,4,2,1408]{3,2,1,0:T(2,128)(2,1)S(1)}, bf16[2,4,2,1408]{3,2,1,0:T(2,128)(2,1)S(1)}, u32[]{:S(2)}, u32[]{:S(2)}) collective-permute-start(bf16[2,4,2,1408]{3,2,1,0:T(2,128)(2,1)S(1)} %pad_maximum_fusion.6), channel_id=1, source_target_pairs={{0,4},{4,8},{8,12},{12,16},{16,20},{20,24},{24,28},{28,32},{32,36}... | collective-permute-start | bytes 135176 | tf_op jit(solution)/shard_map/ppermute | solution.py:65
  254.9 1.0 collective-permute-done
  256.3 1.6 fusion.44
  257.9 4.5 %fusion.38 = bf16[256,2048]{1,0:T(8,128)(2,1)S(1)} fusion(bf16[256,1408]{1,0:T(8,128)(2,1)S(1)} %bitcast.145, bf16[2048,4224]{1,0:T(8,128)(2,1)} %all-gather.6.cloned.1.call-done), kind=kOutput, calls=%fused_computation.48 | convolution fusion | flops 1476919296 | bytes 7536640 | tf_op jit(solution)/shard_map/dot_general | solution.py:215
  262.4 16.7 %all_to_all.16 = bf16[4,64,2048]{2,1,0:T(8,128)(2,1)S(1)} all-to-all(bf16[4,64,2048]{2,1,0:T(8,128)(2,1)S(1)} %bitcast.140), channel_id=1, replica_groups=mesh['grp'=2,'sp'=32,'tp'=4] {'tp'}, dimensions={0} | all-to-all | bytes 2097152 | tf_op jit(solution)/shard_map/all_to_all | solution.py:43
  279.3 0.8 fusion.52
  (139 shorter events, 8.2 us)
Async XLA Ops:
  6.5 194.3 %copy-start = (bf16[512,2048]{1,0:T(8,128)(2,1)S(1)}, bf16[512,2048]{1,0:T(8,128)(2,1)}, u32[]{:S(2)}) copy-start(bf16[512,2048]{1,0:T(8,128)(2,1)} %param.29) | copy-start | bytes 6291460
  6.6 4.5 %copy-start.6 = (bf16[1408,64]{0,1:T(8,128)(2,1)S(1)}, bf16[1408,64]{0,1:T(8,128)(2,1)}, u32[]{:S(2)}) copy-start(bf16[1408,64]{0,1:T(8,128)(2,1)} %param.35) | copy-start | bytes 540676
  6.6 4.5 %copy-start.8 = (bf16[64,1408]{1,0:T(8,128)(2,1)S(1)}, bf16[64,1408]{1,0:T(8,128)(2,1)}, u32[]{:S(2)}) copy-start(bf16[64,1408]{1,0:T(8,128)(2,1)} %param.31) | copy-start | bytes 540676
  6.6 4.5 %copy-start.7 = (bf16[64,1408]{1,0:T(8,128)(2,1)S(1)}, bf16[64,1408]{1,0:T(8,128)(2,1)}, u32[]{:S(2)}) copy-start(bf16[64,1408]{1,0:T(8,128)(2,1)} %param.32) | copy-start | bytes 540676
  6.6 5.4 %copy-start.10 = (bf16[4,64,256]{2,1,0:T(8,128)(2,1)S(1)}, bf16[4,64,256]{2,1,0:T(8,128)(2,1)}, u32[]{:S(2)}) copy-start(bf16[4,64,256]{2,1,0:T(8,128)(2,1)} %param.21) | copy-start | bytes 393220
  6.6 91.3 %all-gather.4.cloned.1.call-start = ((), (), s32[]{:S(2)}) async-start(), calls=%async_computation.3 | async-start | bytes 4325376 | tf_op jit(solution)/shard_map/all_gather | solution.py:33
  8.9 3.4 %copy-start.11 = (bf16[4,64,256]{2,1,0:T(8,128)(2,1)S(1)}, bf16[4,64,256]{2,1,0:T(8,128)(2,1)}, u32[]{:S(2)}) copy-start(bf16[4,64,256]{2,1,0:T(8,128)(2,1)} %param.23) | copy-start | bytes 393220
  10.9 1.6 copy-start.9
  11.0 229.4 %all-gather.6.cloned.1.call-start = ((), (), s32[]{:S(2)}) async-start(), calls=%async_computation.4 | async-start | bytes 17842176 | tf_op jit(solution)/shard_map/all_gather | solution.py:17
  11.1 53.3 %copy-start.16 = (f32[8]{0:T(128)S(1)}, f32[8]{0:T(128)}, u32[]{:S(2)}) copy-start(f32[8]{0:T(128)} %param.26) | copy-start | bytes 100
  105.4 3.3 %copy-start.4 = (bf16[4,2048,256]{1,2,0:T(8,128)(2,1)S(1)}, bf16[4,2048,256]{1,2,0:T(8,128)(2,1)}, u32[]{:S(2)}) copy-start(bf16[4,2048,256]{1,2,0:T(8,128)(2,1)} %copy.51) | copy-start | bytes 12582916 | tf_op jit(solution)/shard_map/cond
  113.3 4.7 %copy-start.1 = (f32[4,2,512,64,4]{2,3,4,1,0:T(8,128)}, f32[4,2,512,64,4]{2,3,4,1,0:T(8,128)S(1)}, u32[]{:S(2)}) copy-start(f32[4,2,512,64,4]{2,3,4,1,0:T(8,128)S(1)} %fusion.90) | copy-start | bytes 12582916 | tf_op jit(solution)/shard_map/cond/branch_1_fun/while
  118.1 6.9 %copy-start.3 = (f32[4,2,512,64,4]{2,3,4,1,0:T(8,128)S(1)}, f32[4,2,512,64,4]{2,3,4,1,0:T(8,128)}, u32[]{:S(2)}) copy-start(f32[4,2,512,64,4]{2,3,4,1,0:T(8,128)} %get-tuple-element.369) | copy-start | bytes 12582916 | tf_op jit(solution)/shard_map/cond/branch_1_fun/while
  125.0 2.5 copy-start.2
  133.0 4.7 %copy-start.1 = (f32[4,2,512,64,4]{2,3,4,1,0:T(8,128)}, f32[4,2,512,64,4]{2,3,4,1,0:T(8,128)S(1)}, u32[]{:S(2)}) copy-start(f32[4,2,512,64,4]{2,3,4,1,0:T(8,128)S(1)} %fusion.90) | copy-start | bytes 12582916 | tf_op jit(solution)/shard_map/cond/branch_1_fun/while
  137.7 7.7 %copy-start.3 = (f32[4,2,512,64,4]{2,3,4,1,0:T(8,128)S(1)}, f32[4,2,512,64,4]{2,3,4,1,0:T(8,128)}, u32[]{:S(2)}) copy-start(f32[4,2,512,64,4]{2,3,4,1,0:T(8,128)} %get-tuple-element.369) | copy-start | bytes 12582916 | tf_op jit(solution)/shard_map/cond/branch_1_fun/while
  145.4 3.6 %copy-start.2 = (f32[4,2,512,64,4]{2,3,4,1,0:T(8,128)S(1)}, f32[4,2,512,64,4]{2,3,4,1,0:T(8,128)}, u32[]{:S(2)}) copy-start(f32[4,2,512,64,4]{2,3,4,1,0:T(8,128)} %copy-done.1) | copy-start | bytes 12582916 | tf_op jit(solution)/shard_map/cond/branch_1_fun/while
  155.5 4.7 %copy-start.1 = (f32[4,2,512,64,4]{2,3,4,1,0:T(8,128)}, f32[4,2,512,64,4]{2,3,4,1,0:T(8,128)S(1)}, u32[]{:S(2)}) copy-start(f32[4,2,512,64,4]{2,3,4,1,0:T(8,128)S(1)} %fusion.90) | copy-start | bytes 12582916 | tf_op jit(solution)/shard_map/cond/branch_1_fun/while
  160.2 7.6 %copy-start.3 = (f32[4,2,512,64,4]{2,3,4,1,0:T(8,128)S(1)}, f32[4,2,512,64,4]{2,3,4,1,0:T(8,128)}, u32[]{:S(2)}) copy-start(f32[4,2,512,64,4]{2,3,4,1,0:T(8,128)} %get-tuple-element.369) | copy-start | bytes 12582916 | tf_op jit(solution)/shard_map/cond/branch_1_fun/while
  167.8 3.6 %copy-start.2 = (f32[4,2,512,64,4]{2,3,4,1,0:T(8,128)S(1)}, f32[4,2,512,64,4]{2,3,4,1,0:T(8,128)}, u32[]{:S(2)}) copy-start(f32[4,2,512,64,4]{2,3,4,1,0:T(8,128)} %copy-done.1) | copy-start | bytes 12582916 | tf_op jit(solution)/shard_map/cond/branch_1_fun/while
  177.9 4.7 %copy-start.1 = (f32[4,2,512,64,4]{2,3,4,1,0:T(8,128)}, f32[4,2,512,64,4]{2,3,4,1,0:T(8,128)S(1)}, u32[]{:S(2)}) copy-start(f32[4,2,512,64,4]{2,3,4,1,0:T(8,128)S(1)} %fusion.90) | copy-start | bytes 12582916 | tf_op jit(solution)/shard_map/cond/branch_1_fun/while
  182.7 7.7 %copy-start.3 = (f32[4,2,512,64,4]{2,3,4,1,0:T(8,128)S(1)}, f32[4,2,512,64,4]{2,3,4,1,0:T(8,128)}, u32[]{:S(2)}) copy-start(f32[4,2,512,64,4]{2,3,4,1,0:T(8,128)} %get-tuple-element.369) | copy-start | bytes 12582916 | tf_op jit(solution)/shard_map/cond/branch_1_fun/while
  190.3 3.6 %copy-start.2 = (f32[4,2,512,64,4]{2,3,4,1,0:T(8,128)S(1)}, f32[4,2,512,64,4]{2,3,4,1,0:T(8,128)}, u32[]{:S(2)}) copy-start(f32[4,2,512,64,4]{2,3,4,1,0:T(8,128)} %copy-done.1) | copy-start | bytes 12582916 | tf_op jit(solution)/shard_map/cond/branch_1_fun/while
  197.3 2.4 copy-start.15
  201.5 19.0 %copy-start.5 = (bf16[1,64,2048]{2,1,0:T(8,128)(2,1)S(1)}, bf16[1,64,2048]{2,1,0:T(8,128)(2,1)}, u32[]{:S(2)}) copy-start(bf16[1,64,2048]{2,1,0:T(8,128)(2,1)} %param.20) | copy-start | bytes 786436
  201.6 19.2 %copy-start.14 = (f32[2048]{0:T(1024)S(1)}, f32[2048]{0:T(1024)}, u32[]{:S(2)}) copy-start(f32[2048]{0:T(1024)} %param.30) | copy-start | bytes 24580
  220.7 10.2 %copy-start.12 = (f32[3,1408]{1,0:T(4,128)S(1)}, f32[3,1408]{1,0:T(4,128)}, u32[]{:S(2)}) copy-start(f32[3,1408]{1,0:T(4,128)} %param.34) | copy-start | bytes 50692
  220.7 10.2 %copy-start.13 = (f32[3,1408]{1,0:T(4,128)S(1)}, f32[3,1408]{1,0:T(4,128)}, u32[]{:S(2)}) copy-start(f32[3,1408]{1,0:T(4,128)} %param.33) | copy-start | bytes 50692
  222.0 18.4 %all-to-all-start.1 = ((bf16[4,1,64,2048]{3,2,1,0:T(8,128)(2,1)}), bf16[4,1,64,2048]{3,2,1,0:T(8,128)(2,1)}, u32[]{:S(2)}, u32[]{:S(2)}) async-start(bf16[4,1,64,2048]{3,2,1,0:T(8,128)(2,1)} %broadcast_in_dim.98), calls=%async_computation.1 | async-start | bytes 2097152 | tf_op jit(solution)/shard_map/all_to_all | solution.py:55
  226.5 5.1 %collective-permute-start.1 = (s32[4,2]{1,0:T(4,128)S(1)}, s32[4,2]{1,0:T(4,128)S(1)}, u32[]{:S(2)}, u32[]{:S(2)}) collective-permute-start(s32[4,2]{1,0:T(4,128)S(1)} %slice.100), channel_id=1, source_target_pairs={{0,4},{4,8},{8,12},{12,16},{16,20},{20,24},{24,28},{28,32},{32,36}... | collective-permute-start | bytes 104 | tf_op jit(solution)/shard_map/ppermute | solution.py:65
  250.0 5.9 %collective-permute-start = (bf16[2,4,2,1408]{3,2,1,0:T(2,128)(2,1)S(1)}, bf16[2,4,2,1408]{3,2,1,0:T(2,128)(2,1)S(1)}, u32[]{:S(2)}, u32[]{:S(2)}) collective-permute-start(bf16[2,4,2,1408]{3,2,1,0:T(2,128)(2,1)S(1)} %pad_maximum_fusion.6), channel_id=1, source_target_pairs={{0,4},{4,8},{8,12},{12,16},{16,20},{20,24},{24,28},{28,32},{32,36}... | collective-permute-start | bytes 135176 | tf_op jit(solution)/shard_map/ppermute | solution.py:65
Sparse Core Ops, SparseCore 0:
  11.1 86.7 all-gather.3
  99.7 104.3 all-gather.5
where the time goes:
time: 288 us; the launch traced here: 287 us
  blocking collectives  86.1 us (30%)
  matrix products  57.2 us (20%)
  waiting for transfers between devices  43.5 us (15%)
  other arithmetic  34.8 us (12%)
  local copies, waits for them, and re-layouts  34.2 us (12%)
  between operations  14.5 us (5%)
  starting transfers between devices  13.8 us (5%)
    all_gather x1, blocking collectives, per_device(): lax.all_gather(doc_ids, 'sp', axis=1, tiled=True)  50.6 us
    all_to_all x2, blocking collectives, sum_at_owner(): tiles = lax.all_to_all(split_up(array, dim, length), axis, 0, 0, tiled=True)  35.5 us
    all_gather x1, waiting for transfers between devices, sent_together(): lax.all_gather(both, axis, axis=dim, tiled=True)  33.1 us
    dot_general x8, matrix products, online_step(): jnp.einsum('shgqk,skhd->shgqd', expd.astype(jnp.bfloat16), vals, preferre...  25.6 us
    reduce_sum x4, other arithmetic, online_step(): new_total = total * fade + jnp.sum(expd, axis=-1)  20.5 us
    dot_general x8, matrix products, online_step(): jnp.einsum('sqhgd,skhd->shgqk', queries, keys, preferred_element_type=jnp...  16.9 us
    ppermute x2, starting transfers between devices, from_behind(): return lax.ppermute(array, axis, pairs)  9.19 us
    all_to_all x1, waiting for transfers between devices, from_everyone(): return lax.all_to_all(copies, axis, split_axis=0, concat_axis=0, tiled=True)  8.62 us
  transfers between devices with their start and end apart: 5, of which 4 were waited for; matrix products, arithmetic and copies ran while one was open for 37% of the time, Pallas kernels for 0%

commit v1 on v0

v1 whole, which is shorter than its diff:
```python
import math

import jax
import jax.numpy as jnp
from jax import lax
from jax.experimental import pallas as pl
from jax.experimental.pallas import tpu as pltpu
from jax.sharding import PartitionSpec as P

NORM_EPS = 1e-06
ROPE_BASE = 500000.0
LOG2E = math.log2(math.e)
DOC_SPAN = 1024
KEY_UP = 4096.0
VAL_UP = 8192.0
LANES = 128
EDGE = 8


def shifted(array, axis, by):
    length = lax.axis_size(axis)
    return lax.ppermute(array, axis, [(i, (i + by) % length) for i in range(length)])


def from_behind(array, axis):
    length = lax.axis_size(axis)
    return lax.ppermute(array, axis, [(i, i + 1) for i in range(length - 1)])


def turn_tables(positions, width):
    half = width // 2
    freqs = ROPE_BASE ** (-jnp.arange(half, dtype=jnp.float32) * 2.0 / width)
    angles = positions.astype(jnp.float32)[:, None] * freqs[None, :]
    cosine = jnp.cos(angles)
    sine = jnp.sin(angles)
    times = LANES // width
    return (
        jnp.tile(jnp.concatenate([cosine, cosine], axis=1), (1, times)),
        jnp.tile(jnp.concatenate([-sine, sine], axis=1), (1, times)),
    )


def attend(q_one, q_two, window, cosine, sine, doc_cols, gain, lam, place):
    seqs, rows, q_lanes = q_one.shape
    ranks, per_rank, _ = window.shape
    keys = ranks * rows
    heads = lam.shape[0]
    width = q_lanes // heads
    half = width // 2
    kv_heads = 2
    group = heads // kv_heads
    head_width = LANES // kv_heads
    mult = width ** (-0.5) * LOG2E

    def body(place_ref, lam_ref, q1_ref, q2_ref, w_ref, c_ref, s_ref, d_ref, g_ref, o_ref):
        first_key = place_ref[0]
        first_row = place_ref[1]
        own = place_ref[2]
        lane = lax.broadcasted_iota(jnp.int32, (rows, LANES), 1)
        low = (lane % width) < half
        cos = c_ref[...]
        sin = s_ref[...]
        gain_row = g_ref[...]
        key_pos = first_key + lax.broadcasted_iota(jnp.int32, (rows, keys), 1)
        row_pos = first_row + lax.broadcasted_iota(jnp.int32, (rows, keys), 0)
        causal = key_pos <= row_pos
        even_lane = lax.broadcasted_iota(jnp.int32, (1, LANES), 1) < rows
        ones = jnp.ones((keys, LANES), jnp.bfloat16)
        for s in range(seqs):
            at = s * rows
            k_all = w_ref[:, at : at + rows, 0:LANES].reshape(keys, LANES)
            v_all = w_ref[:, at : at + rows, LANES : 2 * LANES].reshape(keys, LANES)
            v_ext = jnp.concatenate([v_all, ones], axis=1)
            pieces = []
            for i in range(ranks // 2):
                tail_a = w_ref[2 * i, seqs * rows : per_rank, 0:LANES].astype(jnp.float32)
                tail_b = w_ref[2 * i + 1, seqs * rows : per_rank, 0:LANES].astype(jnp.float32)
                pieces.append(jnp.where(even_lane, tail_a[s : s + 1], tail_b[s : s + 1]))
            key_doc = jnp.concatenate(pieces, axis=1)
            row_doc = d_ref[:, s : s + 1]
            bias = jnp.where(causal & (key_doc == row_doc), 0.0, -1e30)
            placed = []
            for ref in (q1_ref, q2_ref):
                tiles = []
                for h in range(kv_heads):
                    x = ref[s, :, h * LANES : (h + 1) * LANES].astype(jnp.float32)
                    swap = jnp.where(
                        low, pltpu.roll(x, LANES - half, 1), pltpu.roll(x, half, 1)
                    )
                    tiles.append((x * cos + swap * sin).astype(jnp.bfloat16).astype(jnp.float32))
                placed.append(tiles)
            for h in range(kv_heads):
                result = []
                for c in range(2):
                    target = c * kv_heads + h
                    inside = (lane // width) == target
                    parts = []
                    for g in range(group):
                        by = (width * (target - g)) % LANES
                        x = placed[c][h]
                        x = pltpu.roll(x, by, 1) if by else x
                        parts.append(jnp.where(inside, x, 0.0).astype(jnp.bfloat16))
                    q = jnp.concatenate(parts, axis=0)
                    score = lax.dot_general(
                        q, k_all, (((1,), (1,)), ((), ())), preferred_element_type=jnp.float32
                    )
                    score = score.reshape(group, rows, keys) + bias[None]
                    peak = jnp.max(score, axis=-1, keepdims=True)
                    expd = jnp.exp2((score - peak) * mult).astype(jnp.bfloat16)
                    both = jnp.dot(
                        expd.reshape(group * rows, keys), v_ext, preferred_element_type=jnp.float32
                    )
                    result.append(both[:, :LANES] / both[:, LANES:])
                here = (lane // head_width) == h
                outs = []
                for g in range(group):
                    a = result[0][g * rows : (g + 1) * rows]
                    b = result[1][g * rows : (g + 1) * rows]
                    o = jnp.where(here, a - lam_ref[h * group + g] * b, 0.0)
                    meansq = jnp.sum(o * o, axis=-1, keepdims=True) * (1.0 / head_width)
                    o = o * lax.rsqrt(meansq + NORM_EPS) * gain_row
                    if (g % 2) != h:
                        o = pltpu.roll(o, head_width, 1)
                    outs.append(o)
                slot = (s - own + seqs) % seqs
                for j in range(group // 2):
                    tile = (h * group) // 2 + j
                    o_ref[slot, :, tile * LANES : (tile + 1) * LANES] = (
                        outs[2 * j] + outs[2 * j + 1]
                    ).astype(jnp.bfloat16)

    vmem = pl.BlockSpec(memory_space=pltpu.VMEM)
    smem = pl.BlockSpec(memory_space=pltpu.SMEM)
    return pl.pallas_call(
        body,
        out_shape=jax.ShapeDtypeStruct((seqs, rows, heads * head_width), jnp.bfloat16),
        in_specs=[smem, smem] + [vmem] * 7,
        out_specs=vmem,
        name="attend",
    )(place, lam, q_one, q_two, window, cosine, sine, doc_cols, gain)


def feed_forward(blocks, weights, same, conv_gate, conv_value):
    span, width = blocks[0].shape
    count = len(blocks)
    total = span * count
    rows = span - EDGE
    hidden = conv_gate.shape[1]
    step = 2 * LANES
    cuts = [(a, min(a + step, hidden)) for a in range(0, hidden, step)]
    out_step = 4 * LANES

    def body(x0, x1, x2, x3, same_ref, cg_ref, cv_ref, w_hbm, o_ref, x_ref, w_ref, h_ref, sems):
        def up_copy(j):
            a, b = cuts[j]
            return [
                pltpu.make_async_copy(
                    w_hbm.at[:, base + a : base + b],
                    w_ref.at[:, base + a : base + b],
                    sems.at[2 * j + which],
                )
                for which, base in enumerate((0, hidden))
            ]

        down_copy = pltpu.make_async_copy(
            w_hbm.at[:, 2 * hidden : 3 * hidden],
            w_ref.at[:, 2 * hidden : 3 * hidden],
            sems.at[2 * len(cuts)],
        )
        for j in range(len(cuts)):
            for copy in up_copy(j):
                copy.start()
        down_copy.start()
        for k, x in enumerate((x0, x1, x2, x3)):
            x_ref[k * span : (k + 1) * span, :] = x[...]
        one_back = same_ref[:, 0:1]
        two_back = same_ref[:, 1:2]
        for j in range(len(cuts)):
            a, b = cuts[j]
            for copy in up_copy(j):
                copy.wait()
            convs = []
            for base, taps in ((0, cg_ref), (hidden, cv_ref)):
                u = jnp.dot(
                    x_ref[...], w_ref[:, base + a : base + b], preferred_element_type=jnp.float32
                )
                u = u.astype(jnp.bfloat16).astype(jnp.float32)
                convs.append(
                    taps[2:3, a:b] * u
                    + taps[1:2, a:b] * (one_back * pltpu.roll(u, 1, 0))
                    + taps[0:1, a:b] * (two_back * pltpu.roll(u, 2, 0))
                )
            g, v = convs
            act = (g / (1.0 + jnp.exp(-g)) * v).astype(jnp.float32)
            for k in range(count):
                h_ref[k * rows : (k + 1) * rows, a:b] = act[
                    k * span + EDGE : (k + 1) * span
                ].astype(jnp.bfloat16)
        down_copy.wait()
        for a in range(0, width, out_step):
            part = lax.dot_general(
                h_ref[...],
                w_ref[a : a + out_step, 2 * hidden : 3 * hidden],
                (((1,), (1,)), ((), ())),
                preferred_element_type=jnp.float32,
            )
            o_ref[:, :, a : a + out_step] = part.astype(jnp.bfloat16).reshape(count, rows, out_step)

    vmem = pl.BlockSpec(memory_space=pltpu.VMEM)
    return pl.pallas_call(
        body,
        out_shape=jax.ShapeDtypeStruct((count, rows, width), jnp.bfloat16),
        in_specs=[vmem] * 7 + [pl.BlockSpec(memory_space=pltpu.HBM)],
        out_specs=vmem,
        scratch_shapes=[
            pltpu.VMEM((total, width), jnp.bfloat16),
            pltpu.VMEM((width, 3 * hidden), jnp.bfloat16),
            pltpu.VMEM((count * rows, hidden), jnp.bfloat16),
            pltpu.SemaphoreType.DMA((2 * len(cuts) + 1,)),
        ],
        compiler_params=pltpu.CompilerParams(vmem_limit_bytes=56 * 1024 * 1024),
        name="feed_forward",
    )(*blocks, same, conv_gate, conv_value, weights)


def per_device(
    resid_in,
    query_one,
    key_one,
    query_two,
    key_two,
    value,
    lam,
    head_gain,
    doc_ids,
    out_weight,
    norm_gain,
    gate_weight,
    value_weight,
    conv_gate,
    conv_value,
    down_weight,
):
    seqs, rows, q_lanes = query_one.shape
    width = q_lanes // lam.shape[0]
    rank = lax.axis_index("sp")
    ranks = lax.axis_size("sp")
    own = lax.axis_index("tp")
    parts = lax.axis_size("tp")
    model = resid_in.shape[2]

    packed = jnp.concatenate([gate_weight, value_weight, down_weight.T], axis=1)
    weights = lax.all_gather(packed, "sp", axis=0, tiled=True)

    positions = rank * rows + jnp.arange(rows, dtype=jnp.int32)
    cosine, sine = turn_tables(positions, width)
    keys = jnp.concatenate([key_one, key_two], axis=2).astype(jnp.float32)
    half = width // 2
    low = (jnp.arange(LANES) % width) < half
    swap = jnp.where(low, jnp.roll(keys, -half, axis=2), jnp.roll(keys, half, axis=2))
    keys = (keys * cosine + swap * sine).astype(jnp.bfloat16).astype(jnp.float32) * KEY_UP
    vals = value.astype(jnp.float32) * VAL_UP
    body_rows = jnp.concatenate([keys, vals], axis=2).reshape(seqs * rows, 2 * LANES)
    doc_rows = jnp.tile(doc_ids.astype(jnp.float32) * KEY_UP, (1, 2 * LANES // rows))
    doc_rows = jnp.pad(doc_rows, ((0, EDGE - seqs), (0, 0)))
    sent = jnp.concatenate([body_rows, doc_rows], axis=0).astype(jnp.float16)
    everyone = lax.all_gather(sent, "sp", axis=0, tiled=False)

    back = DOC_SPAN // rows
    span = min(back + 2, ranks)
    first = jnp.clip(rank // 2 * 2 - back, 0, ranks - span)
    lanes_down = jnp.where(jnp.arange(2 * LANES) < LANES, 1.0 / KEY_UP, 1.0 / VAL_UP)
    window = lax.dynamic_slice_in_dim(everyone, first, span, 0)
    window = (window.astype(jnp.float32) * lanes_down).astype(jnp.bfloat16)
    behind = lax.dynamic_index_in_dim(everyone, jnp.maximum(rank - 1, 0), 0, keepdims=False)
    behind = behind[seqs * rows : seqs * rows + seqs, rows - 2 : rows].astype(jnp.float32)
    behind = jnp.where(rank > 0, behind * (1.0 / KEY_UP), -1.0)

    docs = doc_ids.astype(jnp.float32)
    gain = jnp.tile(head_gain, 2).reshape(1, LANES)
    place = jnp.stack([first * rows, rank * rows, own]).astype(jnp.int32)
    heads_out = attend(
        query_one, query_two, window, cosine, sine, docs.T, gain, lam, place
    )
    proj = jnp.dot(
        heads_out.reshape(seqs * rows, -1), out_weight, preferred_element_type=jnp.float32
    )
    proj = proj.astype(jnp.bfloat16).reshape(seqs, rows, model)
    mid = resid_in[0].astype(jnp.float32) + proj[0].astype(jnp.float32)
    for k in range(1, parts):
        mid = mid + shifted(proj[k], "tp", k).astype(jnp.float32)
    meansq = jnp.mean(mid * mid, axis=-1, keepdims=True)
    normed = (mid * lax.rsqrt(meansq + NORM_EPS) * norm_gain).astype(jnp.bfloat16)
    edge = from_behind(normed[rows - EDGE :], "sp")
    block = jnp.concatenate([edge, normed], axis=0)
    blocks = [block] + [shifted(block, "tp", k) for k in range(1, parts)]

    joined = jnp.concatenate([behind, docs], axis=1)
    same = jnp.stack([joined[:, 1 : rows + 1] == docs, joined[:, :rows] == docs], axis=-1)
    same = jnp.pad(same.astype(jnp.float32), ((0, 0), (EDGE, 0), (0, 0)))
    order = (own - jnp.arange(parts)) % parts
    pick = (order[:, None] == jnp.arange(seqs)[None, :]).astype(jnp.float32)
    same = jnp.sum(pick[:, :, None, None] * same[None], axis=1)
    partial = feed_forward(
        blocks, weights, same.reshape(parts * (rows + EDGE), 2), conv_gate, conv_value
    )
    out = mid + partial[0].astype(jnp.float32)
    for k in range(1, parts):
        out = out + shifted(partial[k], "tp", -k).astype(jnp.float32)
    return out.astype(jnp.bfloat16)[None]


def solution(mesh):
    placed = (
        P(("grp", "tp"), "sp", None),
        P("grp", "sp", "tp"),
        P("grp", "sp", "tp"),
        P("grp", "sp", "tp"),
        P("grp", "sp", "tp"),
        P("grp", "sp", "tp"),
        P("tp"),
        P(),
        P("grp", "sp"),
        P("tp", None),
        P(),
        P("sp", "tp"),
        P("sp", "tp"),
        P(None, "tp"),
        P(None, "tp"),
        P("tp", "sp"),
    )
    return jax.shard_map(
        per_device,
        mesh=mesh,
        in_specs=placed,
        out_specs=P(("grp", "tp"), "sp", None),
        check_vma=False,
    )
```

time: 288 us -> 203 us (0.70)
  matrix products: 57.2 us -> 1.71 us
  local copies, waits for them, and re-layouts: 34.2 us -> 8.02 us
  Pallas kernels: 0 us -> 23.7 us
  other arithmetic: 34.8 us -> 11.4 us
  waiting for transfers between devices: 43.5 us -> 37.6 us
  blocking collectives: 86.1 us -> 90.7 us
    dot_general x20 -> x1, matrix products: 57.2 us -> 1.71 us  [per_device(): jnp.dot(heads_out.reshape(seqs * rows, -1), out_weight, preferred_element...]
    all_gather x1, blocking collectives: 50.6 us -> 90.7 us  [per_device(): everyone = lax.all_gather(sent, 'sp', axis=0, tiled=False)]
    ppermute x2 -> x10, waiting for transfers between devices: 1.64 us -> 37.6 us  [the longest x9 35.9 us: shifted(): lax.ppermute(array, axis, [(i, (i + by) % length) for i in range(length)])]
    all_to_all x2 -> x0, blocking collectives: 35.5 us -> none  [sum_at_owner(): tiles = lax.all_to_all(split_up(array, dim, length), axis, 0, 0, tiled=True)]
    all_gather x2 -> x1, waiting for transfers between devices: 33.1 us -> 0.01 us  [per_device(): weights = lax.all_gather(packed, 'sp', axis=0, tiled=True)]
    pallas_call x0 -> x2, Pallas kernels: none -> 23.7 us  [the longest x1 12 us: attend(): pl.pallas_call(body, out_shape=jax.ShapeDtypeStruct((seqs, rows, heads *...]
    reduce_sum x8 -> x2, other arithmetic: 23.3 us -> 1.41 us  [the longest x1 1.32 us: per_device(): meansq = jnp.mean(mid * mid, axis=-1, keepdims=True)]
    dynamic_slice x20 -> x0, local copies, waits for them, and re-layouts: 15.5 us -> none  [the longest x4 4.74 us: inner(): lax.dynamic_slice_in_dim(keys_two, offset, step_len, 1)]
  transfers between devices with their start and end apart: 5 -> 11, of which waited for: 4 -> 9; matrix products, arithmetic and copies ran while one was open for 37% -> 7% of each run, Pallas kernels for 0% -> 6%
where the time goes in v1:
time: 203 us; the launch traced here: 202 us
  blocking collectives  90.7 us (45%)
  waiting for transfers between devices  37.6 us (19%)
  Pallas kernels  23.7 us (12%)
  starting transfers between devices  15.4 us (8%)
  between operations  13.7 us (7%)
  other arithmetic  11.4 us (6%)
  local copies, waits for them, and re-layouts  8.02 us (4%)
    all_gather x1, blocking collectives, per_device(): everyone = lax.all_gather(sent, 'sp', axis=0, tiled=False)  90.7 us
    ppermute x9, waiting for transfers between devices, shifted(): lax.ppermute(array, axis, [(i, (i + by) % length) for i in range(length)])  35.9 us
    ppermute x9, starting transfers between devices, shifted(): lax.ppermute(array, axis, [(i, (i + by) % length) for i in range(length)])  12.4 us
    pallas_call x1, Pallas kernels, attend(): pl.pallas_call(body, out_shape=jax.ShapeDtypeStruct((seqs, rows, heads *...  12 us
    pallas_call x1, Pallas kernels, feed_forward(): pl.pallas_call(body, out_shape=jax.ShapeDtypeStruct((count, rows, width),...  11.7 us
  transfers between devices with their start and end apart: 11, of which 9 were waited for; matrix products, arithmetic and copies ran while one was open for 7% of the time, Pallas kernels for 6%

profile of v1, /device:TPU:33, one launch (start us, length us, event | category | flops | bytes accessed | tf_op | source)
XLA Modules:
  0.0 202.2 jit_solution(8773421514869111944)
XLA Ops:
  6.6 0.1 all-gather.3.cloned.1.call-start
  6.6 2.1 %pad_maximum_fusion = bf16[64,4224]{1,0:T(8,128)(2,1)} fusion(bf16[64,1408]{1,0:T(8,128)(2,1)} %bitcast.42, bf16[64,1408]{1,0:T(8,128)(2,1)} %param.28, bf16[64,1408]{1,0:T(8,128)(2,1)} %param.27), kind=kLoop, calls=%fused_computation.2 | loop fusion | flops 1622016 | bytes 1081344 | tf_op jit(solution)/shard_map/concatenate | solution.py:252
  8.7 0.1 all-gather.3.cloned.1.call-update
  8.8 0.1 multiply_cosine_fusion
  9.0 0.1 copy.53.c_ref
  9.0 0.0 copy-start.4
  9.1 0.1 copy.54.s_ref
  9.1 0.0 copy-start.5
  9.1 0.7 convert_element_type.101
  9.8 0.7 multiply_convert_fusion.4
  10.5 0.1 tile.39
  10.6 0.7 copy.55
  11.3 0.7 tile.40
  12.0 0.7 reshape_tile.3.g_ref
  12.6 0.6 pad_add_fusion.1.place_ref
  13.2 1.0 maximum_convert_fusion
  14.3 0.1 fusion.19
  14.4 0.1 fusion.20
  14.5 0.2 multiply_convert_fusion.3
  14.7 90.7 %all-gather.4 = f16[32,264,256]{2,1,0:T(8,128)(2,1)S(1)} all-gather(f16[1,264,256]{2,1,0:T(8,128)(2,1)S(1)} %pad_maximum_fusion.2), channel_id=1, replica_groups=mesh['grp'=2,'sp'=32,'tp'=4] {'sp'}, dimensions={0}, use_global_device_ids=true | all-gather | bytes 4460544 | tf_op jit(solution)/shard_map/all_gather | solution.py:267
  105.4 0.0 copy-done.5
  105.4 2.2 %multiply_convert_fusion.w_ref = bf16[18,264,256]{2,1,0:T(8,128)(2,1)} fusion(f32[256]{0:T(256)S(1)} %compare_select_fusion.2, f16[32,264,256]{2,1,0:T(8,128)(2,1)S(1)} %all-gather.4, s32[]{:T(128)S(6)} %min.4), kind=kLoop, calls=%fused_computation | loop fusion | flops 3649536 | bytes 4867076 | tf_op jit(solution)/shard_map/convert_element_type | solution.py:274
  107.7 0.5 copy-done.1
  108.2 12.0 %attend.1 = bf16[4,64,512]{2,1,0:T(8,128)(2,1)} custom-call(s32[3]{0:T(128)} %pad_add_fusion.1.place_ref, f32[8]{0:T(128)} %lam_ref.1, bf16[4,64,256]{2,1,0:T(8,128)(2,1)} %q1_ref.1, bf16[4,64,256]{2,1,0:T(8,128)(2,1)} %q2_ref.1, bf16[18,264,256]{2,1,0:T(8,128)(2,1)} %multiply_convert_fusion.w_ref, f32[64,128]{1,0:T(8,128)} %copy-done.4, ...), custom_call_target="tpu_custom_call" | custom-call | tf_op jit(solution)/shard_map/attend/pallas_call | solution.py:134
  120.2 0.0 copy-done
  120.2 1.7 convolution_convert_fusion
  121.9 1.0 copy-done.2
  122.9 0.8 fusion.18
  123.7 1.3 collective-permute-start
  125.0 2.8 %collective-permute-start.1 = (bf16[64,2048]{1,0:T(8,128)(2,1)S(1)}, bf16[64,2048]{1,0:T(8,128)(2,1)S(1)}, u32[]{:S(2)}, u32[]{:S(2)}) collective-permute-start(bf16[64,2048]{1,0:T(8,128)(2,1)S(1)} %get-tuple-element.12), channel_id=1, source_target_pairs={{0,2},{1,3},{2,0},{3,1},{4,6},{5,7},{6,4},{7,5},{8,10},{9,11},{10,... | collective-permute-start | bytes 786440 | tf_op jit(solution)/shard_map/ppermute | solution.py:22
  127.8 0.9 collective-permute-start.2
  128.7 0.9 dynamic-slice_bitcast_fusion
  129.6 0.1 multiply_select_fusion
  129.7 0.1 pad_maximum_fusion.6
  129.8 0.1 fusion.13
  129.8 0.1 pad_convert_fusion
  129.9 3.5 %collective-permute-done = bf16[64,2048]{1,0:T(8,128)(2,1)S(1)} collective-permute-done((bf16[64,2048]{1,0:T(8,128)(2,1)}, bf16[64,2048]{1,0:T(8,128)(2,1)S(1)}, u32[]{:S(2)}, u32[]{:S(2)}) %collective-permute-start) | collective-permute-done | bytes 262176 | tf_op jit(solution)/shard_map/ppermute | solution.py:22
  133.4 6.5 %collective-permute-done.1 = bf16[64,2048]{1,0:T(8,128)(2,1)S(1)} collective-permute-done((bf16[64,2048]{1,0:T(8,128)(2,1)S(1)}, bf16[64,2048]{1,0:T(8,128)(2,1)S(1)}, u32[]{:S(2)}, u32[]{:S(2)}) %collective-permute-start.1) | collective-permute-done | bytes 262176 | tf_op jit(solution)/shard_map/ppermute | solution.py:22
  139.9 0.0 collective-permute-done.2
  139.9 1.3 multiply_reduce_fusion
  141.3 0.0 copy-done.13
  141.3 0.1 multiply_convert_fusion.1
  141.4 2.9 %collective-permute-start.3 = (bf16[8,2048]{1,0:T(8,128)(2,1)S(1)}, bf16[8,2048]{1,0:T(8,128)(2,1)S(1)}, u32[]{:S(2)}, u32[]{:S(2)}) collective-permute-start(bf16[8,2048]{1,0:T(8,128)(2,1)S(1)} %slice.80), channel_id=1, source_target_pairs={{0,4},{4,8},{8,12},{12,16},{16,20},{20,24},{24,28},{28,32},{32,36}... | collective-permute-start | bytes 98312 | tf_op jit(solution)/shard_map/ppermute | solution.py:27
  144.4 1.6 collective-permute-done.3
  146.0 0.9 collective-permute-start.4
  146.9 2.1 %collective-permute-start.5 = (bf16[72,2048]{1,0:T(8,128)(2,1)S(1)}, bf16[72,2048]{1,0:T(8,128)(2,1)S(1)}, u32[]{:S(2)}, u32[]{:S(2)}) collective-permute-start(bf16[72,2048]{1,0:T(8,128)(2,1)S(1)} %pad_maximum_fusion.1.x0), channel_id=1, source_target_pairs={{0,2},{1,3},{2,0},{3,1},{4,6},{5,7},{6,4},{7,5},{8,10},{9,11},{10,... | collective-permute-start | bytes 884744 | tf_op jit(solution)/shard_map/ppermute | solution.py:22
  149.0 1.3 collective-permute-start.6
  150.3 0.1 fusion.12
  150.4 0.1 multiply_reduce_fusion.1
  150.5 0.8 copy.58
  151.3 4.0 %collective-permute-done.4.x1 = bf16[72,2048]{1,0:T(8,128)(2,1)S(1)} collective-permute-done((bf16[72,2048]{1,0:T(8,128)(2,1)S(1)}, bf16[72,2048]{1,0:T(8,128)(2,1)S(1)}, u32[]{:S(2)}, u32[]{:S(2)}) %collective-permute-start.4) | collective-permute-done | bytes 294944 | tf_op jit(solution)/shard_map/ppermute | solution.py:22
  155.3 6.9 %collective-permute-done.5.x2 = bf16[72,2048]{1,0:T(8,128)(2,1)S(1)} collective-permute-done((bf16[72,2048]{1,0:T(8,128)(2,1)S(1)}, bf16[72,2048]{1,0:T(8,128)(2,1)S(1)}, u32[]{:S(2)}, u32[]{:S(2)}) %collective-permute-start.5) | collective-permute-done | bytes 294944 | tf_op jit(solution)/shard_map/ppermute | solution.py:22
  162.2 0.4 collective-permute-done.6.x3
  162.6 0.0 copy-done.3
  162.6 0.3 copy-done.7
  162.9 11.7 %feed_forward.1 = bf16[4,64,2048]{2,1,0:T(8,128)(2,1)} custom-call(bf16[72,2048]{1,0:T(8,128)(2,1)} %copy-done.3, bf16[72,2048]{1,0:T(8,128)(2,1)} %copy-done.6, bf16[72,2048]{1,0:T(8,128)(2,1)} %copy-done.7, bf16[72,2048]{1,0:T(8,128)(2,1)} %collective-permute-done.6.x3, f32[288,2]{1,0:T(8,128)} %bitcast.38, f32[3,1408]{1,0:T(4,128)} %cg_ref.1, ...), custom_call_target="tpu_custom_call" | custom-call | tf_op jit(solution)/shard_map/feed_forward/pallas_call | solution.py:210
  174.7 1.2 slice_bitcast_fusion.2
  175.8 2.4 %collective-permute-start.7 = (bf16[64,2048]{1,0:T(8,128)(2,1)S(1)}, bf16[64,2048]{1,0:T(8,128)(2,1)S(1)}, u32[]{:S(2)}, u32[]{:S(2)}) collective-permute-start(bf16[64,2048]{1,0:T(8,128)(2,1)S(1)} %get-tuple-element.7), channel_id=1, source_target_pairs={{0,3},{1,0},{2,1},{3,2},{4,7},{5,4},{6,5},{7,6},{8,11},{9,8},{10,9... | collective-permute-start | bytes 786440 | tf_op jit(solution)/shard_map/ppermute | solution.py:22
  178.2 0.6 collective-permute-start.8
  178.9 0.1 collective-permute-start.9
  179.0 5.0 %collective-permute-done.7 = bf16[64,2048]{1,0:T(8,128)(2,1)S(1)} collective-permute-done((bf16[64,2048]{1,0:T(8,128)(2,1)S(1)}, bf16[64,2048]{1,0:T(8,128)(2,1)S(1)}, u32[]{:S(2)}, u32[]{:S(2)}) %collective-permute-start.7) | collective-permute-done | bytes 262176 | tf_op jit(solution)/shard_map/ppermute | solution.py:22
  184.0 3.0 %collective-permute-done.8 = bf16[64,2048]{1,0:T(8,128)(2,1)S(1)} collective-permute-done((bf16[64,2048]{1,0:T(8,128)(2,1)S(1)}, bf16[64,2048]{1,0:T(8,128)(2,1)S(1)}, u32[]{:S(2)}, u32[]{:S(2)}) %collective-permute-start.8) | collective-permute-done | bytes 262176 | tf_op jit(solution)/shard_map/ppermute | solution.py:22
  187.0 6.6 %collective-permute-done.9 = bf16[64,2048]{1,0:T(8,128)(2,1)S(1)} collective-permute-done((bf16[64,2048]{1,0:T(8,128)(2,1)S(1)}, bf16[64,2048]{1,0:T(8,128)(2,1)S(1)}, u32[]{:S(2)}, u32[]{:S(2)}) %collective-permute-start.9) | collective-permute-done | bytes 262176 | tf_op jit(solution)/shard_map/ppermute | solution.py:22
  193.6 1.8 fusion.7
  (37 shorter events, 0.2 us)
Async XLA Ops:
  6.5 113.6 %copy-start = (bf16[512,2048]{1,0:T(8,128)(2,1)S(1)}, bf16[512,2048]{1,0:T(8,128)(2,1)}, u32[]{:S(2)}) copy-start(bf16[512,2048]{1,0:T(8,128)(2,1)} %param.25) | copy-start | bytes 6291460
  6.6 7.9 %copy-start.10 = (bf16[4,64,64]{2,1,0:T(8,128)(2,1)S(1)}, bf16[4,64,64]{2,1,0:T(8,128)(2,1)}, u32[]{:S(2)}) copy-start(bf16[4,64,64]{2,1,0:T(8,128)(2,1)} %param.18) | copy-start | bytes 98308
  6.6 7.9 %copy-start.9 = (bf16[4,64,64]{2,1,0:T(8,128)(2,1)S(1)}, bf16[4,64,64]{2,1,0:T(8,128)(2,1)}, u32[]{:S(2)}) copy-start(bf16[4,64,64]{2,1,0:T(8,128)(2,1)} %param.20) | copy-start | bytes 98308
  6.6 7.7 %copy-start.11 = (bf16[4,64,128]{2,1,0:T(8,128)(2,1)S(1)}, bf16[4,64,128]{2,1,0:T(8,128)(2,1)}, u32[]{:S(2)}) copy-start(bf16[4,64,128]{2,1,0:T(8,128)(2,1)} %param.21) | copy-start | bytes 196612
  6.6 156.0 %all-gather.3.cloned.1.call-start = ((), (), s32[]{:S(2)}) async-start(), calls=%async_computation | async-start | bytes 17842176 | tf_op jit(solution)/shard_map/all_gather | solution.py:253
  9.0 96.4 %copy-start.4 = (f32[64,128]{1,0:T(8,128)}, f32[64,128]{1,0:T(8,128)S(1)}, u32[]{:S(2)}) copy-start(f32[64,128]{1,0:T(8,128)S(1)} %copy.53.c_ref) | copy-start | bytes 98308
  9.1 96.3 %copy-start.5 = (f32[64,128]{1,0:T(8,128)}, f32[64,128]{1,0:T(8,128)S(1)}, u32[]{:S(2)}) copy-start(f32[64,128]{1,0:T(8,128)S(1)} %copy.54.s_ref) | copy-start | bytes 98308
  105.4 2.8 %copy-start.1 = (f16[32,264,256]{2,1,0:T(8,128)(2,1)}, f16[32,264,256]{2,1,0:T(8,128)(2,1)S(1)}, u32[]{:S(2)}) copy-start(f16[32,264,256]{2,1,0:T(8,128)(2,1)S(1)} %all-gather.4) | copy-start | bytes 12976132
  120.2 9.6 %copy-start.12 = (s32[4,64]{1,0:T(4,128)S(1)}, s32[4,64]{1,0:T(4,128)}, u32[]{:S(2)}) copy-start(s32[4,64]{1,0:T(4,128)} %param.24) | copy-start | bytes 3076
  120.2 19.8 %copy-start.8 = (bf16[1,64,2048]{2,1,0:T(8,128)(2,1)S(1)}, bf16[1,64,2048]{2,1,0:T(8,128)(2,1)}, u32[]{:S(2)}) copy-start(bf16[1,64,2048]{2,1,0:T(8,128)(2,1)} %param.16) | copy-start | bytes 786436
  121.9 1.0 copy-start.2
  122.9 18.4 %copy-start.13 = (f32[2048]{0:T(1024)S(1)}, f32[2048]{0:T(1024)}, u32[]{:S(2)}) copy-start(f32[2048]{0:T(1024)} %param.26) | copy-start | bytes 24580
  123.7 9.8 %collective-permute-start = (bf16[64,2048]{1,0:T(8,128)(2,1)}, bf16[64,2048]{1,0:T(8,128)(2,1)S(1)}, u32[]{:S(2)}, u32[]{:S(2)}) collective-permute-start(bf16[64,2048]{1,0:T(8,128)(2,1)} %get-tuple-element.10), channel_id=1, source_target_pairs={{0,1},{1,2},{2,3},{3,0},{4,5},{5,6},{6,7},{7,4},{8,9},{9,10},{10,1... | collective-permute-start | bytes 786440 | tf_op jit(solution)/shard_map/ppermute | solution.py:22
  125.0 15.0 %collective-permute-start.1 = (bf16[64,2048]{1,0:T(8,128)(2,1)S(1)}, bf16[64,2048]{1,0:T(8,128)(2,1)S(1)}, u32[]{:S(2)}, u32[]{:S(2)}) collective-permute-start(bf16[64,2048]{1,0:T(8,128)(2,1)S(1)} %get-tuple-element.12), channel_id=1, source_target_pairs={{0,2},{1,3},{2,0},{3,1},{4,6},{5,7},{6,4},{7,5},{8,10},{9,11},{10,... | collective-permute-start | bytes 786440 | tf_op jit(solution)/shard_map/ppermute | solution.py:22
  127.8 12.2 %collective-permute-start.2 = (bf16[64,2048]{1,0:T(8,128)(2,1)S(1)}, bf16[64,2048]{1,0:T(8,128)(2,1)}, u32[]{:S(2)}, u32[]{:S(2)}) collective-permute-start(bf16[64,2048]{1,0:T(8,128)(2,1)S(1)} %get-tuple-element.11), channel_id=1, source_target_pairs={{0,3},{1,0},{2,1},{3,2},{4,7},{5,4},{6,5},{7,6},{8,11},{9,8},{10,9... | collective-permute-start | bytes 786440 | tf_op jit(solution)/shard_map/ppermute | solution.py:22
  141.4 4.6 %collective-permute-start.3 = (bf16[8,2048]{1,0:T(8,128)(2,1)S(1)}, bf16[8,2048]{1,0:T(8,128)(2,1)S(1)}, u32[]{:S(2)}, u32[]{:S(2)}) collective-permute-start(bf16[8,2048]{1,0:T(8,128)(2,1)S(1)} %slice.80), channel_id=1, source_target_pairs={{0,4},{4,8},{8,12},{12,16},{16,20},{20,24},{24,28},{28,32},{32,36}... | collective-permute-start | bytes 98312 | tf_op jit(solution)/shard_map/ppermute | solution.py:27
  146.0 16.6 %copy-start.3 = (bf16[72,2048]{1,0:T(8,128)(2,1)}, bf16[72,2048]{1,0:T(8,128)(2,1)S(1)}, u32[]{:S(2)}) copy-start(bf16[72,2048]{1,0:T(8,128)(2,1)S(1)} %pad_maximum_fusion.1.x0) | copy-start | bytes 884740
  146.0 9.2 %collective-permute-start.4 = (bf16[72,2048]{1,0:T(8,128)(2,1)S(1)}, bf16[72,2048]{1,0:T(8,128)(2,1)S(1)}, u32[]{:S(2)}, u32[]{:S(2)}) collective-permute-start(bf16[72,2048]{1,0:T(8,128)(2,1)S(1)} %pad_maximum_fusion.1.x0), channel_id=1, source_target_pairs={{0,1},{1,2},{2,3},{3,0},{4,5},{5,6},{6,7},{7,4},{8,9},{9,10},{10,1... | collective-permute-start | bytes 884744 | tf_op jit(solution)/shard_map/ppermute | solution.py:22
  146.9 15.3 %collective-permute-start.5 = (bf16[72,2048]{1,0:T(8,128)(2,1)S(1)}, bf16[72,2048]{1,0:T(8,128)(2,1)S(1)}, u32[]{:S(2)}, u32[]{:S(2)}) collective-permute-start(bf16[72,2048]{1,0:T(8,128)(2,1)S(1)} %pad_maximum_fusion.1.x0), channel_id=1, source_target_pairs={{0,2},{1,3},{2,0},{3,1},{4,6},{5,7},{6,4},{7,5},{8,10},{9,11},{10,... | collective-permute-start | bytes 884744 | tf_op jit(solution)/shard_map/ppermute | solution.py:22
  149.0 13.6 %collective-permute-start.6 = (bf16[72,2048]{1,0:T(8,128)(2,1)S(1)}, bf16[72,2048]{1,0:T(8,128)(2,1)}, u32[]{:S(2)}, u32[]{:S(2)}) collective-permute-start(bf16[72,2048]{1,0:T(8,128)(2,1)S(1)} %pad_maximum_fusion.1.x0), channel_id=1, source_target_pairs={{0,3},{1,0},{2,1},{3,2},{4,7},{5,4},{6,5},{7,6},{8,11},{9,8},{10,9... | collective-permute-start | bytes 884744 | tf_op jit(solution)/shard_map/ppermute | solution.py:22
  155.3 7.3 %copy-start.6 = (bf16[72,2048]{1,0:T(8,128)(2,1)}, bf16[72,2048]{1,0:T(8,128)(2,1)S(1)}, u32[]{:S(2)}) copy-start(bf16[72,2048]{1,0:T(8,128)(2,1)S(1)} %collective-permute-done.4.x1) | copy-start | bytes 884740
  162.2 0.7 copy-start.7
  175.8 8.1 %collective-permute-start.7 = (bf16[64,2048]{1,0:T(8,128)(2,1)S(1)}, bf16[64,2048]{1,0:T(8,128)(2,1)S(1)}, u32[]{:S(2)}, u32[]{:S(2)}) collective-permute-start(bf16[64,2048]{1,0:T(8,128)(2,1)S(1)} %get-tuple-element.7), channel_id=1, source_target_pairs={{0,3},{1,0},{2,1},{3,2},{4,7},{5,4},{6,5},{7,6},{8,11},{9,8},{10,9... | collective-permute-start | bytes 786440 | tf_op jit(solution)/shard_map/ppermute | solution.py:22
  178.2 8.7 %collective-permute-start.8 = (bf16[64,2048]{1,0:T(8,128)(2,1)S(1)}, bf16[64,2048]{1,0:T(8,128)(2,1)S(1)}, u32[]{:S(2)}, u32[]{:S(2)}) collective-permute-start(bf16[64,2048]{1,0:T(8,128)(2,1)S(1)} %get-tuple-element.9), channel_id=1, source_target_pairs={{0,2},{1,3},{2,0},{3,1},{4,6},{5,7},{6,4},{7,5},{8,10},{9,11},{10,... | collective-permute-start | bytes 786440 | tf_op jit(solution)/shard_map/ppermute | solution.py:22
  178.9 14.7 %collective-permute-start.9 = (bf16[64,2048]{1,0:T(8,128)(2,1)S(1)}, bf16[64,2048]{1,0:T(8,128)(2,1)S(1)}, u32[]{:S(2)}, u32[]{:S(2)}) collective-permute-start(bf16[64,2048]{1,0:T(8,128)(2,1)S(1)} %get-tuple-element.8), channel_id=1, source_target_pairs={{0,1},{1,2},{2,3},{3,0},{4,5},{5,6},{6,7},{7,4},{8,9},{9,10},{10,1... | collective-permute-start | bytes 786440 | tf_op jit(solution)/shard_map/ppermute | solution.py:22
Sparse Core Ops, SparseCore 0:
  9.2 142.9 all-gather.2

commit v2 on v1

v2 whole, which is shorter than its diff:
```python
import math

import jax
import jax.numpy as jnp
from jax import lax
from jax.experimental import pallas as pl
from jax.experimental.pallas import tpu as pltpu
from jax.sharding import PartitionSpec as P

NORM_EPS = 1e-06
ROPE_BASE = 500000.0
LOG2E = math.log2(math.e)
DOC_SPAN = 1024
KEY_UP = 4096.0
VAL_UP = 8192.0
LANES = 128
EDGE = 8


def shifted(array, axis, by):
    length = lax.axis_size(axis)
    return lax.ppermute(array, axis, [(i, (i + by) % length) for i in range(length)])


def from_behind(array, axis):
    length = lax.axis_size(axis)
    return lax.ppermute(array, axis, [(i, i + 1) for i in range(length - 1)])


def turn_tables(positions, width):
    half = width // 2
    freqs = ROPE_BASE ** (-jnp.arange(half, dtype=jnp.float32) * 2.0 / width)
    angles = positions.astype(jnp.float32)[:, None] * freqs[None, :]
    cosine = jnp.cos(angles)
    sine = jnp.sin(angles)
    times = LANES // width
    return (
        jnp.tile(jnp.concatenate([cosine, cosine], axis=1), (1, times)),
        jnp.tile(jnp.concatenate([-sine, sine], axis=1), (1, times)),
    )


def attend(place, q_one, q_two, window, cosine, sine, docs, gain, lam, out_weight, after):
    seqs, rows, q_lanes = q_one.shape
    ranks, per_rank, _ = window.shape
    keys = ranks * rows
    heads = lam.shape[0]
    width = q_lanes // heads
    half = width // 2
    kv_heads = 2
    group = heads // kv_heads
    head_width = LANES // kv_heads
    mult = width ** (-0.5) * LOG2E
    model = out_weight.shape[1]

    def body(
        place_ref, lam_ref, q1_ref, q2_ref, w_ref, e_ref, c_ref, s_ref, d_ref, g_ref, p_ref, _,
        o_ref, m_ref, h_ref,
    ):
        s = place_ref[0]
        first_key = place_ref[1]
        first_row = place_ref[2]
        lane = lax.broadcasted_iota(jnp.int32, (rows, LANES), 1)
        low = (lane % width) < half
        cos = c_ref[...]
        sin = s_ref[...]
        gain_row = jnp.concatenate([g_ref[...], g_ref[...]], axis=1)
        k_all = w_ref[:, :, 0:LANES].reshape(keys, LANES)
        v_all = w_ref[:, :, LANES : 2 * LANES].reshape(keys, LANES)
        v_ext = jnp.concatenate([v_all, jnp.ones((keys, LANES), jnp.bfloat16)], axis=1)

        placed = []
        for ref in (q1_ref, q2_ref):
            tiles = []
            for h in range(kv_heads):
                x = ref[0, :, h * LANES : (h + 1) * LANES].astype(jnp.float32)
                swap = jnp.where(low, pltpu.roll(x, LANES - half, 1), pltpu.roll(x, half, 1))
                tiles.append((x * cos + swap * sin).astype(jnp.bfloat16).astype(jnp.float32))
            placed.append(tiles)

        def scores(h, c):
            target = c * kv_heads + h
            inside = (lane // width) == target
            parts = []
            for g in range(group):
                by = (width * (target - g)) % LANES
                x = placed[c][h]
                x = pltpu.roll(x, by, 1) if by else x
                parts.append(jnp.where(inside, x, 0.0).astype(jnp.bfloat16))
            q = jnp.concatenate(parts, axis=0)
            return lax.dot_general(
                q, k_all, (((1,), (1,)), ((), ())), preferred_element_type=jnp.float32
            )

        key_pos = first_key + lax.broadcasted_iota(jnp.int32, (rows, keys), 1)
        row_pos = first_row + lax.broadcasted_iota(jnp.int32, (rows, keys), 0)
        even_lane = lax.broadcasted_iota(jnp.int32, (1, LANES), 1) < rows
        this_row = lax.broadcasted_iota(jnp.int32, (EDGE, LANES), 0) == s
        pieces = []
        for i in range(ranks // 2):
            two = [
                jnp.sum(
                    jnp.where(this_row, e_ref[2 * i + b, :, 0:LANES].astype(jnp.float32), 0.0),
                    axis=0,
                    keepdims=True,
                )
                for b in range(2)
            ]
            pieces.append(jnp.where(even_lane, two[0], two[1]))
        key_doc = jnp.concatenate(pieces, axis=1)
        diagonal = lax.broadcasted_iota(jnp.int32, (rows, rows), 0) == lax.broadcasted_iota(
            jnp.int32, (rows, rows), 1
        )
        row_doc = jnp.sum(
            jnp.where(diagonal, d_ref[pl.ds(s, 1), :].astype(jnp.float32), 0.0),
            axis=1,
            keepdims=True,
        )
        equal = key_doc == row_doc
        bias = jnp.where((key_pos <= row_pos) & equal, 0.0, -1e30)
        ones_back = [
            jnp.sum(
                jnp.where(equal & (key_pos == row_pos - by), 1.0, 0.0), axis=1, keepdims=True
            )
            for by in (1, 2)
        ]
        m_ref[...] = jnp.where(lane == 0, ones_back[0], ones_back[1])

        pairs = [(h, c) for h in range(kv_heads) for c in range(2)]
        upcoming = scores(*pairs[0])
        results = []
        for at in range(len(pairs)):
            score = upcoming
            if at + 1 < len(pairs):
                upcoming = scores(*pairs[at + 1])
            score = score.reshape(group, rows, keys) + bias[None]
            peak = jnp.max(score, axis=-1, keepdims=True)
            expd = jnp.exp2((score - peak) * mult).astype(jnp.bfloat16)
            both = jnp.dot(
                expd.reshape(group * rows, keys), v_ext, preferred_element_type=jnp.float32
            )
            results.append(both[:, :LANES] / both[:, LANES:])
        for h in range(kv_heads):
            here = (lane // head_width) == h
            outs = []
            for g in range(group):
                a = results[2 * h][g * rows : (g + 1) * rows]
                b = results[2 * h + 1][g * rows : (g + 1) * rows]
                o = jnp.where(here, a - lam_ref[h * group + g] * b, 0.0)
                meansq = jnp.sum(o * o, axis=-1, keepdims=True) * (1.0 / head_width)
                o = o * lax.rsqrt(meansq + NORM_EPS) * gain_row
                if (g % 2) != h:
                    o = pltpu.roll(o, head_width, 1)
                outs.append(o)
            for j in range(group // 2):
                tile = (h * group) // 2 + j
                h_ref[:, tile * LANES : (tile + 1) * LANES] = (
                    outs[2 * j] + outs[2 * j + 1]
                ).astype(jnp.bfloat16)
        o_ref[...] = jnp.dot(
            h_ref[...], p_ref[...], preferred_element_type=jnp.float32
        ).astype(jnp.bfloat16)

    whole = lambda *shape: pl.BlockSpec(shape, lambda i, p: (0,) * len(shape))
    smem = pl.BlockSpec(memory_space=pltpu.SMEM)
    return pl.pallas_call(
        body,
        out_shape=(
            jax.ShapeDtypeStruct((rows, model), jnp.bfloat16),
            jax.ShapeDtypeStruct((rows, LANES), jnp.float32),
        ),
        grid_spec=pltpu.PrefetchScalarGridSpec(
            num_scalar_prefetch=1,
            grid=(1,),
            in_specs=[
                smem,
                pl.BlockSpec((1, rows, q_lanes), lambda i, p: (p[0], 0, 0)),
                pl.BlockSpec((1, rows, q_lanes), lambda i, p: (p[0], 0, 0)),
                pl.BlockSpec((ranks, rows, 2 * LANES), lambda i, p: (0, p[0], 0)),
                pl.BlockSpec((ranks, EDGE, 2 * LANES), lambda i, p: (0, seqs * rows // EDGE, 0)),
                whole(rows, LANES),
                whole(rows, LANES),
                whole(seqs, rows),
                whole(1, head_width),
                whole(*out_weight.shape),
                pl.BlockSpec(memory_space=pl.ANY),
            ],
            out_specs=(whole(rows, model), whole(rows, LANES)),
            scratch_shapes=[pltpu.VMEM((rows, heads * head_width), jnp.bfloat16)],
        ),
        cost_estimate=pl.CostEstimate(flops=3_000_000_000, transcendentals=0, bytes_accessed=4_000_000),
        name="attend",
    )(place, lam, q_one, q_two, window, window, cosine, sine, docs, gain, out_weight, after)


def feed_forward(blocks, edges, same, weights, conv_gate, conv_value):
    rows, width = blocks[0].shape
    count = len(blocks)
    span = rows + EDGE
    total = span * count
    hidden = conv_gate.shape[1]
    step = 2 * LANES
    cuts = [(a, min(a + step, hidden)) for a in range(0, hidden, step)]
    out_step = 4 * LANES

    def body(*refs):
        x_in, e_in, m_in = refs[:count], refs[count : 2 * count], refs[2 * count : 3 * count]
        cg_ref, cv_ref, w_hbm = refs[3 * count : 3 * count + 3]
        outs = refs[3 * count + 3 : 4 * count + 3]
        x_ref, w_ref, h_ref, b_ref, sems = refs[4 * count + 3 :]

        def piece(base, a, b, at):
            return pltpu.make_async_copy(
                w_hbm.at[:, base + a : base + b], w_ref.at[:, base + a : base + b], sems.at[at]
            )

        ups = [
            [piece(base, a, b, 2 * j + n) for n, base in enumerate((0, hidden))]
            for j, (a, b) in enumerate(cuts)
        ]
        down = piece(2 * hidden, 0, hidden, 2 * len(cuts))
        for both in ups:
            for copy in both:
                copy.start()
        down.start()
        for k in range(count):
            x_ref[k * span : k * span + EDGE, :] = e_in[k][...]
            x_ref[k * span + EDGE : (k + 1) * span, :] = x_in[k][...]
            b_ref[k * span : k * span + EDGE, :] = jnp.zeros((EDGE, LANES), jnp.float32)
            b_ref[k * span + EDGE : (k + 1) * span, :] = m_in[k][...]
        one_back = b_ref[:, 0:1]
        two_back = b_ref[:, 1:2]

        def raised(j):
            a, b = cuts[j]
            for copy in ups[j]:
                copy.wait()
            return [
                jnp.dot(
                    x_ref[...], w_ref[:, base + a : base + b], preferred_element_type=jnp.float32
                ).astype(jnp.bfloat16)
                for base in (0, hidden)
            ]

        upcoming = raised(0)
        for j in range(len(cuts)):
            a, b = cuts[j]
            current = upcoming
            if j + 1 < len(cuts):
                upcoming = raised(j + 1)
            convs = []
            for u, taps in zip(current, (cg_ref, cv_ref)):
                u = u.astype(jnp.float32)
                convs.append(
                    taps[2:3, a:b] * u
                    + taps[1:2, a:b] * (one_back * pltpu.roll(u, 1, 0))
                    + taps[0:1, a:b] * (two_back * pltpu.roll(u, 2, 0))
                )
            g, v = convs
            act = g / (1.0 + jnp.exp(-g)) * v
            for k in range(count):
                h_ref[k * rows : (k + 1) * rows, a:b] = act[
                    k * span + EDGE : (k + 1) * span
                ].astype(jnp.bfloat16)
        down.wait()
        for a in range(0, width, out_step):
            part = lax.dot_general(
                h_ref[...],
                w_ref[a : a + out_step, 2 * hidden : 3 * hidden],
                (((1,), (1,)), ((), ())),
                preferred_element_type=jnp.float32,
            ).astype(jnp.bfloat16)
            for k in range(count):
                outs[k][:, a : a + out_step] = part[k * rows : (k + 1) * rows]

    vmem = pl.BlockSpec(memory_space=pltpu.VMEM)
    return pl.pallas_call(
        body,
        out_shape=[jax.ShapeDtypeStruct((rows, width), jnp.bfloat16)] * count,
        in_specs=[vmem] * (3 * count + 2) + [pl.BlockSpec(memory_space=pltpu.HBM)],
        out_specs=[vmem] * count,
        scratch_shapes=[
            pltpu.VMEM((total, width), jnp.bfloat16),
            pltpu.VMEM((width, 3 * hidden), jnp.bfloat16),
            pltpu.VMEM((count * rows, hidden), jnp.bfloat16),
            pltpu.VMEM((total, LANES), jnp.float32),
            pltpu.SemaphoreType.DMA((2 * len(cuts) + 1,)),
        ],
        compiler_params=pltpu.CompilerParams(vmem_limit_bytes=56 * 1024 * 1024),
        name="feed_forward",
    )(*blocks, *edges, *same, conv_gate, conv_value, weights)


def per_device(
    resid_in,
    query_one,
    key_one,
    query_two,
    key_two,
    value,
    lam,
    head_gain,
    doc_ids,
    out_weight,
    norm_gain,
    gate_weight,
    value_weight,
    conv_gate,
    conv_value,
    down_weight,
):
    seqs, rows, q_lanes = query_one.shape
    width = q_lanes // lam.shape[0]
    rank = lax.axis_index("sp")
    ranks = lax.axis_size("sp")
    own = lax.axis_index("tp")
    parts = lax.axis_size("tp")
    model = resid_in.shape[2]

    packed = jnp.concatenate([gate_weight, value_weight, down_weight.T], axis=1)
    weights = lax.all_gather(packed, "sp", axis=0, tiled=True)

    positions = rank * rows + jnp.arange(rows, dtype=jnp.int32)
    cosine, sine = turn_tables(positions, width)
    keys = jnp.concatenate([key_one, key_two], axis=2).astype(jnp.float32)
    half = width // 2
    low = (jnp.arange(LANES) % width) < half
    swap = jnp.where(low, jnp.roll(keys, -half, axis=2), jnp.roll(keys, half, axis=2))
    keys = (keys * cosine + swap * sine).astype(jnp.bfloat16).astype(jnp.float32) * KEY_UP
    vals = value.astype(jnp.float32) * VAL_UP
    body_rows = jnp.concatenate([keys, vals], axis=2).reshape(seqs * rows, 2 * LANES)
    doc_rows = jnp.tile(doc_ids.astype(jnp.float32) * KEY_UP, (1, 2 * LANES // rows))
    doc_rows = jnp.pad(doc_rows, ((0, EDGE - seqs), (0, 0)))
    sent = jnp.concatenate([body_rows, doc_rows], axis=0).astype(jnp.float16)
    everyone = lax.all_gather(sent, "sp", axis=0, tiled=False)

    back = DOC_SPAN // rows
    span = min(back + 2, ranks)
    first = jnp.clip(rank // 2 * 2 - back, 0, ranks - span)
    lanes_down = jnp.where(jnp.arange(2 * LANES) < LANES, 1.0 / KEY_UP, 1.0 / VAL_UP)
    window = lax.dynamic_slice_in_dim(everyone, first, span, 0)
    window = (window.astype(jnp.float32) * lanes_down).astype(jnp.bfloat16)
    gain = head_gain.reshape(1, -1)
    proj = [None] * parts
    same = [None] * parts
    after = lam
    farthest_first = sorted(range(parts), key=lambda k: -min(k, parts - k))
    for k in farthest_first:
        place = jnp.stack([(own + k) % parts, first * rows, rank * rows]).astype(jnp.int32)
        proj[k], same[-k] = attend(
            place, query_one, query_two, window, cosine, sine, doc_ids, gain, lam, out_weight, after
        )
        after = proj[k]
    mid = resid_in[0].astype(jnp.float32) + proj[0].astype(jnp.float32)
    for k in range(1, parts):
        mid = mid + shifted(proj[k], "tp", k).astype(jnp.float32)
    meansq = jnp.mean(mid * mid, axis=-1, keepdims=True)
    normed = (mid * lax.rsqrt(meansq + NORM_EPS) * norm_gain).astype(jnp.bfloat16)
    edge = from_behind(normed[rows - EDGE :], "sp")
    blocks = [normed] + [shifted(normed, "tp", k) for k in range(1, parts)]
    edges = [edge] + [shifted(edge, "tp", k) for k in range(1, parts)]
    partial = feed_forward(blocks, edges, same, weights, conv_gate, conv_value)
    out = mid + partial[0].astype(jnp.float32)
    for k in range(1, parts):
        out = out + shifted(partial[k], "tp", -k).astype(jnp.float32)
    return out.astype(jnp.bfloat16)[None]


def solution(mesh):
    placed = (
        P(("grp", "tp"), "sp", None),
        P("grp", "sp", "tp"),
        P("grp", "sp", "tp"),
        P("grp", "sp", "tp"),
        P("grp", "sp", "tp"),
        P("grp", "sp", "tp"),
        P("tp"),
        P(),
        P("grp", "sp"),
        P("tp", None),
        P(),
        P("sp", "tp"),
        P("sp", "tp"),
        P(None, "tp"),
        P(None, "tp"),
        P("tp", "sp"),
    )
    return jax.shard_map(
        per_device,
        mesh=mesh,
        in_specs=placed,
        out_specs=P(("grp", "tp"), "sp", None),
        check_vma=False,
    )
```

time: 203 us -> 191 us (0.941)
  waiting for transfers between devices: 37.6 us -> 22.9 us
  Pallas kernels: 23.7 us -> 36 us
  local copies, waits for them, and re-layouts: 8.02 us -> 1.31 us
  starting transfers between devices: 15.4 us -> 20 us
  blocking collectives: 90.7 us -> 86.2 us
    ppermute x9 -> x12, waiting for transfers between devices: 35.9 us -> 21.6 us  [shifted(): lax.ppermute(array, axis, [(i, (i + by) % length) for i in range(length)])]
    pallas_call x2 -> x5, Pallas kernels: 23.7 us -> 36 us  [the longest x4 24.7 us: attend(): pl.pallas_call(body, out_shape=(jax.ShapeDtypeStruct((rows, model), jnp.b...]
    all_gather x1, blocking collectives: 90.7 us -> 86.2 us  [per_device(): everyone = lax.all_gather(sent, 'sp', axis=0, tiled=False)]
    ppermute x1, starting transfers between devices: 2.92 us -> 6.36 us  [from_behind(): return lax.ppermute(array, axis, [(i, i + 1) for i in range(length - 1)])]
    squeeze x2 -> x0, local copies, waits for them, and re-layouts: 2.11 us -> none  [the longest x1 1.18 us: per_device(): out = out + shifted(partial[k], 'tp', -k).astype(jnp.float32)]
    ppermute x9 -> x12, starting transfers between devices: 12.4 us -> 13.6 us  [shifted(): lax.ppermute(array, axis, [(i, (i + by) % length) for i in range(length)])]
  transfers between devices with their start and end apart: 11 -> 14, of which waited for: 9 -> 7; matrix products, arithmetic and copies ran while one was open for 7% -> 4% of each run, Pallas kernels for 6% -> 13%
where the time goes in v2:
time: 191 us
  blocking collectives  86.2 us (45%)
  Pallas kernels  36 us (19%)
  waiting for transfers between devices  22.9 us (12%)
  starting transfers between devices  20 us (10%)
  between operations  13.7 us (7%)
  other arithmetic  10.4 us (5%)
    all_gather x1, blocking collectives, per_device(): everyone = lax.all_gather(sent, 'sp', axis=0, tiled=False)  86.2 us
    pallas_call x4, Pallas kernels, attend(): pl.pallas_call(body, out_shape=(jax.ShapeDtypeStruct((rows, model), jnp.b...  24.7 us
    ppermute x12, waiting for transfers between devices, shifted(): lax.ppermute(array, axis, [(i, (i + by) % length) for i in range(length)])  21.6 us
    ppermute x12, starting transfers between devices, shifted(): lax.ppermute(array, axis, [(i, (i + by) % length) for i in range(length)])  13.6 us
    pallas_call x1, Pallas kernels, feed_forward(): pl.pallas_call(body, out_shape=[jax.ShapeDtypeStruct((rows, width), jnp.b...  11.3 us
    ppermute x1, starting transfers between devices, from_behind(): return lax.ppermute(array, axis, [(i, i + 1) for i in range(length - 1)])  6.36 us
  transfers between devices with their start and end apart: 14, of which 7 were waited for; matrix products, arithmetic and copies ran while one was open for 4% of the time, Pallas kernels for 13%

profile of v2, /device:TPU:33, one launch (start us, length us, event | category | flops | bytes accessed | tf_op | source)
XLA Modules:
  0.0 190.6 jit_solution(9082624799311208759)
XLA Ops:
  6.6 0.0 all-gather.3.cloned.1.call-start
  6.6 2.0 %pad_maximum_fusion = bf16[64,4224]{1,0:T(8,128)(2,1)} fusion(bf16[64,1408]{1,0:T(8,128)(2,1)} %bitcast.22, bf16[64,1408]{1,0:T(8,128)(2,1)} %param.28, bf16[64,1408]{1,0:T(8,128)(2,1)} %param.27), kind=kLoop, calls=%fused_computation.1 | loop fusion | flops 1622016 | bytes 1081344 | tf_op jit(solution)/shard_map/concatenate | solution.py:320
  8.6 0.1 all-gather.3.cloned.1.call-update
  8.7 0.1 multiply_cosine_fusion
  8.8 0.1 copy.27.c_ref
  8.9 0.0 copy-start.7
  8.9 0.1 copy.28.s_ref
  9.0 0.0 copy-start.8
  9.0 0.7 multiply_convert_fusion.4
  9.7 0.1 tile.33
  9.8 0.6 add_add_fusion.2
  10.4 1.0 maximum_convert_fusion
  11.4 0.0 copy-done.9
  11.4 0.1 fusion.10
  11.5 0.1 fusion.11
  11.6 0.0 copy-done.6
  11.6 0.0 copy-done.5
  11.7 0.2 multiply_convert_fusion.3
  11.9 86.2 %all-gather.4 = f16[32,264,256]{2,1,0:T(8,128)(2,1)S(1)} all-gather(f16[1,264,256]{2,1,0:T(8,128)(2,1)S(1)} %pad_maximum_fusion.1), channel_id=1, replica_groups=mesh['grp'=2,'sp'=32,'tp'=4] {'sp'}, dimensions={0}, use_global_device_ids=true | all-gather | bytes 4460544 | tf_op jit(solution)/shard_map/all_gather | solution.py:335
  98.1 0.0 copy-done.7
  98.1 0.0 copy-done.8
  98.1 1.9 multiply_convert_fusion.w_ref.e_ref
  100.0 6.1 %attend.4 = (bf16[64,2048]{1,0:T(8,128)(2,1)}, f32[64,128]{1,0:T(8,128)}) custom-call(s32[3]{0:T(128)} %get-tuple-element.41.place_ref, f32[8]{0:T(128)} %lam_ref.7, bf16[4,64,256]{2,1,0:T(8,128)(2,1)} %q1_ref.7, bf16[4,64,256]{2,1,0:T(8,128)(2,1)} %q2_ref.7, bf16[18,264,256]{2,1,0:T(8,128)(2,1)} %multiply_convert_fusion.w_ref.e_ref, ...), custom_call_target="tpu_custom_call" | custom-call | flops 3000000000 | bytes 4000000 | tf_op jit(solution)/shard_map/attend/pallas_call | solution.py:166
  106.2 3.6 %collective-permute-start.1 = (bf16[64,2048]{1,0:T(8,128)(2,1)}, bf16[64,2048]{1,0:T(8,128)(2,1)S(1)}, u32[]{:S(2)}, u32[]{:S(2)}) collective-permute-start(bf16[64,2048]{1,0:T(8,128)(2,1)} %get-tuple-element.17._), channel_id=1, source_target_pairs={{0,2},{1,3},{2,0},{3,1},{4,6},{5,7},{6,4},{7,5},{8,10},{9,11},{10,... | collective-permute-start | bytes 786440 | tf_op jit(solution)/shard_map/ppermute | solution.py:22
  109.8 6.1 %attend.5 = (bf16[64,2048]{1,0:T(8,128)(2,1)}, f32[64,128]{1,0:T(8,128)}) custom-call(s32[3]{0:T(128)} %get-tuple-element.40.place_ref, f32[8]{0:T(128)} %lam_ref.7, bf16[4,64,256]{2,1,0:T(8,128)(2,1)} %q1_ref.7, bf16[4,64,256]{2,1,0:T(8,128)(2,1)} %q2_ref.7, bf16[18,264,256]{2,1,0:T(8,128)(2,1)} %multiply_convert_fusion.w_ref.e_ref, ...), custom_call_target="tpu_custom_call" | custom-call | flops 3000000000 | bytes 4000000 | tf_op jit(solution)/shard_map/attend/pallas_call | solution.py:166
  115.9 0.6 collective-permute-start
  116.6 0.6 add_add_fusion
  117.2 6.1 %attend.6 = (bf16[64,2048]{1,0:T(8,128)(2,1)}, f32[64,128]{1,0:T(8,128)}) custom-call(s32[3]{0:T(128)} %get-tuple-element.39.place_ref, f32[8]{0:T(128)} %lam_ref.7, bf16[4,64,256]{2,1,0:T(8,128)(2,1)} %q1_ref.7, bf16[4,64,256]{2,1,0:T(8,128)(2,1)} %q2_ref.7, bf16[18,264,256]{2,1,0:T(8,128)(2,1)} %multiply_convert_fusion.w_ref.e_ref, ...), custom_call_target="tpu_custom_call" | custom-call | flops 3000000000 | bytes 4000000 | tf_op jit(solution)/shard_map/attend/pallas_call | solution.py:166
  123.4 2.0 %collective-permute-start.2 = (bf16[64,2048]{1,0:T(8,128)(2,1)}, bf16[64,2048]{1,0:T(8,128)(2,1)S(1)}, u32[]{:S(2)}, u32[]{:S(2)}) collective-permute-start(bf16[64,2048]{1,0:T(8,128)(2,1)} %get-tuple-element.19._), channel_id=1, source_target_pairs={{0,3},{1,0},{2,1},{3,2},{4,7},{5,4},{6,5},{7,6},{8,11},{9,8},{10,9... | collective-permute-start | bytes 786440 | tf_op jit(solution)/shard_map/ppermute | solution.py:22
  125.3 6.3 %attend.7 = (bf16[64,2048]{1,0:T(8,128)(2,1)}, f32[64,128]{1,0:T(8,128)}) custom-call(s32[3]{0:T(128)} %get-tuple-element.38.place_ref, f32[8]{0:T(128)} %lam_ref.7, bf16[4,64,256]{2,1,0:T(8,128)(2,1)} %q1_ref.7, bf16[4,64,256]{2,1,0:T(8,128)(2,1)} %q2_ref.7, bf16[18,264,256]{2,1,0:T(8,128)(2,1)} %multiply_convert_fusion.w_ref.e_ref, ...), custom_call_target="tpu_custom_call" | custom-call | flops 3000000000 | bytes 4000000 | tf_op jit(solution)/shard_map/attend/pallas_call | solution.py:166
  131.6 0.0 collective-permute-done.2
  131.6 0.0 collective-permute-done
  131.6 0.0 collective-permute-done.1
  131.7 1.2 multiply_reduce_fusion
  132.9 0.1 multiply_convert_fusion.1.refs_0_
  133.1 0.0 copy-start
  133.1 0.1 collective-permute-start.3
  133.2 3.6 %collective-permute-start.4 = (bf16[64,2048]{1,0:T(8,128)(2,1)S(1)}, bf16[64,2048]{1,0:T(8,128)(2,1)S(1)}, u32[]{:S(2)}, u32[]{:S(2)}) collective-permute-start(bf16[64,2048]{1,0:T(8,128)(2,1)S(1)} %multiply_convert_fusion.1.refs_0_), channel_id=1, source_target_pairs={{0,2},{1,3},{2,0},{3,1},{4,6},{5,7},{6,4},{7,5},{8,10},{9,11},{10,... | collective-permute-start | bytes 786440 | tf_op jit(solution)/shard_map/ppermute | solution.py:22
  136.8 0.0 collective-permute-start.5
  136.8 6.4 %collective-permute-start.6 = (bf16[8,2048]{1,0:T(8,128)(2,1)S(1)}, bf16[8,2048]{1,0:T(8,128)(2,1)S(1)}, u32[]{:S(2)}, u32[]{:S(2)}) collective-permute-start(bf16[8,2048]{1,0:T(8,128)(2,1)S(1)} %slice.28), channel_id=1, source_target_pairs={{0,4},{4,8},{8,12},{12,16},{16,20},{20,24},{24,28},{28,32},{32,36}... | collective-permute-start | bytes 98312 | tf_op jit(solution)/shard_map/ppermute | solution.py:27
  143.2 1.3 collective-permute-done.6.refs_4_
  144.4 1.6 collective-permute-start.7
  146.0 0.0 collective-permute-start.8
  146.1 4.0 %collective-permute-done.7.refs_5_ = bf16[8,2048]{1,0:T(8,128)(2,1)S(1)} collective-permute-done((bf16[8,2048]{1,0:T(8,128)(2,1)S(1)}, bf16[8,2048]{1,0:T(8,128)(2,1)S(1)}, u32[]{:S(2)}, u32[]{:S(2)}) %collective-permute-start.7) | collective-permute-done | bytes 32800 | tf_op jit(solution)/shard_map/ppermute | solution.py:22
  150.0 0.0 collective-permute-start.9
  150.0 0.4 collective-permute-done.8.refs_6_
  150.5 2.3 %collective-permute-done.9.refs_7_ = bf16[8,2048]{1,0:T(8,128)(2,1)S(1)} collective-permute-done((bf16[8,2048]{1,0:T(8,128)(2,1)S(1)}, bf16[8,2048]{1,0:T(8,128)(2,1)S(1)}, u32[]{:S(2)}, u32[]{:S(2)}) %collective-permute-start.9) | collective-permute-done | bytes 32800 | tf_op jit(solution)/shard_map/ppermute | solution.py:22
  152.8 0.0 collective-permute-done.3.refs_1_
  152.8 0.0 collective-permute-done.4.refs_2_
  152.8 0.0 copy-start.2
  152.8 0.0 collective-permute-done.5.refs_3_
  152.8 0.0 all-gather.3.cloned.1.call-done.refs_14_
  152.9 0.5 copy-done.13
  153.4 0.1 copy-done.1
  153.5 0.1 copy-done.2
  153.6 0.1 copy-done.3
  153.7 11.3 %feed_forward.1 = (bf16[64,2048]{1,0:T(8,128)(2,1)}, bf16[64,2048]{1,0:T(8,128)(2,1)}, bf16[64,2048]{1,0:T(8,128)(2,1)}, bf16[64,2048]{1,0:T(8,128)(2,1)}) custom-call(bf16[64,2048]{1,0:T(8,128)(2,1)} %copy-done, bf16[64,2048]{1,0:T(8,128)(2,1)} %copy-done.1, bf16[64,2048]{1,0:T(8,128)(2,1)} %copy-done.2, bf16[64,2048]{1,0:T(8,128)(2,1)} %copy-done.3, ...), custom_call_target="tpu_custom_call" | custom-call | tf_op jit(solution)/shard_map/feed_forward/pallas_call | solution.py:277
  165.0 1.3 collective-permute-start.10
  166.3 0.3 collective-permute-start.11
  166.6 0.4 collective-permute-start.12
  167.1 6.3 %collective-permute-done.10 = bf16[64,2048]{1,0:T(8,128)(2,1)S(1)} collective-permute-done((bf16[64,2048]{1,0:T(8,128)(2,1)}, bf16[64,2048]{1,0:T(8,128)(2,1)S(1)}, u32[]{:S(2)}, u32[]{:S(2)}) %collective-permute-start.10) | collective-permute-done | bytes 262176 | tf_op jit(solution)/shard_map/ppermute | solution.py:22
  173.4 0.5 collective-permute-done.11
  173.9 8.0 %collective-permute-done.12 = bf16[64,2048]{1,0:T(8,128)(2,1)S(1)} collective-permute-done((bf16[64,2048]{1,0:T(8,128)(2,1)}, bf16[64,2048]{1,0:T(8,128)(2,1)S(1)}, u32[]{:S(2)}, u32[]{:S(2)}) %collective-permute-start.12) | collective-permute-done | bytes 262176 | tf_op jit(solution)/shard_map/ppermute | solution.py:22
  181.9 1.8 fusion.3
  (31 shorter events, 0.2 us)
Async XLA Ops:
  6.5 5.1 %copy-start.6 = (bf16[4,64,64]{2,1,0:T(8,128)(2,1)S(1)}, bf16[4,64,64]{2,1,0:T(8,128)(2,1)}, u32[]{:S(2)}) copy-start(bf16[4,64,64]{2,1,0:T(8,128)(2,1)} %param.18) | copy-start | bytes 98308
  6.5 5.1 %copy-start.5 = (bf16[4,64,64]{2,1,0:T(8,128)(2,1)S(1)}, bf16[4,64,64]{2,1,0:T(8,128)(2,1)}, u32[]{:S(2)}) copy-start(bf16[4,64,64]{2,1,0:T(8,128)(2,1)} %param.20) | copy-start | bytes 98308
  6.6 4.8 %copy-start.9 = (bf16[4,64,128]{2,1,0:T(8,128)(2,1)S(1)}, bf16[4,64,128]{2,1,0:T(8,128)(2,1)}, u32[]{:S(2)}) copy-start(bf16[4,64,128]{2,1,0:T(8,128)(2,1)} %param.21) | copy-start | bytes 196612
  6.6 146.3 %all-gather.3.cloned.1.call-start = ((), (), s32[]{:S(2)}) async-start(), calls=%async_computation | async-start | bytes 17842176 | tf_op jit(solution)/shard_map/all_gather | solution.py:321
  8.9 89.2 %copy-start.7 = (f32[64,128]{1,0:T(8,128)}, f32[64,128]{1,0:T(8,128)S(1)}, u32[]{:S(2)}) copy-start(f32[64,128]{1,0:T(8,128)S(1)} %copy.27.c_ref) | copy-start | bytes 98308
  9.0 89.1 %copy-start.8 = (f32[64,128]{1,0:T(8,128)}, f32[64,128]{1,0:T(8,128)S(1)}, u32[]{:S(2)}) copy-start(f32[64,128]{1,0:T(8,128)S(1)} %copy.28.s_ref) | copy-start | bytes 98308
  106.2 25.5 %collective-permute-start.1 = (bf16[64,2048]{1,0:T(8,128)(2,1)}, bf16[64,2048]{1,0:T(8,128)(2,1)S(1)}, u32[]{:S(2)}, u32[]{:S(2)}) collective-permute-start(bf16[64,2048]{1,0:T(8,128)(2,1)} %get-tuple-element.17._), channel_id=1, source_target_pairs={{0,2},{1,3},{2,0},{3,1},{4,6},{5,7},{6,4},{7,5},{8,10},{9,11},{10,... | collective-permute-start | bytes 786440 | tf_op jit(solution)/shard_map/ppermute | solution.py:22
  115.9 15.7 %collective-permute-start = (bf16[64,2048]{1,0:T(8,128)(2,1)}, bf16[64,2048]{1,0:T(8,128)(2,1)S(1)}, u32[]{:S(2)}, u32[]{:S(2)}) collective-permute-start(bf16[64,2048]{1,0:T(8,128)(2,1)} %get-tuple-element.18._), channel_id=1, source_target_pairs={{0,1},{1,2},{2,3},{3,0},{4,5},{5,6},{6,7},{7,4},{8,9},{9,10},{10,1... | collective-permute-start | bytes 786440 | tf_op jit(solution)/shard_map/ppermute | solution.py:22
  123.4 8.3 %collective-permute-start.2 = (bf16[64,2048]{1,0:T(8,128)(2,1)}, bf16[64,2048]{1,0:T(8,128)(2,1)S(1)}, u32[]{:S(2)}, u32[]{:S(2)}) collective-permute-start(bf16[64,2048]{1,0:T(8,128)(2,1)} %get-tuple-element.19._), channel_id=1, source_target_pairs={{0,3},{1,0},{2,1},{3,2},{4,7},{5,4},{6,5},{7,6},{8,11},{9,8},{10,9... | collective-permute-start | bytes 786440 | tf_op jit(solution)/shard_map/ppermute | solution.py:22
  125.3 6.3 %copy-start.4 = (bf16[1,64,2048]{2,1,0:T(8,128)(2,1)S(1)}, bf16[1,64,2048]{2,1,0:T(8,128)(2,1)}, u32[]{:S(2)}) copy-start(bf16[1,64,2048]{2,1,0:T(8,128)(2,1)} %param.16) | copy-start | bytes 786436
  125.3 7.6 %copy-start.14 = (f32[2048]{0:T(1024)S(1)}, f32[2048]{0:T(1024)}, u32[]{:S(2)}) copy-start(f32[2048]{0:T(1024)} %param.26) | copy-start | bytes 24580
  133.1 19.8 %copy-start = (bf16[64,2048]{1,0:T(8,128)(2,1)}, bf16[64,2048]{1,0:T(8,128)(2,1)S(1)}, u32[]{:S(2)}) copy-start(bf16[64,2048]{1,0:T(8,128)(2,1)S(1)} %multiply_convert_fusion.1.refs_0_) | copy-start | bytes 786436
  133.1 19.7 %collective-permute-start.3 = (bf16[64,2048]{1,0:T(8,128)(2,1)S(1)}, bf16[64,2048]{1,0:T(8,128)(2,1)S(1)}, u32[]{:S(2)}, u32[]{:S(2)}) collective-permute-start(bf16[64,2048]{1,0:T(8,128)(2,1)S(1)} %multiply_convert_fusion.1.refs_0_), channel_id=1, source_target_pairs={{0,1},{1,2},{2,3},{3,0},{4,5},{5,6},{6,7},{7,4},{8,9},{9,10},{10,1... | collective-permute-start | bytes 786440 | tf_op jit(solution)/shard_map/ppermute | solution.py:22
  133.2 19.6 %collective-permute-start.4 = (bf16[64,2048]{1,0:T(8,128)(2,1)S(1)}, bf16[64,2048]{1,0:T(8,128)(2,1)S(1)}, u32[]{:S(2)}, u32[]{:S(2)}) collective-permute-start(bf16[64,2048]{1,0:T(8,128)(2,1)S(1)} %multiply_convert_fusion.1.refs_0_), channel_id=1, source_target_pairs={{0,2},{1,3},{2,0},{3,1},{4,6},{5,7},{6,4},{7,5},{8,10},{9,11},{10,... | collective-permute-start | bytes 786440 | tf_op jit(solution)/shard_map/ppermute | solution.py:22
  136.8 16.0 %collective-permute-start.5 = (bf16[64,2048]{1,0:T(8,128)(2,1)S(1)}, bf16[64,2048]{1,0:T(8,128)(2,1)S(1)}, u32[]{:S(2)}, u32[]{:S(2)}) collective-permute-start(bf16[64,2048]{1,0:T(8,128)(2,1)S(1)} %multiply_convert_fusion.1.refs_0_), channel_id=1, source_target_pairs={{0,3},{1,0},{2,1},{3,2},{4,7},{5,4},{6,5},{7,6},{8,11},{9,8},{10,9... | collective-permute-start | bytes 786440 | tf_op jit(solution)/shard_map/ppermute | solution.py:22
  136.8 7.7 %collective-permute-start.6 = (bf16[8,2048]{1,0:T(8,128)(2,1)S(1)}, bf16[8,2048]{1,0:T(8,128)(2,1)S(1)}, u32[]{:S(2)}, u32[]{:S(2)}) collective-permute-start(bf16[8,2048]{1,0:T(8,128)(2,1)S(1)} %slice.28), channel_id=1, source_target_pairs={{0,4},{4,8},{8,12},{12,16},{16,20},{20,24},{24,28},{28,32},{32,36}... | collective-permute-start | bytes 98312 | tf_op jit(solution)/shard_map/ppermute | solution.py:27
  144.4 8.4 %copy-start.10 = (bf16[8,2048]{1,0:T(8,128)(2,1)}, bf16[8,2048]{1,0:T(8,128)(2,1)S(1)}, u32[]{:S(2)}) copy-start(bf16[8,2048]{1,0:T(8,128)(2,1)S(1)} %collective-permute-done.6.refs_4_) | copy-start | bytes 98308
  144.4 5.6 %collective-permute-start.7 = (bf16[8,2048]{1,0:T(8,128)(2,1)S(1)}, bf16[8,2048]{1,0:T(8,128)(2,1)S(1)}, u32[]{:S(2)}, u32[]{:S(2)}) collective-permute-start(bf16[8,2048]{1,0:T(8,128)(2,1)S(1)} %collective-permute-done.6.refs_4_), channel_id=1, source_target_pairs={{0,1},{1,2},{2,3},{3,0},{4,5},{5,6},{6,7},{7,4},{8,9},{9,10},{10,1... | collective-permute-start | bytes 98312 | tf_op jit(solution)/shard_map/ppermute | solution.py:22
  146.0 4.4 %collective-permute-start.8 = (bf16[8,2048]{1,0:T(8,128)(2,1)S(1)}, bf16[8,2048]{1,0:T(8,128)(2,1)S(1)}, u32[]{:S(2)}, u32[]{:S(2)}) collective-permute-start(bf16[8,2048]{1,0:T(8,128)(2,1)S(1)} %collective-permute-done.6.refs_4_), channel_id=1, source_target_pairs={{0,2},{1,3},{2,0},{3,1},{4,6},{5,7},{6,4},{7,5},{8,10},{9,11},{10,... | collective-permute-start | bytes 98312 | tf_op jit(solution)/shard_map/ppermute | solution.py:22
  150.0 2.9 %copy-start.11 = (bf16[8,2048]{1,0:T(8,128)(2,1)}, bf16[8,2048]{1,0:T(8,128)(2,1)S(1)}, u32[]{:S(2)}) copy-start(bf16[8,2048]{1,0:T(8,128)(2,1)S(1)} %collective-permute-done.7.refs_5_) | copy-start | bytes 98308
  150.0 2.8 %collective-permute-start.9 = (bf16[8,2048]{1,0:T(8,128)(2,1)S(1)}, bf16[8,2048]{1,0:T(8,128)(2,1)S(1)}, u32[]{:S(2)}, u32[]{:S(2)}) collective-permute-start(bf16[8,2048]{1,0:T(8,128)(2,1)S(1)} %collective-permute-done.6.refs_4_), channel_id=1, source_target_pairs={{0,3},{1,0},{2,1},{3,2},{4,7},{5,4},{6,5},{7,6},{8,11},{9,8},{10,9... | collective-permute-start | bytes 98312 | tf_op jit(solution)/shard_map/ppermute | solution.py:22
  150.5 2.4 %copy-start.12 = (bf16[8,2048]{1,0:T(8,128)(2,1)}, bf16[8,2048]{1,0:T(8,128)(2,1)S(1)}, u32[]{:S(2)}) copy-start(bf16[8,2048]{1,0:T(8,128)(2,1)S(1)} %collective-permute-done.8.refs_6_) | copy-start | bytes 98308
  152.8 0.6 copy-start.13
  152.8 0.7 copy-start.1
  152.8 0.8 copy-start.2
  152.8 0.9 copy-start.3
  165.0 8.4 %collective-permute-start.10 = (bf16[64,2048]{1,0:T(8,128)(2,1)}, bf16[64,2048]{1,0:T(8,128)(2,1)S(1)}, u32[]{:S(2)}, u32[]{:S(2)}) collective-permute-start(bf16[64,2048]{1,0:T(8,128)(2,1)} %get-tuple-element.26), channel_id=1, source_target_pairs={{0,3},{1,0},{2,1},{3,2},{4,7},{5,4},{6,5},{7,6},{8,11},{9,8},{10,9... | collective-permute-start | bytes 786440 | tf_op jit(solution)/shard_map/ppermute | solution.py:22
  166.3 7.6 %collective-permute-start.11 = (bf16[64,2048]{1,0:T(8,128)(2,1)}, bf16[64,2048]{1,0:T(8,128)(2,1)S(1)}, u32[]{:S(2)}, u32[]{:S(2)}) collective-permute-start(bf16[64,2048]{1,0:T(8,128)(2,1)} %get-tuple-element.27), channel_id=1, source_target_pairs={{0,2},{1,3},{2,0},{3,1},{4,6},{5,7},{6,4},{7,5},{8,10},{9,11},{10,... | collective-permute-start | bytes 786440 | tf_op jit(solution)/shard_map/ppermute | solution.py:22
  166.6 15.3 %collective-permute-start.12 = (bf16[64,2048]{1,0:T(8,128)(2,1)}, bf16[64,2048]{1,0:T(8,128)(2,1)S(1)}, u32[]{:S(2)}, u32[]{:S(2)}) collective-permute-start(bf16[64,2048]{1,0:T(8,128)(2,1)} %get-tuple-element.28), channel_id=1, source_target_pairs={{0,1},{1,2},{2,3},{3,0},{4,5},{5,6},{6,7},{7,4},{8,9},{9,10},{10,1... | collective-permute-start | bytes 786440 | tf_op jit(solution)/shard_map/ppermute | solution.py:22
Sparse Core Ops, SparseCore 0:
  9.2 142.3 all-gather.2

commit v3 on v2

--- a/solution.py
+++ b/solution.py
@@ -15,6 +15,7 @@
 VAL_UP = 8192.0
 LANES = 128
 EDGE = 8
+AHEAD = 3
 
 
 def shifted(array, axis, by):
@@ -54,7 +55,7 @@
     model = out_weight.shape[1]
 
     def body(
-        place_ref, lam_ref, q1_ref, q2_ref, w_ref, e_ref, c_ref, s_ref, d_ref, g_ref, p_ref, _,
+        place_ref, lam_ref, q1_ref, q2_ref, w_ref, c_ref, s_ref, d_ref, g_ref, p_ref, _,
         o_ref, m_ref, h_ref,
     ):
         s = place_ref[0]
@@ -65,15 +66,16 @@
         cos = c_ref[...]
         sin = s_ref[...]
         gain_row = jnp.concatenate([g_ref[...], g_ref[...]], axis=1)
-        k_all = w_ref[:, :, 0:LANES].reshape(keys, LANES)
-        v_all = w_ref[:, :, LANES : 2 * LANES].reshape(keys, LANES)
+        these = pl.ds(pl.multiple_of(s * rows, rows), rows)
+        k_all = w_ref[:, these, 0:LANES].reshape(keys, LANES)
+        v_all = w_ref[:, these, LANES : 2 * LANES].reshape(keys, LANES)
         v_ext = jnp.concatenate([v_all, jnp.ones((keys, LANES), jnp.bfloat16)], axis=1)
 
         placed = []
         for ref in (q1_ref, q2_ref):
             tiles = []
             for h in range(kv_heads):
-                x = ref[0, :, h * LANES : (h + 1) * LANES].astype(jnp.float32)
+                x = ref[s, :, h * LANES : (h + 1) * LANES].astype(jnp.float32)
                 swap = jnp.where(low, pltpu.roll(x, LANES - half, 1), pltpu.roll(x, half, 1))
                 tiles.append((x * cos + swap * sin).astype(jnp.bfloat16).astype(jnp.float32))
             placed.append(tiles)
@@ -100,7 +102,7 @@
         for i in range(ranks // 2):
             two = [
                 jnp.sum(
-                    jnp.where(this_row, e_ref[2 * i + b, :, 0:LANES].astype(jnp.float32), 0.0),
+                    jnp.where(this_row, w_ref[2 * i + b, seqs * rows : per_rank, 0:LANES].astype(jnp.float32), 0.0),
                     axis=0,
                     keepdims=True,
                 )
@@ -161,36 +163,23 @@
             h_ref[...], p_ref[...], preferred_element_type=jnp.float32
         ).astype(jnp.bfloat16)
 
-    whole = lambda *shape: pl.BlockSpec(shape, lambda i, p: (0,) * len(shape))
     smem = pl.BlockSpec(memory_space=pltpu.SMEM)
+    vmem = pl.BlockSpec(memory_space=pltpu.VMEM)
     return pl.pallas_call(
         body,
         out_shape=(
             jax.ShapeDtypeStruct((rows, model), jnp.bfloat16),
             jax.ShapeDtypeStruct((rows, LANES), jnp.float32),
         ),
-        grid_spec=pltpu.PrefetchScalarGridSpec(
-            num_scalar_prefetch=1,
-            grid=(1,),
-            in_specs=[
-                smem,
-                pl.BlockSpec((1, rows, q_lanes), lambda i, p: (p[0], 0, 0)),
-                pl.BlockSpec((1, rows, q_lanes), lambda i, p: (p[0], 0, 0)),
-                pl.BlockSpec((ranks, rows, 2 * LANES), lambda i, p: (0, p[0], 0)),
-                pl.BlockSpec((ranks, EDGE, 2 * LANES), lambda i, p: (0, seqs * rows // EDGE, 0)),
-                whole(rows, LANES),
-                whole(rows, LANES),
-                whole(seqs, rows),
-                whole(1, head_width),
-                whole(*out_weight.shape),
-                pl.BlockSpec(memory_space=pl.ANY),
-            ],
-            out_specs=(whole(rows, model), whole(rows, LANES)),
-            scratch_shapes=[pltpu.VMEM((rows, heads * head_width), jnp.bfloat16)],
+        in_specs=[smem, smem] + [vmem] * 8 + [pl.BlockSpec(memory_space=pl.ANY)],
+        out_specs=(vmem, vmem),
+        scratch_shapes=[pltpu.VMEM((rows, heads * head_width), jnp.bfloat16)],
+        compiler_params=pltpu.CompilerParams(vmem_limit_bytes=24 * 1024 * 1024),
+        cost_estimate=pl.CostEstimate(
+            flops=3_000_000_000, transcendentals=0, bytes_accessed=4_000_000
         ),
-        cost_estimate=pl.CostEstimate(flops=3_000_000_000, transcendentals=0, bytes_accessed=4_000_000),
         name="attend",
-    )(place, lam, q_one, q_two, window, window, cosine, sine, docs, gain, out_weight, after)
+    )(place, lam, q_one, q_two, window, cosine, sine, docs, gain, out_weight, after)
 
 
 def feed_forward(blocks, edges, same, weights, conv_gate, conv_value):
@@ -209,20 +198,30 @@
         outs = refs[3 * count + 3 : 4 * count + 3]
         x_ref, w_ref, h_ref, b_ref, sems = refs[4 * count + 3 :]
 
-        def piece(base, a, b, at):
-            return pltpu.make_async_copy(
-                w_hbm.at[:, base + a : base + b], w_ref.at[:, base + a : base + b], sems.at[at]
+        def piece(at, low, high, base, a, b):
+            spot = (slice(low, high), slice(base + a, base + b))
+            return pltpu.make_async_copy(w_hbm.at[spot], w_ref.at[spot], sems.at[at])
+
+        queue = []
+        for j, (a, b) in enumerate(cuts):
+            queue.append([piece(2 * j + n, 0, width, n * hidden, a, b) for n in range(2)])
+        for j in range(0, width, out_step):
+            queue.append(
+                [piece(2 * len(cuts) + j // out_step, j, j + out_step, 2 * hidden, 0, hidden)]
             )
 
-        ups = [
-            [piece(base, a, b, 2 * j + n) for n, base in enumerate((0, hidden))]
-            for j, (a, b) in enumerate(cuts)
-        ]
-        down = piece(2 * hidden, 0, hidden, 2 * len(cuts))
-        for both in ups:
-            for copy in both:
-                copy.start()
-        down.start()
+        def launch(at):
+            if at < len(queue):
+                for copy in queue[at]:
+                    copy.start()
+
+        def arrive(at):
+            for copy in queue[at]:
+                copy.wait()
+            launch(at + AHEAD)
+
+        for at in range(AHEAD):
+            launch(at)
         for k in range(count):
             x_ref[k * span : k * span + EDGE, :] = e_in[k][...]
             x_ref[k * span + EDGE : (k + 1) * span, :] = x_in[k][...]
@@ -233,8 +232,7 @@
 
         def raised(j):
             a, b = cuts[j]
-            for copy in ups[j]:
-                copy.wait()
+            arrive(j)
             return [
                 jnp.dot(
                     x_ref[...], w_ref[:, base + a : base + b], preferred_element_type=jnp.float32
@@ -262,8 +260,8 @@
                 h_ref[k * rows : (k + 1) * rows, a:b] = act[
                     k * span + EDGE : (k + 1) * span
                 ].astype(jnp.bfloat16)
-        down.wait()
         for a in range(0, width, out_step):
+            arrive(len(cuts) + a // out_step)
             part = lax.dot_general(
                 h_ref[...],
                 w_ref[a : a + out_step, 2 * hidden : 3 * hidden],
@@ -284,9 +282,9 @@
             pltpu.VMEM((width, 3 * hidden), jnp.bfloat16),
             pltpu.VMEM((count * rows, hidden), jnp.bfloat16),
             pltpu.VMEM((total, LANES), jnp.float32),
-            pltpu.SemaphoreType.DMA((2 * len(cuts) + 1,)),
+            pltpu.SemaphoreType.DMA((2 * len(cuts) + width // out_step,)),
         ],
-        compiler_params=pltpu.CompilerParams(vmem_limit_bytes=56 * 1024 * 1024),
+        compiler_params=pltpu.CompilerParams(vmem_limit_bytes=48 * 1024 * 1024),
         name="feed_forward",
     )(*blocks, *edges, *same, conv_gate, conv_value, weights)
 

time: 191 us -> 187 us (0.979)
  Pallas kernels: 36 us -> 23 us
  waiting for transfers between devices: 22.9 us -> 30.1 us
  starting transfers between devices: 20 us -> 23.6 us
  other arithmetic: 10.4 us -> 7.09 us
  local copies, waits for them, and re-layouts: 1.31 us -> 3.25 us
    pallas_call x4, Pallas kernels: 24.7 us -> 13.3 us  [attend(): pl.pallas_call(body, out_shape=(jax.ShapeDtypeStruct((rows, model), jnp.b...]
    all_gather x1, waiting for transfers between devices: 0.02 us -> 5.65 us  [per_device(): weights = lax.all_gather(packed, 'sp', axis=0, tiled=True)]
    ppermute x12, starting transfers between devices: 13.6 us -> 17.3 us  [shifted(): lax.ppermute(array, axis, [(i, (i + by) % length) for i in range(length)])]
    unnamed x30 -> x28, local copies, waits for them, and re-layouts: 0.88 us -> 2.8 us
  transfers between devices with their start and end apart: 14 -> 14, of which waited for: 7 -> 8; matrix products, arithmetic and copies ran while one was open for 4% -> 3% of each run, Pallas kernels for 13% -> 7%
where the time goes in v3:
time: 187 us
  blocking collectives  86.1 us (46%)
  waiting for transfers between devices  30.1 us (16%)
  starting transfers between devices  23.6 us (13%)
  Pallas kernels  23 us (12%)
  between operations  13.7 us (7%)
  other arithmetic  7.09 us (4%)
  local copies, waits for them, and re-layouts  3.25 us (2%)
    all_gather x1, blocking collectives, per_device(): everyone = lax.all_gather(sent, 'sp', axis=0, tiled=False)  86.1 us
    ppermute x12, waiting for transfers between devices, shifted(): lax.ppermute(array, axis, [(i, (i + by) % length) for i in range(length)])  23.3 us
    ppermute x12, starting transfers between devices, shifted(): lax.ppermute(array, axis, [(i, (i + by) % length) for i in range(length)])  17.3 us
    pallas_call x4, Pallas kernels, attend(): pl.pallas_call(body, out_shape=(jax.ShapeDtypeStruct((rows, model), jnp.b...  13.3 us
    pallas_call x1, Pallas kernels, feed_forward(): pl.pallas_call(body, out_shape=[jax.ShapeDtypeStruct((rows, width), jnp.b...  9.67 us
    ppermute x1, starting transfers between devices, from_behind(): return lax.ppermute(array, axis, [(i, i + 1) for i in range(length - 1)])  6.32 us
    all_gather x1, waiting for transfers between devices, per_device(): weights = lax.all_gather(packed, 'sp', axis=0, tiled=True)  5.65 us
  transfers between devices with their start and end apart: 14, of which 8 were waited for; matrix products, arithmetic and copies ran while one was open for 3% of the time, Pallas kernels for 7%

profile of v3, /device:TPU:33, one launch (start us, length us, event | category | flops | bytes accessed | tf_op | source)
XLA Modules:
  0.0 186.8 jit_solution(3038267487745437411)
XLA Ops:
  6.6 0.0 all-gather.3.cloned.1.call-start
  6.6 2.0 %pad_maximum_fusion = bf16[64,4224]{1,0:T(8,128)(2,1)} fusion(bf16[64,1408]{1,0:T(8,128)(2,1)} %bitcast.26, bf16[64,1408]{1,0:T(8,128)(2,1)} %param.28, bf16[64,1408]{1,0:T(8,128)(2,1)} %param.27), kind=kLoop, calls=%fused_computation.1 | loop fusion | flops 1622016 | bytes 1081344 | tf_op jit(solution)/shard_map/concatenate | solution.py:318
  8.5 0.1 all-gather.3.cloned.1.call-update
  8.7 0.1 multiply_cosine_fusion
  8.8 0.1 copy.27.c_ref
  8.9 0.1 copy.28.s_ref
  9.0 0.7 multiply_convert_fusion.4
  9.7 0.1 tile.33
  9.8 0.1 add_add_fusion.2
  9.9 1.0 maximum_convert_fusion
  10.8 0.0 copy-done.12
  10.9 0.1 fusion.10
  11.0 0.1 fusion.11
  11.1 0.0 copy-done.11
  11.1 0.0 copy-done.10
  11.1 0.2 multiply_convert_fusion.3
  11.4 86.1 %all-gather.4 = f16[32,264,256]{2,1,0:T(8,128)(2,1)S(1)} all-gather(f16[1,264,256]{2,1,0:T(8,128)(2,1)S(1)} %pad_maximum_fusion.1), channel_id=1, replica_groups=mesh['grp'=2,'sp'=32,'tp'=4] {'sp'}, dimensions={0}, use_global_device_ids=true | all-gather | bytes 4460544 | tf_op jit(solution)/shard_map/all_gather | solution.py:333
  97.5 0.0 copy-start.7
  97.5 0.0 copy-start.8
  97.5 0.5 multiply_convert_fusion.w_ref
  98.1 0.1 copy-done.2
  98.2 1.0 copy-done.3
  99.1 0.0 copy-done.5
  99.1 0.0 copy-done.7
  99.1 3.3 %attend.4 = (bf16[64,2048]{1,0:T(8,128)(2,1)S(1)}, f32[64,128]{1,0:T(8,128)S(1)}) custom-call(s32[3]{0:T(128)S(1)} %get-tuple-element.41.place_ref, f32[8]{0:T(128)S(1)} %copy-done.7, bf16[4,64,256]{2,1,0:T(8,128)(2,1)S(1)} %copy-done.5, bf16[4,64,256]{2,1,0:T(8,128)(2,1)S(1)} %copy-done.6, bf16[18,264,256]{2,1,0:T(8,128)(2,1)S(1)} %multiply_convert_fusion.w_ref, ...), custom_call_target="tpu_custom_call" | custom-call | flops 3000000000 | bytes 4000000 | tf_op jit(solution)/shard_map/attend/pallas_call | solution.py:168
  102.5 3.7 %collective-permute-start.1 = (bf16[64,2048]{1,0:T(8,128)(2,1)S(1)}, bf16[64,2048]{1,0:T(8,128)(2,1)}, u32[]{:S(2)}, u32[]{:S(2)}) collective-permute-start(bf16[64,2048]{1,0:T(8,128)(2,1)S(1)} %get-tuple-element.17._), channel_id=1, source_target_pairs={{0,2},{1,3},{2,0},{3,1},{4,6},{5,7},{6,4},{7,5},{8,10},{9,11},{10,... | collective-permute-start | bytes 786440 | tf_op jit(solution)/shard_map/ppermute | solution.py:23
  106.2 3.3 %attend.5 = (bf16[64,2048]{1,0:T(8,128)(2,1)S(1)}, f32[64,128]{1,0:T(8,128)S(1)}) custom-call(s32[3]{0:T(128)S(1)} %get-tuple-element.40.place_ref, f32[8]{0:T(128)S(1)} %copy-done.7, bf16[4,64,256]{2,1,0:T(8,128)(2,1)S(1)} %copy-done.5, bf16[4,64,256]{2,1,0:T(8,128)(2,1)S(1)} %copy-done.6, bf16[18,264,256]{2,1,0:T(8,128)(2,1)S(1)} %multiply_convert_fusion.w_ref, ...), custom_call_target="tpu_custom_call" | custom-call | flops 3000000000 | bytes 4000000 | tf_op jit(solution)/shard_map/attend/pallas_call | solution.py:168
  109.5 0.7 collective-permute-start
  110.2 0.1 add_add_fusion
  110.3 1.7 copy-done.4
  111.9 3.3 %attend.6 = (bf16[64,2048]{1,0:T(8,128)(2,1)S(1)}, f32[64,128]{1,0:T(8,128)S(1)}) custom-call(s32[3]{0:T(128)S(1)} %get-tuple-element.39.place_ref, f32[8]{0:T(128)S(1)} %copy-done.7, bf16[4,64,256]{2,1,0:T(8,128)(2,1)S(1)} %copy-done.5, bf16[4,64,256]{2,1,0:T(8,128)(2,1)S(1)} %copy-done.6, bf16[18,264,256]{2,1,0:T(8,128)(2,1)S(1)} %multiply_convert_fusion.w_ref, ...), custom_call_target="tpu_custom_call" | custom-call | flops 3000000000 | bytes 4000000 | tf_op jit(solution)/shard_map/attend/pallas_call | solution.py:168
  115.3 2.3 %collective-permute-start.2 = (bf16[64,2048]{1,0:T(8,128)(2,1)S(1)}, bf16[64,2048]{1,0:T(8,128)(2,1)S(1)}, u32[]{:S(2)}, u32[]{:S(2)}) collective-permute-start(bf16[64,2048]{1,0:T(8,128)(2,1)S(1)} %get-tuple-element.19._), channel_id=1, source_target_pairs={{0,3},{1,0},{2,1},{3,2},{4,7},{5,4},{6,5},{7,6},{8,11},{9,8},{10,9... | collective-permute-start | bytes 786440 | tf_op jit(solution)/shard_map/ppermute | solution.py:23
  117.6 3.3 %attend.7 = (bf16[64,2048]{1,0:T(8,128)(2,1)S(1)}, f32[64,128]{1,0:T(8,128)S(1)}) custom-call(s32[3]{0:T(128)S(1)} %get-tuple-element.38.place_ref, f32[8]{0:T(128)S(1)} %copy-done.7, bf16[4,64,256]{2,1,0:T(8,128)(2,1)S(1)} %copy-done.5, bf16[4,64,256]{2,1,0:T(8,128)(2,1)S(1)} %copy-done.6, bf16[18,264,256]{2,1,0:T(8,128)(2,1)S(1)} %multiply_convert_fusion.w_ref, ...), custom_call_target="tpu_custom_call" | custom-call | flops 3000000000 | bytes 4000000 | tf_op jit(solution)/shard_map/attend/pallas_call | solution.py:168
  120.9 0.0 copy-start
  120.9 0.0 copy-start.1
  120.9 1.9 %collective-permute-done.2 = bf16[64,2048]{1,0:T(8,128)(2,1)S(1)} collective-permute-done((bf16[64,2048]{1,0:T(8,128)(2,1)S(1)}, bf16[64,2048]{1,0:T(8,128)(2,1)S(1)}, u32[]{:S(2)}, u32[]{:S(2)}) %collective-permute-start.2) | collective-permute-done | bytes 262176 | tf_op jit(solution)/shard_map/ppermute | solution.py:23
  122.9 0.0 collective-permute-done
  122.9 0.0 collective-permute-done.1
  122.9 1.3 multiply_reduce_fusion
  124.2 0.0 copy-done.13
  124.2 0.1 multiply_convert_fusion.1.refs_0_
  124.3 0.4 collective-permute-start.3
  124.7 4.2 %collective-permute-start.4 = (bf16[64,2048]{1,0:T(8,128)(2,1)S(1)}, bf16[64,2048]{1,0:T(8,128)(2,1)S(1)}, u32[]{:S(2)}, u32[]{:S(2)}) collective-permute-start(bf16[64,2048]{1,0:T(8,128)(2,1)S(1)} %multiply_convert_fusion.1.refs_0_), channel_id=1, source_target_pairs={{0,2},{1,3},{2,0},{3,1},{4,6},{5,7},{6,4},{7,5},{8,10},{9,11},{10,... | collective-permute-start | bytes 786440 | tf_op jit(solution)/shard_map/ppermute | solution.py:23
  128.9 0.0 collective-permute-start.5
  128.9 6.3 %collective-permute-start.6 = (bf16[8,2048]{1,0:T(8,128)(2,1)S(1)}, bf16[8,2048]{1,0:T(8,128)(2,1)S(1)}, u32[]{:S(2)}, u32[]{:S(2)}) collective-permute-start(bf16[8,2048]{1,0:T(8,128)(2,1)S(1)} %slice.28), channel_id=1, source_target_pairs={{0,4},{4,8},{8,12},{12,16},{16,20},{20,24},{24,28},{28,32},{32,36}... | collective-permute-start | bytes 98312 | tf_op jit(solution)/shard_map/ppermute | solution.py:28
  135.2 1.1 collective-permute-done.6.refs_4_
  136.4 2.0 %collective-permute-start.7 = (bf16[8,2048]{1,0:T(8,128)(2,1)S(1)}, bf16[8,2048]{1,0:T(8,128)(2,1)S(1)}, u32[]{:S(2)}, u32[]{:S(2)}) collective-permute-start(bf16[8,2048]{1,0:T(8,128)(2,1)S(1)} %collective-permute-done.6.refs_4_), channel_id=1, source_target_pairs={{0,1},{1,2},{2,3},{3,0},{4,5},{5,6},{6,7},{7,4},{8,9},{9,10},{10,1... | collective-permute-start | bytes 98312 | tf_op jit(solution)/shard_map/ppermute | solution.py:23
  138.3 0.0 collective-permute-start.8
  138.3 3.9 %collective-permute-done.7.refs_5_ = bf16[8,2048]{1,0:T(8,128)(2,1)S(1)} collective-permute-done((bf16[8,2048]{1,0:T(8,128)(2,1)S(1)}, bf16[8,2048]{1,0:T(8,128)(2,1)S(1)}, u32[]{:S(2)}, u32[]{:S(2)}) %collective-permute-start.7) | collective-permute-done | bytes 32800 | tf_op jit(solution)/shard_map/ppermute | solution.py:23
  142.2 0.0 collective-permute-start.9
  142.2 0.4 collective-permute-done.8.refs_6_
  142.7 2.7 %collective-permute-done.9.refs_7_ = bf16[8,2048]{1,0:T(8,128)(2,1)S(1)} collective-permute-done((bf16[8,2048]{1,0:T(8,128)(2,1)S(1)}, bf16[8,2048]{1,0:T(8,128)(2,1)S(1)}, u32[]{:S(2)}, u32[]{:S(2)}) %collective-permute-start.9) | collective-permute-done | bytes 32800 | tf_op jit(solution)/shard_map/ppermute | solution.py:23
  145.4 0.0 collective-permute-done.3.refs_1_
  145.4 0.0 collective-permute-done.4.refs_2_
  145.4 0.0 collective-permute-done.5.refs_3_
  145.4 5.7 %all-gather.3.cloned.1.call-done.refs_14_ = bf16[2048,4224]{1,0:T(8,128)(2,1)} async-done(((bf16[64,4224]{1,0:T(8,128)(2,1)}), bf16[2048,4224]{1,0:T(8,128)(2,1)}) %all-gather.3.cloned.1.call-update) | async-done | bytes 17301520 | tf_op jit(solution)/shard_map/all_gather | solution.py:319
  151.1 9.7 %feed_forward.1 = (bf16[64,2048]{1,0:T(8,128)(2,1)S(1)}, bf16[64,2048]{1,0:T(8,128)(2,1)S(1)}, bf16[64,2048]{1,0:T(8,128)(2,1)S(1)}, bf16[64,2048]{1,0:T(8,128)(2,1)S(1)}) custom-call(bf16[64,2048]{1,0:T(8,128)(2,1)S(1)} %multiply_convert_fusion.1.refs_0_, bf16[64,2048]{1,0:T(8,128)(2,1)S(1)} %collective-permute-done.3.refs_1_, ...), custom_call_target="tpu_custom_call" | custom-call | tf_op jit(solution)/shard_map/feed_forward/pallas_call | solution.py:275
  160.8 3.0 %collective-permute-start.10 = (bf16[64,2048]{1,0:T(8,128)(2,1)S(1)}, bf16[64,2048]{1,0:T(8,128)(2,1)S(1)}, u32[]{:S(2)}, u32[]{:S(2)}) collective-permute-start(bf16[64,2048]{1,0:T(8,128)(2,1)S(1)} %get-tuple-element.26), channel_id=1, source_target_pairs={{0,3},{1,0},{2,1},{3,2},{4,7},{5,4},{6,5},{7,6},{8,11},{9,8},{10,9... | collective-permute-start | bytes 786440 | tf_op jit(solution)/shard_map/ppermute | solution.py:23
  163.8 0.3 collective-permute-start.11
  164.0 0.7 collective-permute-start.12
  164.8 9.9 %collective-permute-done.10 = bf16[64,2048]{1,0:T(8,128)(2,1)S(1)} collective-permute-done((bf16[64,2048]{1,0:T(8,128)(2,1)S(1)}, bf16[64,2048]{1,0:T(8,128)(2,1)S(1)}, u32[]{:S(2)}, u32[]{:S(2)}) %collective-permute-start.10) | collective-permute-done | bytes 262176 | tf_op jit(solution)/shard_map/ppermute | solution.py:23
  174.6 0.0 collective-permute-done.11
  174.6 4.5 %collective-permute-done.12 = bf16[64,2048]{1,0:T(8,128)(2,1)S(1)} collective-permute-done((bf16[64,2048]{1,0:T(8,128)(2,1)S(1)}, bf16[64,2048]{1,0:T(8,128)(2,1)S(1)}, u32[]{:S(2)}, u32[]{:S(2)}) %collective-permute-start.12) | collective-permute-done | bytes 262176 | tf_op jit(solution)/shard_map/ppermute | solution.py:23
  179.1 0.9 fusion.3
  (29 shorter events, 0.2 us)
Async XLA Ops:
  6.5 4.5 %copy-start.11 = (bf16[4,64,64]{2,1,0:T(8,128)(2,1)S(1)}, bf16[4,64,64]{2,1,0:T(8,128)(2,1)}, u32[]{:S(2)}) copy-start(bf16[4,64,64]{2,1,0:T(8,128)(2,1)} %param.18) | copy-start | bytes 98308
  6.5 4.6 %copy-start.10 = (bf16[4,64,64]{2,1,0:T(8,128)(2,1)S(1)}, bf16[4,64,64]{2,1,0:T(8,128)(2,1)}, u32[]{:S(2)}) copy-start(bf16[4,64,64]{2,1,0:T(8,128)(2,1)} %param.20) | copy-start | bytes 98308
  6.6 4.3 %copy-start.12 = (bf16[4,64,128]{2,1,0:T(8,128)(2,1)S(1)}, bf16[4,64,128]{2,1,0:T(8,128)(2,1)}, u32[]{:S(2)}) copy-start(bf16[4,64,128]{2,1,0:T(8,128)(2,1)} %param.21) | copy-start | bytes 196612
  6.6 144.5 %all-gather.3.cloned.1.call-start = ((), (), s32[]{:S(2)}) async-start(), calls=%async_computation | async-start | bytes 17842176 | tf_op jit(solution)/shard_map/all_gather | solution.py:319
  97.5 0.7 copy-start.2
  97.5 1.6 copy-start.3
  97.5 1.6 copy-start.5
  97.5 1.6 copy-start.6
  97.5 1.6 copy-start.7
  97.5 1.6 copy-start.8
  102.5 20.4 %collective-permute-start.1 = (bf16[64,2048]{1,0:T(8,128)(2,1)S(1)}, bf16[64,2048]{1,0:T(8,128)(2,1)}, u32[]{:S(2)}, u32[]{:S(2)}) collective-permute-start(bf16[64,2048]{1,0:T(8,128)(2,1)S(1)} %get-tuple-element.17._), channel_id=1, source_target_pairs={{0,2},{1,3},{2,0},{3,1},{4,6},{5,7},{6,4},{7,5},{8,10},{9,11},{10,... | collective-permute-start | bytes 786440 | tf_op jit(solution)/shard_map/ppermute | solution.py:23
  109.5 13.3 %collective-permute-start = (bf16[64,2048]{1,0:T(8,128)(2,1)S(1)}, bf16[64,2048]{1,0:T(8,128)(2,1)}, u32[]{:S(2)}, u32[]{:S(2)}) collective-permute-start(bf16[64,2048]{1,0:T(8,128)(2,1)S(1)} %get-tuple-element.18._), channel_id=1, source_target_pairs={{0,1},{1,2},{2,3},{3,0},{4,5},{5,6},{6,7},{7,4},{8,9},{9,10},{10,1... | collective-permute-start | bytes 786440 | tf_op jit(solution)/shard_map/ppermute | solution.py:23
  110.2 1.7 copy-start.4
  115.3 7.6 %collective-permute-start.2 = (bf16[64,2048]{1,0:T(8,128)(2,1)S(1)}, bf16[64,2048]{1,0:T(8,128)(2,1)S(1)}, u32[]{:S(2)}, u32[]{:S(2)}) collective-permute-start(bf16[64,2048]{1,0:T(8,128)(2,1)S(1)} %get-tuple-element.19._), channel_id=1, source_target_pairs={{0,3},{1,0},{2,1},{3,2},{4,7},{5,4},{6,5},{7,6},{8,11},{9,8},{10,9... | collective-permute-start | bytes 786440 | tf_op jit(solution)/shard_map/ppermute | solution.py:23
  117.6 5.3 %copy-start.9 = (bf16[1,64,2048]{2,1,0:T(8,128)(2,1)S(1)}, bf16[1,64,2048]{2,1,0:T(8,128)(2,1)}, u32[]{:S(2)}) copy-start(bf16[1,64,2048]{2,1,0:T(8,128)(2,1)} %param.16) | copy-start | bytes 786436
  117.6 6.6 %copy-start.13 = (f32[2048]{0:T(1024)S(1)}, f32[2048]{0:T(1024)}, u32[]{:S(2)}) copy-start(f32[2048]{0:T(1024)} %param.26) | copy-start | bytes 24580
  120.9 30.1 %copy-start = (f32[3,1408]{1,0:T(4,128)S(1)}, f32[3,1408]{1,0:T(4,128)}, u32[]{:S(2)}) copy-start(f32[3,1408]{1,0:T(4,128)} %refs_12_.1) | copy-start | bytes 50692
  120.9 30.1 %copy-start.1 = (f32[3,1408]{1,0:T(4,128)S(1)}, f32[3,1408]{1,0:T(4,128)}, u32[]{:S(2)}) copy-start(f32[3,1408]{1,0:T(4,128)} %refs_13_.1) | copy-start | bytes 50692
  124.3 21.1 %collective-permute-start.3 = (bf16[64,2048]{1,0:T(8,128)(2,1)S(1)}, bf16[64,2048]{1,0:T(8,128)(2,1)S(1)}, u32[]{:S(2)}, u32[]{:S(2)}) collective-permute-start(bf16[64,2048]{1,0:T(8,128)(2,1)S(1)} %multiply_convert_fusion.1.refs_0_), channel_id=1, source_target_pairs={{0,1},{1,2},{2,3},{3,0},{4,5},{5,6},{6,7},{7,4},{8,9},{9,10},{10,1... | collective-permute-start | bytes 786440 | tf_op jit(solution)/shard_map/ppermute | solution.py:23
  124.7 20.7 %collective-permute-start.4 = (bf16[64,2048]{1,0:T(8,128)(2,1)S(1)}, bf16[64,2048]{1,0:T(8,128)(2,1)S(1)}, u32[]{:S(2)}, u32[]{:S(2)}) collective-permute-start(bf16[64,2048]{1,0:T(8,128)(2,1)S(1)} %multiply_convert_fusion.1.refs_0_), channel_id=1, source_target_pairs={{0,2},{1,3},{2,0},{3,1},{4,6},{5,7},{6,4},{7,5},{8,10},{9,11},{10,... | collective-permute-start | bytes 786440 | tf_op jit(solution)/shard_map/ppermute | solution.py:23
  128.9 16.5 %collective-permute-start.5 = (bf16[64,2048]{1,0:T(8,128)(2,1)S(1)}, bf16[64,2048]{1,0:T(8,128)(2,1)S(1)}, u32[]{:S(2)}, u32[]{:S(2)}) collective-permute-start(bf16[64,2048]{1,0:T(8,128)(2,1)S(1)} %multiply_convert_fusion.1.refs_0_), channel_id=1, source_target_pairs={{0,3},{1,0},{2,1},{3,2},{4,7},{5,4},{6,5},{7,6},{8,11},{9,8},{10,9... | collective-permute-start | bytes 786440 | tf_op jit(solution)/shard_map/ppermute | solution.py:23
  128.9 7.4 %collective-permute-start.6 = (bf16[8,2048]{1,0:T(8,128)(2,1)S(1)}, bf16[8,2048]{1,0:T(8,128)(2,1)S(1)}, u32[]{:S(2)}, u32[]{:S(2)}) collective-permute-start(bf16[8,2048]{1,0:T(8,128)(2,1)S(1)} %slice.28), channel_id=1, source_target_pairs={{0,4},{4,8},{8,12},{12,16},{16,20},{20,24},{24,28},{28,32},{32,36}... | collective-permute-start | bytes 98312 | tf_op jit(solution)/shard_map/ppermute | solution.py:28
  136.4 5.9 %collective-permute-start.7 = (bf16[8,2048]{1,0:T(8,128)(2,1)S(1)}, bf16[8,2048]{1,0:T(8,128)(2,1)S(1)}, u32[]{:S(2)}, u32[]{:S(2)}) collective-permute-start(bf16[8,2048]{1,0:T(8,128)(2,1)S(1)} %collective-permute-done.6.refs_4_), channel_id=1, source_target_pairs={{0,1},{1,2},{2,3},{3,0},{4,5},{5,6},{6,7},{7,4},{8,9},{9,10},{10,1... | collective-permute-start | bytes 98312 | tf_op jit(solution)/shard_map/ppermute | solution.py:23
  138.3 4.3 %collective-permute-start.8 = (bf16[8,2048]{1,0:T(8,128)(2,1)S(1)}, bf16[8,2048]{1,0:T(8,128)(2,1)S(1)}, u32[]{:S(2)}, u32[]{:S(2)}) collective-permute-start(bf16[8,2048]{1,0:T(8,128)(2,1)S(1)} %collective-permute-done.6.refs_4_), channel_id=1, source_target_pairs={{0,2},{1,3},{2,0},{3,1},{4,6},{5,7},{6,4},{7,5},{8,10},{9,11},{10,... | collective-permute-start | bytes 98312 | tf_op jit(solution)/shard_map/ppermute | solution.py:23
  142.2 3.2 %collective-permute-start.9 = (bf16[8,2048]{1,0:T(8,128)(2,1)S(1)}, bf16[8,2048]{1,0:T(8,128)(2,1)S(1)}, u32[]{:S(2)}, u32[]{:S(2)}) collective-permute-start(bf16[8,2048]{1,0:T(8,128)(2,1)S(1)} %collective-permute-done.6.refs_4_), channel_id=1, source_target_pairs={{0,3},{1,0},{2,1},{3,2},{4,7},{5,4},{6,5},{7,6},{8,11},{9,8},{10,9... | collective-permute-start | bytes 98312 | tf_op jit(solution)/shard_map/ppermute | solution.py:23
  160.8 13.9 %collective-permute-start.10 = (bf16[64,2048]{1,0:T(8,128)(2,1)S(1)}, bf16[64,2048]{1,0:T(8,128)(2,1)S(1)}, u32[]{:S(2)}, u32[]{:S(2)}) collective-permute-start(bf16[64,2048]{1,0:T(8,128)(2,1)S(1)} %get-tuple-element.26), channel_id=1, source_target_pairs={{0,3},{1,0},{2,1},{3,2},{4,7},{5,4},{6,5},{7,6},{8,11},{9,8},{10,9... | collective-permute-start | bytes 786440 | tf_op jit(solution)/shard_map/ppermute | solution.py:23
  163.8 10.9 %collective-permute-start.11 = (bf16[64,2048]{1,0:T(8,128)(2,1)S(1)}, bf16[64,2048]{1,0:T(8,128)(2,1)S(1)}, u32[]{:S(2)}, u32[]{:S(2)}) collective-permute-start(bf16[64,2048]{1,0:T(8,128)(2,1)S(1)} %get-tuple-element.27), channel_id=1, source_target_pairs={{0,2},{1,3},{2,0},{3,1},{4,6},{5,7},{6,4},{7,5},{8,10},{9,11},{10,... | collective-permute-start | bytes 786440 | tf_op jit(solution)/shard_map/ppermute | solution.py:23
  164.0 15.1 %collective-permute-start.12 = (bf16[64,2048]{1,0:T(8,128)(2,1)S(1)}, bf16[64,2048]{1,0:T(8,128)(2,1)S(1)}, u32[]{:S(2)}, u32[]{:S(2)}) collective-permute-start(bf16[64,2048]{1,0:T(8,128)(2,1)S(1)} %get-tuple-element.28), channel_id=1, source_target_pairs={{0,1},{1,2},{2,3},{3,0},{4,5},{5,6},{6,7},{7,4},{8,9},{9,10},{10,1... | collective-permute-start | bytes 786440 | tf_op jit(solution)/shard_map/ppermute | solution.py:23
Sparse Core Ops, SparseCore 0:
  9.2 141.8 all-gather.2

commit v4 on v3

--- a/solution.py
+++ b/solution.py
@@ -6,6 +6,7 @@
 from jax.experimental import pallas as pl
 from jax.experimental.pallas import tpu as pltpu
 from jax.sharding import PartitionSpec as P
+
 
 NORM_EPS = 1e-06
 ROPE_BASE = 500000.0
@@ -15,6 +16,7 @@
 VAL_UP = 8192.0
 LANES = 128
 EDGE = 8
+WEIGHT_UP = 262144.0
 AHEAD = 3
 
 
@@ -182,32 +184,37 @@
     )(place, lam, q_one, q_two, window, cosine, sine, docs, gain, out_weight, after)
 
 
-def feed_forward(blocks, edges, same, weights, conv_gate, conv_value):
+def feed_forward(blocks, edges, same, early, weights, conv_gate, conv_value):
     rows, width = blocks[0].shape
     count = len(blocks)
     span = rows + EDGE
     total = span * count
     hidden = conv_gate.shape[1]
     step = 2 * LANES
-    cuts = [(a, min(a + step, hidden)) for a in range(0, hidden, step)]
-    out_step = 4 * LANES
+    ready = early.shape[1] // 2
+    later = hidden - ready
+    bounds = [0, ready] + list(range(ready + step, hidden + 1, step))
+    assert bounds[-1] == hidden and ready % LANES == 0
+    cuts = list(zip(bounds[:-1], bounds[1:]))
+    out_step = 16 * LANES
 
     def body(*refs):
         x_in, e_in, m_in = refs[:count], refs[count : 2 * count], refs[2 * count : 3 * count]
-        cg_ref, cv_ref, w_hbm = refs[3 * count : 3 * count + 3]
-        outs = refs[3 * count + 3 : 4 * count + 3]
-        x_ref, w_ref, h_ref, b_ref, sems = refs[4 * count + 3 :]
+        cg_ref, cv_ref, early_ref, w_hbm = refs[3 * count : 3 * count + 4]
+        outs = refs[3 * count + 4 : 4 * count + 4]
+        x_ref, w_ref, h_ref, b_ref, sems = refs[4 * count + 4 :]
 
         def piece(at, low, high, base, a, b):
             spot = (slice(low, high), slice(base + a, base + b))
             return pltpu.make_async_copy(w_hbm.at[spot], w_ref.at[spot], sems.at[at])
 
         queue = []
-        for j, (a, b) in enumerate(cuts):
-            queue.append([piece(2 * j + n, 0, width, n * hidden, a, b) for n in range(2)])
+        for j, (a, b) in enumerate(cuts[1:]):
+            a, b = a - ready, b - ready
+            queue.append([piece(2 * j + n, 0, width, n * later, a, b) for n in range(2)])
         for j in range(0, width, out_step):
             queue.append(
-                [piece(2 * len(cuts) + j // out_step, j, j + out_step, 2 * hidden, 0, hidden)]
+                [piece(2 * len(cuts) + j // out_step, j, j + out_step, 2 * later, 0, hidden)]
             )
 
         def launch(at):
@@ -232,12 +239,15 @@
 
         def raised(j):
             a, b = cuts[j]
-            arrive(j)
+            if j:
+                arrive(j - 1)
+                a, b = a - ready, b - ready
+            source, far = (w_ref, later) if j else (early_ref, ready)
             return [
                 jnp.dot(
-                    x_ref[...], w_ref[:, base + a : base + b], preferred_element_type=jnp.float32
+                    x_ref[...], source[:, base + a : base + b], preferred_element_type=jnp.float32
                 ).astype(jnp.bfloat16)
-                for base in (0, hidden)
+                for base in (0, far)
             ]
 
         upcoming = raised(0)
@@ -261,10 +271,10 @@
                     k * span + EDGE : (k + 1) * span
                 ].astype(jnp.bfloat16)
         for a in range(0, width, out_step):
-            arrive(len(cuts) + a // out_step)
+            arrive(len(cuts) - 1 + a // out_step)
             part = lax.dot_general(
                 h_ref[...],
-                w_ref[a : a + out_step, 2 * hidden : 3 * hidden],
+                w_ref[a : a + out_step, 2 * later : 2 * later + hidden],
                 (((1,), (1,)), ((), ())),
                 preferred_element_type=jnp.float32,
             ).astype(jnp.bfloat16)
@@ -275,18 +285,18 @@
     return pl.pallas_call(
         body,
         out_shape=[jax.ShapeDtypeStruct((rows, width), jnp.bfloat16)] * count,
-        in_specs=[vmem] * (3 * count + 2) + [pl.BlockSpec(memory_space=pltpu.HBM)],
+        in_specs=[vmem] * (3 * count + 3) + [pl.BlockSpec(memory_space=pltpu.HBM)],
         out_specs=[vmem] * count,
         scratch_shapes=[
             pltpu.VMEM((total, width), jnp.bfloat16),
-            pltpu.VMEM((width, 3 * hidden), jnp.bfloat16),
+            pltpu.VMEM((width, 2 * later + hidden), jnp.bfloat16),
             pltpu.VMEM((count * rows, hidden), jnp.bfloat16),
             pltpu.VMEM((total, LANES), jnp.float32),
             pltpu.SemaphoreType.DMA((2 * len(cuts) + width // out_step,)),
         ],
         compiler_params=pltpu.CompilerParams(vmem_limit_bytes=48 * 1024 * 1024),
         name="feed_forward",
-    )(*blocks, *edges, *same, conv_gate, conv_value, weights)
+    )(*blocks, *edges, *same, conv_gate, conv_value, early, weights)
 
 
 def per_device(
@@ -315,7 +325,9 @@
     parts = lax.axis_size("tp")
     model = resid_in.shape[2]
 
-    packed = jnp.concatenate([gate_weight, value_weight, down_weight.T], axis=1)
+    packed = jnp.concatenate(
+        [gate_weight[:, LANES:], value_weight[:, LANES:], down_weight.T], axis=1
+    )
     weights = lax.all_gather(packed, "sp", axis=0, tiled=True)
 
     positions = rank * rows + jnp.arange(rows, dtype=jnp.int32)
@@ -329,14 +341,19 @@
     body_rows = jnp.concatenate([keys, vals], axis=2).reshape(seqs * rows, 2 * LANES)
     doc_rows = jnp.tile(doc_ids.astype(jnp.float32) * KEY_UP, (1, 2 * LANES // rows))
     doc_rows = jnp.pad(doc_rows, ((0, EDGE - seqs), (0, 0)))
-    sent = jnp.concatenate([body_rows, doc_rows], axis=0).astype(jnp.float16)
+    first_weights = jnp.concatenate([gate_weight[:, :LANES], value_weight[:, :LANES]], axis=1)
+    first_weights = first_weights.astype(jnp.float32) * WEIGHT_UP
+    sent = jnp.concatenate([body_rows, doc_rows, first_weights], axis=0).astype(jnp.float16)
     everyone = lax.all_gather(sent, "sp", axis=0, tiled=False)
 
     back = DOC_SPAN // rows
     span = min(back + 2, ranks)
     first = jnp.clip(rank // 2 * 2 - back, 0, ranks - span)
     lanes_down = jnp.where(jnp.arange(2 * LANES) < LANES, 1.0 / KEY_UP, 1.0 / VAL_UP)
-    window = lax.dynamic_slice_in_dim(everyone, first, span, 0)
+    known = seqs * rows + EDGE
+    early = everyone[:, known:].reshape(model, 2 * LANES)
+    early = (early.astype(jnp.float32) * (1.0 / WEIGHT_UP)).astype(jnp.bfloat16)
+    window = lax.dynamic_slice(everyone, (first, 0, 0), (span, known, 2 * LANES))
     window = (window.astype(jnp.float32) * lanes_down).astype(jnp.bfloat16)
     gain = head_gain.reshape(1, -1)
     proj = [None] * parts
@@ -357,7 +374,7 @@
     edge = from_behind(normed[rows - EDGE :], "sp")
     blocks = [normed] + [shifted(normed, "tp", k) for k in range(1, parts)]
     edges = [edge] + [shifted(edge, "tp", k) for k in range(1, parts)]
-    partial = feed_forward(blocks, edges, same, weights, conv_gate, conv_value)
+    partial = feed_forward(blocks, edges, same, early, weights, conv_gate, conv_value)
     out = mid + partial[0].astype(jnp.float32)
     for k in range(1, parts):
         out = out + shifted(partial[k], "tp", -k).astype(jnp.float32)
@@ -383,6 +400,7 @@
         P(None, "tp"),
         P("tp", "sp"),
     )
+
     return jax.shard_map(
         per_device,
         mesh=mesh,

time: 187 us -> 200 us (1.070)
  blocking collectives: 86.1 us -> 101 us
  waiting for transfers between devices: 30.1 us -> 22.6 us
  other arithmetic: 7.09 us -> 10.1 us
  local copies, waits for them, and re-layouts: 3.25 us -> 5.42 us
    all_gather x1, blocking collectives: 86.1 us -> 101 us  [per_device(): everyone = lax.all_gather(sent, 'sp', axis=0, tiled=False)]
    all_gather x1, waiting for transfers between devices: 5.65 us -> 0.02 us  [per_device(): weights = lax.all_gather(packed, 'sp', axis=0, tiled=True)]
    slice x0 -> x4, local copies, waits for them, and re-layouts: none -> 3.3 us  [the longest x1 0.93 us: per_device(): value_weight[:, LANES:]]
    ppermute x12, waiting for transfers between devices: 23.3 us -> 20.8 us  [shifted(): lax.ppermute(array, axis, [(i, (i + by) % length) for i in range(length)])]
    ppermute x12, starting transfers between devices: 17.3 us -> 19.7 us  [shifted(): lax.ppermute(array, axis, [(i, (i + by) % length) for i in range(length)])]
  transfers between devices with their start and end apart: 14 -> 14, of which waited for: 8 -> 6; matrix products, arithmetic and copies ran while one was open for 3% -> 5% of each run, Pallas kernels for 7% -> 7%
where the time goes in v4:
time: 200 us; the launch traced here: 199 us
  blocking collectives  101 us (50%)
  starting transfers between devices  24.3 us (12%)
  waiting for transfers between devices  22.6 us (11%)
  Pallas kernels  22.3 us (11%)
  between operations  13.8 us (7%)
  other arithmetic  10.1 us (5%)
  local copies, waits for them, and re-layouts  5.42 us (3%)
    all_gather x1, blocking collectives, per_device(): everyone = lax.all_gather(sent, 'sp', axis=0, tiled=False)  101 us
    ppermute x12, waiting for transfers between devices, shifted(): lax.ppermute(array, axis, [(i, (i + by) % length) for i in range(length)])  20.8 us
    ppermute x12, starting transfers between devices, shifted(): lax.ppermute(array, axis, [(i, (i + by) % length) for i in range(length)])  19.7 us
    pallas_call x4, Pallas kernels, attend(): pl.pallas_call(body, out_shape=(jax.ShapeDtypeStruct((rows, model), jnp.b...  13.3 us
    pallas_call x1, Pallas kernels, feed_forward(): pl.pallas_call(body, out_shape=[jax.ShapeDtypeStruct((rows, width), jnp.b...  8.98 us
    ppermute x1, starting transfers between devices, from_behind(): return lax.ppermute(array, axis, [(i, i + 1) for i in range(length - 1)])  4.67 us
  transfers between devices with their start and end apart: 14, of which 6 were waited for; matrix products, arithmetic and copies ran while one was open for 5% of the time, Pallas kernels for 7%

profile of v4, /device:TPU:33, one launch (start us, length us, event | category | flops | bytes accessed | tf_op | source)
XLA Modules:
  0.0 199.3 jit_solution(16824491719427977591)
XLA Ops:
  6.6 0.9 slice.42
  7.5 0.9 slice.43
  8.4 1.8 pad_maximum_fusion
  10.2 0.1 all-gather.3.cloned.1.call-update
  10.3 0.7 slice.38
  11.0 0.7 slice.39
  11.7 0.1 multiply_cosine_fusion
  11.9 0.1 copy.27.c_ref
  12.0 0.1 copy.28.s_ref
  12.0 0.7 multiply_convert_fusion.6
  12.8 0.1 tile.33
  12.9 0.1 add_add_fusion.2
  13.0 1.0 maximum_convert_fusion
  13.9 0.9 multiply_convert_fusion.3
  14.8 0.1 fusion.11
  14.9 0.1 fusion.12
  15.0 1.0 multiply_convert_fusion.4
  16.1 0.1 pad_maximum_fusion.1
  16.2 0.0 copy-start.2
  16.2 0.0 copy-start.3
  16.2 0.0 copy-start.5
  16.2 0.0 copy-start.6
  16.2 0.0 copy-start.7
  16.2 0.0 copy-start.8
  16.2 100.8 %all-gather.4 = f16[32,328,256]{2,1,0:T(8,128)(2,1)S(1)} all-gather(f16[1,328,256]{2,1,0:T(8,128)(2,1)S(1)} %pad_maximum_fusion.1), channel_id=1, replica_groups=mesh['grp'=2,'sp'=32,'tp'=4] {'sp'}, dimensions={0}, use_global_device_ids=true | all-gather | bytes 5541888 | tf_op jit(solution)/shard_map/all_gather | solution.py:347
  117.0 0.5 multiply_convert_fusion.w_ref
  117.6 3.3 %attend.4 = (bf16[64,2048]{1,0:T(8,128)(2,1)S(1)}, f32[64,128]{1,0:T(8,128)S(1)}) custom-call(s32[3]{0:T(128)S(1)} %get-tuple-element.41.place_ref, f32[8]{0:T(128)S(1)} %copy-done.7, bf16[4,64,256]{2,1,0:T(8,128)(2,1)S(1)} %copy-done.5, bf16[4,64,256]{2,1,0:T(8,128)(2,1)S(1)} %copy-done.6, bf16[18,264,256]{2,1,0:T(8,128)(2,1)S(1)} %multiply_convert_fusion.w_ref, ...), custom_call_target="tpu_custom_call" | custom-call | flops 3000000000 | bytes 4000000 | tf_op jit(solution)/shard_map/attend/pallas_call | solution.py:170
  121.0 3.4 %collective-permute-start.1 = (bf16[64,2048]{1,0:T(8,128)(2,1)S(1)}, bf16[64,2048]{1,0:T(8,128)(2,1)}, u32[]{:S(2)}, u32[]{:S(2)}) collective-permute-start(bf16[64,2048]{1,0:T(8,128)(2,1)S(1)} %get-tuple-element.17._), channel_id=1, source_target_pairs={{0,2},{1,3},{2,0},{3,1},{4,6},{5,7},{6,4},{7,5},{8,10},{9,11},{10,... | collective-permute-start | bytes 786440 | tf_op jit(solution)/shard_map/ppermute | solution.py:25
  124.3 3.3 %attend.5 = (bf16[64,2048]{1,0:T(8,128)(2,1)S(1)}, f32[64,128]{1,0:T(8,128)S(1)}) custom-call(s32[3]{0:T(128)S(1)} %get-tuple-element.40.place_ref, f32[8]{0:T(128)S(1)} %copy-done.7, bf16[4,64,256]{2,1,0:T(8,128)(2,1)S(1)} %copy-done.5, bf16[4,64,256]{2,1,0:T(8,128)(2,1)S(1)} %copy-done.6, bf16[18,264,256]{2,1,0:T(8,128)(2,1)S(1)} %multiply_convert_fusion.w_ref, ...), custom_call_target="tpu_custom_call" | custom-call | flops 3000000000 | bytes 4000000 | tf_op jit(solution)/shard_map/attend/pallas_call | solution.py:170
  127.6 0.6 collective-permute-start
  128.3 0.1 add_add_fusion
  128.3 1.6 copy-done.4
  130.0 3.3 %attend.6 = (bf16[64,2048]{1,0:T(8,128)(2,1)S(1)}, f32[64,128]{1,0:T(8,128)S(1)}) custom-call(s32[3]{0:T(128)S(1)} %get-tuple-element.39.place_ref, f32[8]{0:T(128)S(1)} %copy-done.7, bf16[4,64,256]{2,1,0:T(8,128)(2,1)S(1)} %copy-done.5, bf16[4,64,256]{2,1,0:T(8,128)(2,1)S(1)} %copy-done.6, bf16[18,264,256]{2,1,0:T(8,128)(2,1)S(1)} %multiply_convert_fusion.w_ref, ...), custom_call_target="tpu_custom_call" | custom-call | flops 3000000000 | bytes 4000000 | tf_op jit(solution)/shard_map/attend/pallas_call | solution.py:170
  133.3 2.5 %collective-permute-start.2 = (bf16[64,2048]{1,0:T(8,128)(2,1)S(1)}, bf16[64,2048]{1,0:T(8,128)(2,1)S(1)}, u32[]{:S(2)}, u32[]{:S(2)}) collective-permute-start(bf16[64,2048]{1,0:T(8,128)(2,1)S(1)} %get-tuple-element.19._), channel_id=1, source_target_pairs={{0,3},{1,0},{2,1},{3,2},{4,7},{5,4},{6,5},{7,6},{8,11},{9,8},{10,9... | collective-permute-start | bytes 786440 | tf_op jit(solution)/shard_map/ppermute | solution.py:25
  135.8 3.3 %attend.7 = (bf16[64,2048]{1,0:T(8,128)(2,1)S(1)}, f32[64,128]{1,0:T(8,128)S(1)}) custom-call(s32[3]{0:T(128)S(1)} %get-tuple-element.38.place_ref, f32[8]{0:T(128)S(1)} %copy-done.7, bf16[4,64,256]{2,1,0:T(8,128)(2,1)S(1)} %copy-done.5, bf16[4,64,256]{2,1,0:T(8,128)(2,1)S(1)} %copy-done.6, bf16[18,264,256]{2,1,0:T(8,128)(2,1)S(1)} %multiply_convert_fusion.w_ref, ...), custom_call_target="tpu_custom_call" | custom-call | flops 3000000000 | bytes 4000000 | tf_op jit(solution)/shard_map/attend/pallas_call | solution.py:170
  139.1 1.7 collective-permute-done.2
  140.8 0.0 collective-permute-done
  140.8 0.0 collective-permute-done.1
  140.9 1.3 multiply_reduce_fusion
  142.2 0.1 multiply_convert_fusion.2.refs_0_
  142.4 4.7 %collective-permute-start.6 = (bf16[8,2048]{1,0:T(8,128)(2,1)S(1)}, bf16[8,2048]{1,0:T(8,128)(2,1)S(1)}, u32[]{:S(2)}, u32[]{:S(2)}) collective-permute-start(bf16[8,2048]{1,0:T(8,128)(2,1)S(1)} %slice.48), channel_id=1, source_target_pairs={{0,4},{4,8},{8,12},{12,16},{16,20},{20,24},{24,28},{28,32},{32,36}... | collective-permute-start | bytes 98312 | tf_op jit(solution)/shard_map/ppermute | solution.py:30
  147.0 1.7 collective-permute-done.6.refs_4_
  148.7 0.0 collective-permute-start.7
  148.7 1.5 collective-permute-start.3
  150.2 3.0 %collective-permute-start.4 = (bf16[64,2048]{1,0:T(8,128)(2,1)S(1)}, bf16[64,2048]{1,0:T(8,128)(2,1)S(1)}, u32[]{:S(2)}, u32[]{:S(2)}) collective-permute-start(bf16[64,2048]{1,0:T(8,128)(2,1)S(1)} %multiply_convert_fusion.2.refs_0_), channel_id=1, source_target_pairs={{0,2},{1,3},{2,0},{3,1},{4,6},{5,7},{6,4},{7,5},{8,10},{9,11},{10,... | collective-permute-start | bytes 786440 | tf_op jit(solution)/shard_map/ppermute | solution.py:25
  153.2 2.1 %collective-permute-start.5 = (bf16[64,2048]{1,0:T(8,128)(2,1)S(1)}, bf16[64,2048]{1,0:T(8,128)(2,1)S(1)}, u32[]{:S(2)}, u32[]{:S(2)}) collective-permute-start(bf16[64,2048]{1,0:T(8,128)(2,1)S(1)} %multiply_convert_fusion.2.refs_0_), channel_id=1, source_target_pairs={{0,3},{1,0},{2,1},{3,2},{4,7},{5,4},{6,5},{7,6},{8,11},{9,8},{10,9... | collective-permute-start | bytes 786440 | tf_op jit(solution)/shard_map/ppermute | solution.py:25
  155.2 0.0 collective-permute-start.8
  155.3 0.0 collective-permute-done.7.refs_5_
  155.3 1.8 collective-permute-start.9
  157.1 1.5 multiply_convert_fusion.1
  158.6 6.1 %collective-permute-done.8.refs_6_ = bf16[8,2048]{1,0:T(8,128)(2,1)S(1)} collective-permute-done((bf16[8,2048]{1,0:T(8,128)(2,1)S(1)}, bf16[8,2048]{1,0:T(8,128)(2,1)S(1)}, u32[]{:S(2)}, u32[]{:S(2)}) %collective-permute-start.8) | collective-permute-done | bytes 32800 | tf_op jit(solution)/shard_map/ppermute | solution.py:25
  164.6 0.0 collective-permute-done.9.refs_7_
  164.6 0.0 collective-permute-done.3.refs_1_
  164.6 0.0 collective-permute-done.4.refs_2_
  164.6 0.0 collective-permute-done.5.refs_3_
  164.6 0.0 all-gather.3.cloned.1.call-done.refs_15_
  164.7 9.0 %feed_forward.1 = (bf16[64,2048]{1,0:T(8,128)(2,1)S(1)}, bf16[64,2048]{1,0:T(8,128)(2,1)S(1)}, bf16[64,2048]{1,0:T(8,128)(2,1)S(1)}, bf16[64,2048]{1,0:T(8,128)(2,1)S(1)}) custom-call(bf16[64,2048]{1,0:T(8,128)(2,1)S(1)} %multiply_convert_fusion.2.refs_0_, bf16[64,2048]{1,0:T(8,128)(2,1)S(1)} %collective-permute-done.3.refs_1_, ...), custom_call_target="tpu_custom_call" | custom-call | tf_op jit(solution)/shard_map/feed_forward/pallas_call | solution.py:285
  173.7 2.5 %collective-permute-start.10 = (bf16[64,2048]{1,0:T(8,128)(2,1)S(1)}, bf16[64,2048]{1,0:T(8,128)(2,1)S(1)}, u32[]{:S(2)}, u32[]{:S(2)}) collective-permute-start(bf16[64,2048]{1,0:T(8,128)(2,1)S(1)} %get-tuple-element.26), channel_id=1, source_target_pairs={{0,3},{1,0},{2,1},{3,2},{4,7},{5,4},{6,5},{7,6},{8,11},{9,8},{10,9... | collective-permute-start | bytes 786440 | tf_op jit(solution)/shard_map/ppermute | solution.py:25
  176.1 2.3 %collective-permute-start.11 = (bf16[64,2048]{1,0:T(8,128)(2,1)S(1)}, bf16[64,2048]{1,0:T(8,128)(2,1)S(1)}, u32[]{:S(2)}, u32[]{:S(2)}) collective-permute-start(bf16[64,2048]{1,0:T(8,128)(2,1)S(1)} %get-tuple-element.27), channel_id=1, source_target_pairs={{0,2},{1,3},{2,0},{3,1},{4,6},{5,7},{6,4},{7,5},{8,10},{9,11},{10,... | collective-permute-start | bytes 786440 | tf_op jit(solution)/shard_map/ppermute | solution.py:25
  178.5 0.0 collective-permute-start.12
  178.5 5.1 %collective-permute-done.10 = bf16[64,2048]{1,0:T(8,128)(2,1)S(1)} collective-permute-done((bf16[64,2048]{1,0:T(8,128)(2,1)S(1)}, bf16[64,2048]{1,0:T(8,128)(2,1)S(1)}, u32[]{:S(2)}, u32[]{:S(2)}) %collective-permute-start.10) | collective-permute-done | bytes 262176 | tf_op jit(solution)/shard_map/ppermute | solution.py:25
  183.6 1.8 collective-permute-done.11
  185.3 6.2 %collective-permute-done.12 = bf16[64,2048]{1,0:T(8,128)(2,1)S(1)} collective-permute-done((bf16[64,2048]{1,0:T(8,128)(2,1)S(1)}, bf16[64,2048]{1,0:T(8,128)(2,1)S(1)}, u32[]{:S(2)}, u32[]{:S(2)}) %collective-permute-start.12) | collective-permute-done | bytes 262176 | tf_op jit(solution)/shard_map/ppermute | solution.py:25
  191.6 0.9 fusion.3
  (31 shorter events, 0.2 us)
Async XLA Ops:
  6.5 158.1 %all-gather.3.cloned.1.call-start = ((), (), s32[]{:S(2)}) async-start(), calls=%async_computation | async-start | bytes 16760832 | tf_op jit(solution)/shard_map/all_gather | solution.py:331
  16.2 101.4 %copy-start.2 = (s32[4,64]{1,0:T(4,128)S(1)}, s32[4,64]{1,0:T(4,128)}, u32[]{:S(2)}) copy-start(s32[4,64]{1,0:T(4,128)} %d_ref.7) | copy-start | bytes 3076
  16.2 101.4 %copy-start.3 = (bf16[512,2048]{1,0:T(8,128)(2,1)S(1)}, bf16[512,2048]{1,0:T(8,128)(2,1)}, u32[]{:S(2)}) copy-start(bf16[512,2048]{1,0:T(8,128)(2,1)} %p_ref.7) | copy-start | bytes 6291460
  16.2 101.4 %copy-start.5 = (bf16[4,64,256]{2,1,0:T(8,128)(2,1)S(1)}, bf16[4,64,256]{2,1,0:T(8,128)(2,1)}, u32[]{:S(2)}) copy-start(bf16[4,64,256]{2,1,0:T(8,128)(2,1)} %q1_ref.7) | copy-start | bytes 393220
  16.2 101.4 %copy-start.6 = (bf16[4,64,256]{2,1,0:T(8,128)(2,1)S(1)}, bf16[4,64,256]{2,1,0:T(8,128)(2,1)}, u32[]{:S(2)}) copy-start(bf16[4,64,256]{2,1,0:T(8,128)(2,1)} %q2_ref.7) | copy-start | bytes 393220
  16.2 101.4 %copy-start.7 = (f32[8]{0:T(128)S(1)}, f32[8]{0:T(128)}, u32[]{:S(2)}) copy-start(f32[8]{0:T(128)} %lam_ref.7) | copy-start | bytes 100
  16.2 101.4 %copy-start.8 = (f32[64]{0:T(128)S(1)}, f32[64]{0:T(128)}, u32[]{:S(2)}) copy-start(f32[64]{0:T(128)} %param.23) | copy-start | bytes 772
  117.0 3.9 %copy-start.9 = (f16[32,328,256]{2,1,0:T(8,128)(2,1)}, f16[32,328,256]{2,1,0:T(8,128)(2,1)S(1)}, u32[]{:S(2)}) copy-start(f16[32,328,256]{2,1,0:T(8,128)(2,1)S(1)} %all-gather.4) | copy-start | bytes 16121860
  121.0 19.9 %collective-permute-start.1 = (bf16[64,2048]{1,0:T(8,128)(2,1)S(1)}, bf16[64,2048]{1,0:T(8,128)(2,1)}, u32[]{:S(2)}, u32[]{:S(2)}) collective-permute-start(bf16[64,2048]{1,0:T(8,128)(2,1)S(1)} %get-tuple-element.17._), channel_id=1, source_target_pairs={{0,2},{1,3},{2,0},{3,1},{4,6},{5,7},{6,4},{7,5},{8,10},{9,11},{10,... | collective-permute-start | bytes 786440 | tf_op jit(solution)/shard_map/ppermute | solution.py:25
  127.6 13.2 %collective-permute-start = (bf16[64,2048]{1,0:T(8,128)(2,1)S(1)}, bf16[64,2048]{1,0:T(8,128)(2,1)}, u32[]{:S(2)}, u32[]{:S(2)}) collective-permute-start(bf16[64,2048]{1,0:T(8,128)(2,1)S(1)} %get-tuple-element.18._), channel_id=1, source_target_pairs={{0,1},{1,2},{2,3},{3,0},{4,5},{5,6},{6,7},{7,4},{8,9},{9,10},{10,1... | collective-permute-start | bytes 786440 | tf_op jit(solution)/shard_map/ppermute | solution.py:25
  128.3 1.6 copy-start.4
  133.3 7.6 %collective-permute-start.2 = (bf16[64,2048]{1,0:T(8,128)(2,1)S(1)}, bf16[64,2048]{1,0:T(8,128)(2,1)S(1)}, u32[]{:S(2)}, u32[]{:S(2)}) collective-permute-start(bf16[64,2048]{1,0:T(8,128)(2,1)S(1)} %get-tuple-element.19._), channel_id=1, source_target_pairs={{0,3},{1,0},{2,1},{3,2},{4,7},{5,4},{6,5},{7,6},{8,11},{9,8},{10,9... | collective-permute-start | bytes 786440 | tf_op jit(solution)/shard_map/ppermute | solution.py:25
  135.8 5.1 %copy-start.10 = (bf16[1,64,2048]{2,1,0:T(8,128)(2,1)S(1)}, bf16[1,64,2048]{2,1,0:T(8,128)(2,1)}, u32[]{:S(2)}) copy-start(bf16[1,64,2048]{2,1,0:T(8,128)(2,1)} %param.16) | copy-start | bytes 786436
  135.8 6.4 %copy-start.11 = (f32[2048]{0:T(1024)S(1)}, f32[2048]{0:T(1024)}, u32[]{:S(2)}) copy-start(f32[2048]{0:T(1024)} %param.26) | copy-start | bytes 24580
  135.8 28.9 %copy-start = (f32[3,1408]{1,0:T(4,128)S(1)}, f32[3,1408]{1,0:T(4,128)}, u32[]{:S(2)}) copy-start(f32[3,1408]{1,0:T(4,128)} %refs_12_.1) | copy-start | bytes 50692
  135.8 28.9 %copy-start.1 = (f32[3,1408]{1,0:T(4,128)S(1)}, f32[3,1408]{1,0:T(4,128)}, u32[]{:S(2)}) copy-start(f32[3,1408]{1,0:T(4,128)} %refs_13_.1) | copy-start | bytes 50692
  142.4 6.3 %collective-permute-start.6 = (bf16[8,2048]{1,0:T(8,128)(2,1)S(1)}, bf16[8,2048]{1,0:T(8,128)(2,1)S(1)}, u32[]{:S(2)}, u32[]{:S(2)}) collective-permute-start(bf16[8,2048]{1,0:T(8,128)(2,1)S(1)} %slice.48), channel_id=1, source_target_pairs={{0,4},{4,8},{8,12},{12,16},{16,20},{20,24},{24,28},{28,32},{32,36}... | collective-permute-start | bytes 98312 | tf_op jit(solution)/shard_map/ppermute | solution.py:30
  148.7 6.6 %collective-permute-start.7 = (bf16[8,2048]{1,0:T(8,128)(2,1)S(1)}, bf16[8,2048]{1,0:T(8,128)(2,1)S(1)}, u32[]{:S(2)}, u32[]{:S(2)}) collective-permute-start(bf16[8,2048]{1,0:T(8,128)(2,1)S(1)} %collective-permute-done.6.refs_4_), channel_id=1, source_target_pairs={{0,1},{1,2},{2,3},{3,0},{4,5},{5,6},{6,7},{7,4},{8,9},{9,10},{10,1... | collective-permute-start | bytes 98312 | tf_op jit(solution)/shard_map/ppermute | solution.py:25
  148.7 15.9 %collective-permute-start.3 = (bf16[64,2048]{1,0:T(8,128)(2,1)S(1)}, bf16[64,2048]{1,0:T(8,128)(2,1)S(1)}, u32[]{:S(2)}, u32[]{:S(2)}) collective-permute-start(bf16[64,2048]{1,0:T(8,128)(2,1)S(1)} %multiply_convert_fusion.2.refs_0_), channel_id=1, source_target_pairs={{0,1},{1,2},{2,3},{3,0},{4,5},{5,6},{6,7},{7,4},{8,9},{9,10},{10,1... | collective-permute-start | bytes 786440 | tf_op jit(solution)/shard_map/ppermute | solution.py:25
  150.2 14.4 %collective-permute-start.4 = (bf16[64,2048]{1,0:T(8,128)(2,1)S(1)}, bf16[64,2048]{1,0:T(8,128)(2,1)S(1)}, u32[]{:S(2)}, u32[]{:S(2)}) collective-permute-start(bf16[64,2048]{1,0:T(8,128)(2,1)S(1)} %multiply_convert_fusion.2.refs_0_), channel_id=1, source_target_pairs={{0,2},{1,3},{2,0},{3,1},{4,6},{5,7},{6,4},{7,5},{8,10},{9,11},{10,... | collective-permute-start | bytes 786440 | tf_op jit(solution)/shard_map/ppermute | solution.py:25
  153.2 11.4 %collective-permute-start.5 = (bf16[64,2048]{1,0:T(8,128)(2,1)S(1)}, bf16[64,2048]{1,0:T(8,128)(2,1)S(1)}, u32[]{:S(2)}, u32[]{:S(2)}) collective-permute-start(bf16[64,2048]{1,0:T(8,128)(2,1)S(1)} %multiply_convert_fusion.2.refs_0_), channel_id=1, source_target_pairs={{0,3},{1,0},{2,1},{3,2},{4,7},{5,4},{6,5},{7,6},{8,11},{9,8},{10,9... | collective-permute-start | bytes 786440 | tf_op jit(solution)/shard_map/ppermute | solution.py:25
  155.2 9.4 %collective-permute-start.8 = (bf16[8,2048]{1,0:T(8,128)(2,1)S(1)}, bf16[8,2048]{1,0:T(8,128)(2,1)S(1)}, u32[]{:S(2)}, u32[]{:S(2)}) collective-permute-start(bf16[8,2048]{1,0:T(8,128)(2,1)S(1)} %collective-permute-done.6.refs_4_), channel_id=1, source_target_pairs={{0,2},{1,3},{2,0},{3,1},{4,6},{5,7},{6,4},{7,5},{8,10},{9,11},{10,... | collective-permute-start | bytes 98312 | tf_op jit(solution)/shard_map/ppermute | solution.py:25
  155.3 9.4 %collective-permute-start.9 = (bf16[8,2048]{1,0:T(8,128)(2,1)S(1)}, bf16[8,2048]{1,0:T(8,128)(2,1)S(1)}, u32[]{:S(2)}, u32[]{:S(2)}) collective-permute-start(bf16[8,2048]{1,0:T(8,128)(2,1)S(1)} %collective-permute-done.6.refs_4_), channel_id=1, source_target_pairs={{0,3},{1,0},{2,1},{3,2},{4,7},{5,4},{6,5},{7,6},{8,11},{9,8},{10,9... | collective-permute-start | bytes 98312 | tf_op jit(solution)/shard_map/ppermute | solution.py:25
  173.7 9.9 %collective-permute-start.10 = (bf16[64,2048]{1,0:T(8,128)(2,1)S(1)}, bf16[64,2048]{1,0:T(8,128)(2,1)S(1)}, u32[]{:S(2)}, u32[]{:S(2)}) collective-permute-start(bf16[64,2048]{1,0:T(8,128)(2,1)S(1)} %get-tuple-element.26), channel_id=1, source_target_pairs={{0,3},{1,0},{2,1},{3,2},{4,7},{5,4},{6,5},{7,6},{8,11},{9,8},{10,9... | collective-permute-start | bytes 786440 | tf_op jit(solution)/shard_map/ppermute | solution.py:25
  176.1 9.2 %collective-permute-start.11 = (bf16[64,2048]{1,0:T(8,128)(2,1)S(1)}, bf16[64,2048]{1,0:T(8,128)(2,1)S(1)}, u32[]{:S(2)}, u32[]{:S(2)}) collective-permute-start(bf16[64,2048]{1,0:T(8,128)(2,1)S(1)} %get-tuple-element.27), channel_id=1, source_target_pairs={{0,2},{1,3},{2,0},{3,1},{4,6},{5,7},{6,4},{7,5},{8,10},{9,11},{10,... | collective-permute-start | bytes 786440 | tf_op jit(solution)/shard_map/ppermute | solution.py:25
  178.5 13.1 %collective-permute-start.12 = (bf16[64,2048]{1,0:T(8,128)(2,1)S(1)}, bf16[64,2048]{1,0:T(8,128)(2,1)S(1)}, u32[]{:S(2)}, u32[]{:S(2)}) collective-permute-start(bf16[64,2048]{1,0:T(8,128)(2,1)S(1)} %get-tuple-element.28), channel_id=1, source_target_pairs={{0,1},{1,2},{2,3},{3,0},{4,5},{5,6},{6,7},{7,4},{8,9},{9,10},{10,1... | collective-permute-start | bytes 786440 | tf_op jit(solution)/shard_map/ppermute | solution.py:25
Sparse Core Ops, SparseCore 0:
  10.4 143.7 all-gather.2

commit v5 on v3

--- a/solution.py
+++ b/solution.py
@@ -189,8 +189,9 @@
     total = span * count
     hidden = conv_gate.shape[1]
     step = 2 * LANES
-    cuts = [(a, min(a + step, hidden)) for a in range(0, hidden, step)]
-    out_step = 4 * LANES
+    bounds = [0] + list(range(hidden % step, hidden + 1, step))
+    cuts = list(zip(bounds[:-1], bounds[1:]))
+    out_step = 16 * LANES
 
     def body(*refs):
         x_in, e_in, m_in = refs[:count], refs[count : 2 * count], refs[2 * count : 3 * count]

time: 187 us -> 186 us (level)
  no operation moved by 1% of the time
where the time goes in v5:
time: 186 us
  blocking collectives  86.1 us (46%)
  waiting for transfers between devices  30.1 us (16%)
  starting transfers between devices  23.6 us (13%)
  Pallas kernels  22 us (12%)
  between operations  13.7 us (7%)
  other arithmetic  7.09 us (4%)
  local copies, waits for them, and re-layouts  3.25 us (2%)
    all_gather x1, blocking collectives, per_device(): everyone = lax.all_gather(sent, 'sp', axis=0, tiled=False)  86.1 us
    ppermute x12, waiting for transfers between devices, shifted(): lax.ppermute(array, axis, [(i, (i + by) % length) for i in range(length)])  23.3 us
    ppermute x12, starting transfers between devices, shifted(): lax.ppermute(array, axis, [(i, (i + by) % length) for i in range(length)])  17.2 us
    pallas_call x4, Pallas kernels, attend(): pl.pallas_call(body, out_shape=(jax.ShapeDtypeStruct((rows, model), jnp.b...  13.3 us
    pallas_call x1, Pallas kernels, feed_forward(): pl.pallas_call(body, out_shape=[jax.ShapeDtypeStruct((rows, width), jnp.b...  8.75 us
    ppermute x1, starting transfers between devices, from_behind(): return lax.ppermute(array, axis, [(i, i + 1) for i in range(length - 1)])  6.32 us
    all_gather x1, waiting for transfers between devices, per_device(): weights = lax.all_gather(packed, 'sp', axis=0, tiled=True)  5.65 us
  transfers between devices with their start and end apart: 14, of which 8 were waited for; matrix products, arithmetic and copies ran while one was open for 3% of the time, Pallas kernels for 7%

profile of v5, /device:TPU:33, one launch (start us, length us, event | category | flops | bytes accessed | tf_op | source)
XLA Modules:
  0.0 185.9 jit_solution(12326972256323741858)
XLA Ops:
  6.6 0.0 all-gather.3.cloned.1.call-start
  6.6 2.0 %pad_maximum_fusion = bf16[64,4224]{1,0:T(8,128)(2,1)} fusion(bf16[64,1408]{1,0:T(8,128)(2,1)} %bitcast.26, bf16[64,1408]{1,0:T(8,128)(2,1)} %param.28, bf16[64,1408]{1,0:T(8,128)(2,1)} %param.27), kind=kLoop, calls=%fused_computation.1 | loop fusion | flops 1622016 | bytes 1081344 | tf_op jit(solution)/shard_map/concatenate | solution.py:319
  8.5 0.1 all-gather.3.cloned.1.call-update
  8.7 0.1 multiply_cosine_fusion
  8.8 0.1 copy.27.c_ref
  8.9 0.1 copy.28.s_ref
  9.0 0.7 multiply_convert_fusion.4
  9.7 0.1 tile.33
  9.8 0.1 add_add_fusion.2
  9.9 1.0 maximum_convert_fusion
  10.8 0.0 copy-done.12
  10.9 0.1 fusion.10
  11.0 0.1 fusion.11
  11.1 0.0 copy-done.11
  11.1 0.0 copy-done.10
  11.1 0.2 multiply_convert_fusion.3
  11.4 86.1 %all-gather.4 = f16[32,264,256]{2,1,0:T(8,128)(2,1)S(1)} all-gather(f16[1,264,256]{2,1,0:T(8,128)(2,1)S(1)} %pad_maximum_fusion.1), channel_id=1, replica_groups=mesh['grp'=2,'sp'=32,'tp'=4] {'sp'}, dimensions={0}, use_global_device_ids=true | all-gather | bytes 4460544 | tf_op jit(solution)/shard_map/all_gather | solution.py:334
  97.5 0.0 copy-start.7
  97.5 0.0 copy-start.8
  97.5 0.5 multiply_convert_fusion.w_ref
  98.1 0.1 copy-done.2
  98.2 1.0 copy-done.3
  99.1 0.0 copy-done.5
  99.1 3.3 %attend.4 = (bf16[64,2048]{1,0:T(8,128)(2,1)S(1)}, f32[64,128]{1,0:T(8,128)S(1)}) custom-call(s32[3]{0:T(128)S(1)} %get-tuple-element.41.place_ref, f32[8]{0:T(128)S(1)} %copy-done.7, bf16[4,64,256]{2,1,0:T(8,128)(2,1)S(1)} %copy-done.5, bf16[4,64,256]{2,1,0:T(8,128)(2,1)S(1)} %copy-done.6, bf16[18,264,256]{2,1,0:T(8,128)(2,1)S(1)} %multiply_convert_fusion.w_ref, ...), custom_call_target="tpu_custom_call" | custom-call | flops 3000000000 | bytes 4000000 | tf_op jit(solution)/shard_map/attend/pallas_call | solution.py:168
  102.5 3.7 %collective-permute-start.1 = (bf16[64,2048]{1,0:T(8,128)(2,1)S(1)}, bf16[64,2048]{1,0:T(8,128)(2,1)}, u32[]{:S(2)}, u32[]{:S(2)}) collective-permute-start(bf16[64,2048]{1,0:T(8,128)(2,1)S(1)} %get-tuple-element.17._), channel_id=1, source_target_pairs={{0,2},{1,3},{2,0},{3,1},{4,6},{5,7},{6,4},{7,5},{8,10},{9,11},{10,... | collective-permute-start | bytes 786440 | tf_op jit(solution)/shard_map/ppermute | solution.py:23
  106.2 3.3 %attend.5 = (bf16[64,2048]{1,0:T(8,128)(2,1)S(1)}, f32[64,128]{1,0:T(8,128)S(1)}) custom-call(s32[3]{0:T(128)S(1)} %get-tuple-element.40.place_ref, f32[8]{0:T(128)S(1)} %copy-done.7, bf16[4,64,256]{2,1,0:T(8,128)(2,1)S(1)} %copy-done.5, bf16[4,64,256]{2,1,0:T(8,128)(2,1)S(1)} %copy-done.6, bf16[18,264,256]{2,1,0:T(8,128)(2,1)S(1)} %multiply_convert_fusion.w_ref, ...), custom_call_target="tpu_custom_call" | custom-call | flops 3000000000 | bytes 4000000 | tf_op jit(solution)/shard_map/attend/pallas_call | solution.py:168
  109.5 0.7 collective-permute-start
  110.2 0.1 add_add_fusion
  110.3 1.7 copy-done.4
  111.9 3.3 %attend.6 = (bf16[64,2048]{1,0:T(8,128)(2,1)S(1)}, f32[64,128]{1,0:T(8,128)S(1)}) custom-call(s32[3]{0:T(128)S(1)} %get-tuple-element.39.place_ref, f32[8]{0:T(128)S(1)} %copy-done.7, bf16[4,64,256]{2,1,0:T(8,128)(2,1)S(1)} %copy-done.5, bf16[4,64,256]{2,1,0:T(8,128)(2,1)S(1)} %copy-done.6, bf16[18,264,256]{2,1,0:T(8,128)(2,1)S(1)} %multiply_convert_fusion.w_ref, ...), custom_call_target="tpu_custom_call" | custom-call | flops 3000000000 | bytes 4000000 | tf_op jit(solution)/shard_map/attend/pallas_call | solution.py:168
  115.3 2.3 %collective-permute-start.2 = (bf16[64,2048]{1,0:T(8,128)(2,1)S(1)}, bf16[64,2048]{1,0:T(8,128)(2,1)S(1)}, u32[]{:S(2)}, u32[]{:S(2)}) collective-permute-start(bf16[64,2048]{1,0:T(8,128)(2,1)S(1)} %get-tuple-element.19._), channel_id=1, source_target_pairs={{0,3},{1,0},{2,1},{3,2},{4,7},{5,4},{6,5},{7,6},{8,11},{9,8},{10,9... | collective-permute-start | bytes 786440 | tf_op jit(solution)/shard_map/ppermute | solution.py:23
  117.6 3.3 %attend.7 = (bf16[64,2048]{1,0:T(8,128)(2,1)S(1)}, f32[64,128]{1,0:T(8,128)S(1)}) custom-call(s32[3]{0:T(128)S(1)} %get-tuple-element.38.place_ref, f32[8]{0:T(128)S(1)} %copy-done.7, bf16[4,64,256]{2,1,0:T(8,128)(2,1)S(1)} %copy-done.5, bf16[4,64,256]{2,1,0:T(8,128)(2,1)S(1)} %copy-done.6, bf16[18,264,256]{2,1,0:T(8,128)(2,1)S(1)} %multiply_convert_fusion.w_ref, ...), custom_call_target="tpu_custom_call" | custom-call | flops 3000000000 | bytes 4000000 | tf_op jit(solution)/shard_map/attend/pallas_call | solution.py:168
  120.9 0.0 copy-start
  120.9 0.0 copy-start.1
  120.9 1.9 %collective-permute-done.2 = bf16[64,2048]{1,0:T(8,128)(2,1)S(1)} collective-permute-done((bf16[64,2048]{1,0:T(8,128)(2,1)S(1)}, bf16[64,2048]{1,0:T(8,128)(2,1)S(1)}, u32[]{:S(2)}, u32[]{:S(2)}) %collective-permute-start.2) | collective-permute-done | bytes 262176 | tf_op jit(solution)/shard_map/ppermute | solution.py:23
  122.9 0.0 collective-permute-done
  122.9 0.0 collective-permute-done.1
  122.9 0.0 copy-done.9
  122.9 1.3 multiply_reduce_fusion
  124.2 0.1 multiply_convert_fusion.1.refs_0_
  124.3 0.4 collective-permute-start.3
  124.7 4.2 %collective-permute-start.4 = (bf16[64,2048]{1,0:T(8,128)(2,1)S(1)}, bf16[64,2048]{1,0:T(8,128)(2,1)S(1)}, u32[]{:S(2)}, u32[]{:S(2)}) collective-permute-start(bf16[64,2048]{1,0:T(8,128)(2,1)S(1)} %multiply_convert_fusion.1.refs_0_), channel_id=1, source_target_pairs={{0,2},{1,3},{2,0},{3,1},{4,6},{5,7},{6,4},{7,5},{8,10},{9,11},{10,... | collective-permute-start | bytes 786440 | tf_op jit(solution)/shard_map/ppermute | solution.py:23
  128.9 0.0 collective-permute-start.5
  128.9 6.3 %collective-permute-start.6 = (bf16[8,2048]{1,0:T(8,128)(2,1)S(1)}, bf16[8,2048]{1,0:T(8,128)(2,1)S(1)}, u32[]{:S(2)}, u32[]{:S(2)}) collective-permute-start(bf16[8,2048]{1,0:T(8,128)(2,1)S(1)} %slice.28), channel_id=1, source_target_pairs={{0,4},{4,8},{8,12},{12,16},{16,20},{20,24},{24,28},{28,32},{32,36}... | collective-permute-start | bytes 98312 | tf_op jit(solution)/shard_map/ppermute | solution.py:28
  135.2 1.1 collective-permute-done.6.refs_4_
  136.4 2.0 %collective-permute-start.7 = (bf16[8,2048]{1,0:T(8,128)(2,1)S(1)}, bf16[8,2048]{1,0:T(8,128)(2,1)S(1)}, u32[]{:S(2)}, u32[]{:S(2)}) collective-permute-start(bf16[8,2048]{1,0:T(8,128)(2,1)S(1)} %collective-permute-done.6.refs_4_), channel_id=1, source_target_pairs={{0,1},{1,2},{2,3},{3,0},{4,5},{5,6},{6,7},{7,4},{8,9},{9,10},{10,1... | collective-permute-start | bytes 98312 | tf_op jit(solution)/shard_map/ppermute | solution.py:23
  138.3 0.0 collective-permute-start.8
  138.3 3.9 %collective-permute-done.7.refs_5_ = bf16[8,2048]{1,0:T(8,128)(2,1)S(1)} collective-permute-done((bf16[8,2048]{1,0:T(8,128)(2,1)S(1)}, bf16[8,2048]{1,0:T(8,128)(2,1)S(1)}, u32[]{:S(2)}, u32[]{:S(2)}) %collective-permute-start.7) | collective-permute-done | bytes 32800 | tf_op jit(solution)/shard_map/ppermute | solution.py:23
  142.2 0.0 collective-permute-start.9
  142.2 0.4 collective-permute-done.8.refs_6_
  142.7 2.7 %collective-permute-done.9.refs_7_ = bf16[8,2048]{1,0:T(8,128)(2,1)S(1)} collective-permute-done((bf16[8,2048]{1,0:T(8,128)(2,1)S(1)}, bf16[8,2048]{1,0:T(8,128)(2,1)S(1)}, u32[]{:S(2)}, u32[]{:S(2)}) %collective-permute-start.9) | collective-permute-done | bytes 32800 | tf_op jit(solution)/shard_map/ppermute | solution.py:23
  145.4 0.0 collective-permute-done.3.refs_1_
  145.4 0.0 collective-permute-done.4.refs_2_
  145.4 0.0 collective-permute-done.5.refs_3_
  145.4 5.7 %all-gather.3.cloned.1.call-done.refs_14_ = bf16[2048,4224]{1,0:T(8,128)(2,1)} async-done(((bf16[64,4224]{1,0:T(8,128)(2,1)}), bf16[2048,4224]{1,0:T(8,128)(2,1)}) %all-gather.3.cloned.1.call-update) | async-done | bytes 17301520 | tf_op jit(solution)/shard_map/all_gather | solution.py:320
  151.1 0.0 copy-done.1
  151.1 8.8 %feed_forward.1 = (bf16[64,2048]{1,0:T(8,128)(2,1)S(1)}, bf16[64,2048]{1,0:T(8,128)(2,1)S(1)}, bf16[64,2048]{1,0:T(8,128)(2,1)S(1)}, bf16[64,2048]{1,0:T(8,128)(2,1)S(1)}) custom-call(bf16[64,2048]{1,0:T(8,128)(2,1)S(1)} %multiply_convert_fusion.1.refs_0_, bf16[64,2048]{1,0:T(8,128)(2,1)S(1)} %collective-permute-done.3.refs_1_, ...), custom_call_target="tpu_custom_call" | custom-call | tf_op jit(solution)/shard_map/feed_forward/pallas_call | solution.py:276
  159.8 3.0 %collective-permute-start.10 = (bf16[64,2048]{1,0:T(8,128)(2,1)S(1)}, bf16[64,2048]{1,0:T(8,128)(2,1)S(1)}, u32[]{:S(2)}, u32[]{:S(2)}) collective-permute-start(bf16[64,2048]{1,0:T(8,128)(2,1)S(1)} %get-tuple-element.26), channel_id=1, source_target_pairs={{0,3},{1,0},{2,1},{3,2},{4,7},{5,4},{6,5},{7,6},{8,11},{9,8},{10,9... | collective-permute-start | bytes 786440 | tf_op jit(solution)/shard_map/ppermute | solution.py:23
  162.8 0.3 collective-permute-start.11
  163.1 0.7 collective-permute-start.12
  163.8 9.9 %collective-permute-done.10 = bf16[64,2048]{1,0:T(8,128)(2,1)S(1)} collective-permute-done((bf16[64,2048]{1,0:T(8,128)(2,1)S(1)}, bf16[64,2048]{1,0:T(8,128)(2,1)S(1)}, u32[]{:S(2)}, u32[]{:S(2)}) %collective-permute-start.10) | collective-permute-done | bytes 262176 | tf_op jit(solution)/shard_map/ppermute | solution.py:23
  173.7 0.0 collective-permute-done.11
  173.7 4.5 %collective-permute-done.12 = bf16[64,2048]{1,0:T(8,128)(2,1)S(1)} collective-permute-done((bf16[64,2048]{1,0:T(8,128)(2,1)S(1)}, bf16[64,2048]{1,0:T(8,128)(2,1)S(1)}, u32[]{:S(2)}, u32[]{:S(2)}) %collective-permute-start.12) | collective-permute-done | bytes 262176 | tf_op jit(solution)/shard_map/ppermute | solution.py:23
  178.2 0.9 fusion.3
  (29 shorter events, 0.2 us)
Async XLA Ops:
  6.5 4.5 %copy-start.11 = (bf16[4,64,64]{2,1,0:T(8,128)(2,1)S(1)}, bf16[4,64,64]{2,1,0:T(8,128)(2,1)}, u32[]{:S(2)}) copy-start(bf16[4,64,64]{2,1,0:T(8,128)(2,1)} %param.18) | copy-start | bytes 98308
  6.5 4.6 %copy-start.10 = (bf16[4,64,64]{2,1,0:T(8,128)(2,1)S(1)}, bf16[4,64,64]{2,1,0:T(8,128)(2,1)}, u32[]{:S(2)}) copy-start(bf16[4,64,64]{2,1,0:T(8,128)(2,1)} %param.20) | copy-start | bytes 98308
  6.6 4.3 %copy-start.12 = (bf16[4,64,128]{2,1,0:T(8,128)(2,1)S(1)}, bf16[4,64,128]{2,1,0:T(8,128)(2,1)}, u32[]{:S(2)}) copy-start(bf16[4,64,128]{2,1,0:T(8,128)(2,1)} %param.21) | copy-start | bytes 196612
  6.6 144.5 %all-gather.3.cloned.1.call-start = ((), (), s32[]{:S(2)}) async-start(), calls=%async_computation | async-start | bytes 17842176 | tf_op jit(solution)/shard_map/all_gather | solution.py:320
  97.5 0.7 copy-start.2
  97.5 1.6 copy-start.3
  97.5 1.6 copy-start.5
  97.5 1.6 copy-start.6
  97.5 1.6 copy-start.7
  97.5 1.6 copy-start.8
  102.5 20.4 %collective-permute-start.1 = (bf16[64,2048]{1,0:T(8,128)(2,1)S(1)}, bf16[64,2048]{1,0:T(8,128)(2,1)}, u32[]{:S(2)}, u32[]{:S(2)}) collective-permute-start(bf16[64,2048]{1,0:T(8,128)(2,1)S(1)} %get-tuple-element.17._), channel_id=1, source_target_pairs={{0,2},{1,3},{2,0},{3,1},{4,6},{5,7},{6,4},{7,5},{8,10},{9,11},{10,... | collective-permute-start | bytes 786440 | tf_op jit(solution)/shard_map/ppermute | solution.py:23
  109.5 13.3 %collective-permute-start = (bf16[64,2048]{1,0:T(8,128)(2,1)S(1)}, bf16[64,2048]{1,0:T(8,128)(2,1)}, u32[]{:S(2)}, u32[]{:S(2)}) collective-permute-start(bf16[64,2048]{1,0:T(8,128)(2,1)S(1)} %get-tuple-element.18._), channel_id=1, source_target_pairs={{0,1},{1,2},{2,3},{3,0},{4,5},{5,6},{6,7},{7,4},{8,9},{9,10},{10,1... | collective-permute-start | bytes 786440 | tf_op jit(solution)/shard_map/ppermute | solution.py:23
  110.2 1.7 copy-start.4
  115.3 7.6 %collective-permute-start.2 = (bf16[64,2048]{1,0:T(8,128)(2,1)S(1)}, bf16[64,2048]{1,0:T(8,128)(2,1)S(1)}, u32[]{:S(2)}, u32[]{:S(2)}) collective-permute-start(bf16[64,2048]{1,0:T(8,128)(2,1)S(1)} %get-tuple-element.19._), channel_id=1, source_target_pairs={{0,3},{1,0},{2,1},{3,2},{4,7},{5,4},{6,5},{7,6},{8,11},{9,8},{10,9... | collective-permute-start | bytes 786440 | tf_op jit(solution)/shard_map/ppermute | solution.py:23
  117.6 5.3 %copy-start.9 = (bf16[1,64,2048]{2,1,0:T(8,128)(2,1)S(1)}, bf16[1,64,2048]{2,1,0:T(8,128)(2,1)}, u32[]{:S(2)}) copy-start(bf16[1,64,2048]{2,1,0:T(8,128)(2,1)} %param.16) | copy-start | bytes 786436
  117.6 6.6 %copy-start.13 = (f32[2048]{0:T(1024)S(1)}, f32[2048]{0:T(1024)}, u32[]{:S(2)}) copy-start(f32[2048]{0:T(1024)} %param.26) | copy-start | bytes 24580
  120.9 30.1 %copy-start = (f32[3,1408]{1,0:T(4,128)S(1)}, f32[3,1408]{1,0:T(4,128)}, u32[]{:S(2)}) copy-start(f32[3,1408]{1,0:T(4,128)} %refs_12_.1) | copy-start | bytes 50692
  120.9 30.1 %copy-start.1 = (f32[3,1408]{1,0:T(4,128)S(1)}, f32[3,1408]{1,0:T(4,128)}, u32[]{:S(2)}) copy-start(f32[3,1408]{1,0:T(4,128)} %refs_13_.1) | copy-start | bytes 50692
  124.3 21.1 %collective-permute-start.3 = (bf16[64,2048]{1,0:T(8,128)(2,1)S(1)}, bf16[64,2048]{1,0:T(8,128)(2,1)S(1)}, u32[]{:S(2)}, u32[]{:S(2)}) collective-permute-start(bf16[64,2048]{1,0:T(8,128)(2,1)S(1)} %multiply_convert_fusion.1.refs_0_), channel_id=1, source_target_pairs={{0,1},{1,2},{2,3},{3,0},{4,5},{5,6},{6,7},{7,4},{8,9},{9,10},{10,1... | collective-permute-start | bytes 786440 | tf_op jit(solution)/shard_map/ppermute | solution.py:23
  124.7 20.7 %collective-permute-start.4 = (bf16[64,2048]{1,0:T(8,128)(2,1)S(1)}, bf16[64,2048]{1,0:T(8,128)(2,1)S(1)}, u32[]{:S(2)}, u32[]{:S(2)}) collective-permute-start(bf16[64,2048]{1,0:T(8,128)(2,1)S(1)} %multiply_convert_fusion.1.refs_0_), channel_id=1, source_target_pairs={{0,2},{1,3},{2,0},{3,1},{4,6},{5,7},{6,4},{7,5},{8,10},{9,11},{10,... | collective-permute-start | bytes 786440 | tf_op jit(solution)/shard_map/ppermute | solution.py:23
  128.9 16.5 %collective-permute-start.5 = (bf16[64,2048]{1,0:T(8,128)(2,1)S(1)}, bf16[64,2048]{1,0:T(8,128)(2,1)S(1)}, u32[]{:S(2)}, u32[]{:S(2)}) collective-permute-start(bf16[64,2048]{1,0:T(8,128)(2,1)S(1)} %multiply_convert_fusion.1.refs_0_), channel_id=1, source_target_pairs={{0,3},{1,0},{2,1},{3,2},{4,7},{5,4},{6,5},{7,6},{8,11},{9,8},{10,9... | collective-permute-start | bytes 786440 | tf_op jit(solution)/shard_map/ppermute | solution.py:23
  128.9 7.4 %collective-permute-start.6 = (bf16[8,2048]{1,0:T(8,128)(2,1)S(1)}, bf16[8,2048]{1,0:T(8,128)(2,1)S(1)}, u32[]{:S(2)}, u32[]{:S(2)}) collective-permute-start(bf16[8,2048]{1,0:T(8,128)(2,1)S(1)} %slice.28), channel_id=1, source_target_pairs={{0,4},{4,8},{8,12},{12,16},{16,20},{20,24},{24,28},{28,32},{32,36}... | collective-permute-start | bytes 98312 | tf_op jit(solution)/shard_map/ppermute | solution.py:28
  136.4 5.9 %collective-permute-start.7 = (bf16[8,2048]{1,0:T(8,128)(2,1)S(1)}, bf16[8,2048]{1,0:T(8,128)(2,1)S(1)}, u32[]{:S(2)}, u32[]{:S(2)}) collective-permute-start(bf16[8,2048]{1,0:T(8,128)(2,1)S(1)} %collective-permute-done.6.refs_4_), channel_id=1, source_target_pairs={{0,1},{1,2},{2,3},{3,0},{4,5},{5,6},{6,7},{7,4},{8,9},{9,10},{10,1... | collective-permute-start | bytes 98312 | tf_op jit(solution)/shard_map/ppermute | solution.py:23
  138.3 4.3 %collective-permute-start.8 = (bf16[8,2048]{1,0:T(8,128)(2,1)S(1)}, bf16[8,2048]{1,0:T(8,128)(2,1)S(1)}, u32[]{:S(2)}, u32[]{:S(2)}) collective-permute-start(bf16[8,2048]{1,0:T(8,128)(2,1)S(1)} %collective-permute-done.6.refs_4_), channel_id=1, source_target_pairs={{0,2},{1,3},{2,0},{3,1},{4,6},{5,7},{6,4},{7,5},{8,10},{9,11},{10,... | collective-permute-start | bytes 98312 | tf_op jit(solution)/shard_map/ppermute | solution.py:23
  142.2 3.2 %collective-permute-start.9 = (bf16[8,2048]{1,0:T(8,128)(2,1)S(1)}, bf16[8,2048]{1,0:T(8,128)(2,1)S(1)}, u32[]{:S(2)}, u32[]{:S(2)}) collective-permute-start(bf16[8,2048]{1,0:T(8,128)(2,1)S(1)} %collective-permute-done.6.refs_4_), channel_id=1, source_target_pairs={{0,3},{1,0},{2,1},{3,2},{4,7},{5,4},{6,5},{7,6},{8,11},{9,8},{10,9... | collective-permute-start | bytes 98312 | tf_op jit(solution)/shard_map/ppermute | solution.py:23
  159.8 13.9 %collective-permute-start.10 = (bf16[64,2048]{1,0:T(8,128)(2,1)S(1)}, bf16[64,2048]{1,0:T(8,128)(2,1)S(1)}, u32[]{:S(2)}, u32[]{:S(2)}) collective-permute-start(bf16[64,2048]{1,0:T(8,128)(2,1)S(1)} %get-tuple-element.26), channel_id=1, source_target_pairs={{0,3},{1,0},{2,1},{3,2},{4,7},{5,4},{6,5},{7,6},{8,11},{9,8},{10,9... | collective-permute-start | bytes 786440 | tf_op jit(solution)/shard_map/ppermute | solution.py:23
  162.8 10.9 %collective-permute-start.11 = (bf16[64,2048]{1,0:T(8,128)(2,1)S(1)}, bf16[64,2048]{1,0:T(8,128)(2,1)S(1)}, u32[]{:S(2)}, u32[]{:S(2)}) collective-permute-start(bf16[64,2048]{1,0:T(8,128)(2,1)S(1)} %get-tuple-element.27), channel_id=1, source_target_pairs={{0,2},{1,3},{2,0},{3,1},{4,6},{5,7},{6,4},{7,5},{8,10},{9,11},{10,... | collective-permute-start | bytes 786440 | tf_op jit(solution)/shard_map/ppermute | solution.py:23
  163.1 15.0 %collective-permute-start.12 = (bf16[64,2048]{1,0:T(8,128)(2,1)S(1)}, bf16[64,2048]{1,0:T(8,128)(2,1)S(1)}, u32[]{:S(2)}, u32[]{:S(2)}) collective-permute-start(bf16[64,2048]{1,0:T(8,128)(2,1)S(1)} %get-tuple-element.28), channel_id=1, source_target_pairs={{0,1},{1,2},{2,3},{3,0},{4,5},{5,6},{6,7},{7,4},{8,9},{9,10},{10,1... | collective-permute-start | bytes 786440 | tf_op jit(solution)/shard_map/ppermute | solution.py:23
Sparse Core Ops, SparseCore 0:
  9.2 141.8 all-gather.2

commit v6 on v5

--- a/solution.py
+++ b/solution.py
@@ -182,7 +182,7 @@
     )(place, lam, q_one, q_two, window, cosine, sine, docs, gain, out_weight, after)
 
 
-def feed_forward(blocks, edges, same, weights, conv_gate, conv_value):
+def feed_forward(own, blocks, edges, same, weights, conv_gate, conv_value):
     rows, width = blocks[0].shape
     count = len(blocks)
     span = rows + EDGE
@@ -193,11 +193,10 @@
     cuts = list(zip(bounds[:-1], bounds[1:]))
     out_step = 16 * LANES
 
-    def body(*refs):
+    def body(own_ref, *refs):
         x_in, e_in, m_in = refs[:count], refs[count : 2 * count], refs[2 * count : 3 * count]
         cg_ref, cv_ref, w_hbm = refs[3 * count : 3 * count + 3]
-        outs = refs[3 * count + 3 : 4 * count + 3]
-        x_ref, w_ref, h_ref, b_ref, sems = refs[4 * count + 3 :]
+        o_ref, x_ref, w_ref, h_ref, b_ref, sems = refs[3 * count + 3 :]
 
         def piece(at, low, high, base, a, b):
             spot = (slice(low, high), slice(base + a, base + b))
@@ -270,14 +269,15 @@
                 preferred_element_type=jnp.float32,
             ).astype(jnp.bfloat16)
             for k in range(count):
-                outs[k][:, a : a + out_step] = part[k * rows : (k + 1) * rows]
+                slot = (own_ref[0] - k + count) % count
+                o_ref[slot, :, a : a + out_step] = part[k * rows : (k + 1) * rows]
 
     vmem = pl.BlockSpec(memory_space=pltpu.VMEM)
     return pl.pallas_call(
         body,
-        out_shape=[jax.ShapeDtypeStruct((rows, width), jnp.bfloat16)] * count,
-        in_specs=[vmem] * (3 * count + 2) + [pl.BlockSpec(memory_space=pltpu.HBM)],
-        out_specs=[vmem] * count,
+        out_shape=jax.ShapeDtypeStruct((count, rows, width), jnp.bfloat16),
+        in_specs=[pl.BlockSpec(memory_space=pltpu.SMEM)] + [vmem] * (3 * count + 2) + [pl.BlockSpec(memory_space=pltpu.HBM)],
+        out_specs=vmem,
         scratch_shapes=[
             pltpu.VMEM((total, width), jnp.bfloat16),
             pltpu.VMEM((width, 3 * hidden), jnp.bfloat16),
@@ -287,7 +287,7 @@
         ],
         compiler_params=pltpu.CompilerParams(vmem_limit_bytes=48 * 1024 * 1024),
         name="feed_forward",
-    )(*blocks, *edges, *same, conv_gate, conv_value, weights)
+    )(own, *blocks, *edges, *same, conv_gate, conv_value, weights)
 
 
 def per_device(
@@ -358,10 +358,11 @@
     edge = from_behind(normed[rows - EDGE :], "sp")
     blocks = [normed] + [shifted(normed, "tp", k) for k in range(1, parts)]
     edges = [edge] + [shifted(edge, "tp", k) for k in range(1, parts)]
-    partial = feed_forward(blocks, edges, same, weights, conv_gate, conv_value)
-    out = mid + partial[0].astype(jnp.float32)
-    for k in range(1, parts):
-        out = out + shifted(partial[k], "tp", -k).astype(jnp.float32)
+    partial = feed_forward(
+        own.reshape(1), blocks, edges, same, weights, conv_gate, conv_value
+    )
+    arrived = lax.all_to_all(partial, "tp", 0, 0, tiled=True)
+    out = mid + jnp.sum(arrived.astype(jnp.float32), axis=0)
     return out.astype(jnp.bfloat16)[None]
 
 

time: 186 us -> 187 us (level)
  blocking collectives: 86.1 us -> 105 us
  waiting for transfers between devices: 30.1 us -> 15.7 us
  starting transfers between devices: 23.6 us -> 19.6 us
    all_to_all x0 -> x1, blocking collectives: none -> 18.7 us  [per_device(): arrived = lax.all_to_all(partial, 'tp', 0, 0, tiled=True)]
    ppermute x12 -> x9, waiting for transfers between devices: 23.3 us -> 8.95 us  [shifted(): lax.ppermute(array, axis, [(i, (i + by) % length) for i in range(length)])]
    ppermute x12 -> x9, starting transfers between devices: 17.2 us -> 13.4 us  [shifted(): lax.ppermute(array, axis, [(i, (i + by) % length) for i in range(length)])]
  transfers between devices with their start and end apart: 14 -> 11, of which waited for: 8 -> 6; matrix products, arithmetic and copies ran while one was open for 3% -> 3% of each run, Pallas kernels for 7% -> 7%
where the time goes in v6:
time: 187 us; the launch traced here: 186 us
  blocking collectives  105 us (56%)
  Pallas kernels  22 us (12%)
  starting transfers between devices  19.6 us (10%)
  waiting for transfers between devices  15.7 us (8%)
  between operations  13.7 us (7%)
  other arithmetic  7.16 us (4%)
  local copies, waits for them, and re-layouts  3.25 us (2%)
    all_gather x1, blocking collectives, per_device(): everyone = lax.all_gather(sent, 'sp', axis=0, tiled=False)  86.1 us
    all_to_all x1, blocking collectives, per_device(): arrived = lax.all_to_all(partial, 'tp', 0, 0, tiled=True)  18.7 us
    ppermute x9, starting transfers between devices, shifted(): lax.ppermute(array, axis, [(i, (i + by) % length) for i in range(length)])  13.4 us
    pallas_call x4, Pallas kernels, attend(): pl.pallas_call(body, out_shape=(jax.ShapeDtypeStruct((rows, model), jnp.b...  13.3 us
    ppermute x9, waiting for transfers between devices, shifted(): lax.ppermute(array, axis, [(i, (i + by) % length) for i in range(length)])  8.95 us
    pallas_call x1, Pallas kernels, feed_forward(): pl.pallas_call(body, out_shape=jax.ShapeDtypeStruct((count, rows, width),...  8.76 us
    ppermute x1, starting transfers between devices, from_behind(): return lax.ppermute(array, axis, [(i, i + 1) for i in range(length - 1)])  6.24 us
    all_gather x1, waiting for transfers between devices, per_device(): weights = lax.all_gather(packed, 'sp', axis=0, tiled=True)  5.63 us
  transfers between devices with their start and end apart: 11, of which 6 were waited for; matrix products, arithmetic and copies ran while one was open for 3% of the time, Pallas kernels for 7%

profile of v6, /device:TPU:33, one launch (start us, length us, event | category | flops | bytes accessed | tf_op | source)
XLA Modules:
  0.0 186.4 jit_solution(4333912623604045275)
XLA Ops:
  6.6 0.0 all-gather.3.cloned.1.call-start
  6.6 2.0 %pad_maximum_fusion = bf16[64,4224]{1,0:T(8,128)(2,1)} fusion(bf16[64,1408]{1,0:T(8,128)(2,1)} %bitcast.27, bf16[64,1408]{1,0:T(8,128)(2,1)} %param.28, bf16[64,1408]{1,0:T(8,128)(2,1)} %param.27), kind=kLoop, calls=%fused_computation.2 | loop fusion | flops 1622016 | bytes 1081344 | tf_op jit(solution)/shard_map/concatenate | solution.py:319
  8.6 0.1 all-gather.3.cloned.1.call-update
  8.7 0.1 multiply_cosine_fusion
  8.8 0.1 copy.27.c_ref
  8.9 0.1 copy.28.s_ref
  9.0 0.7 multiply_convert_fusion.4
  9.7 0.1 tile.33
  9.8 0.1 add_add_fusion.2
  9.9 1.0 maximum_convert_fusion
  10.9 0.0 copy-done.12
  10.9 0.1 fusion.10
  11.0 0.1 fusion.11
  11.1 0.0 copy-done.11
  11.1 0.0 copy-done.10
  11.1 0.2 multiply_convert_fusion.3
  11.4 86.1 %all-gather.4 = f16[32,264,256]{2,1,0:T(8,128)(2,1)S(1)} all-gather(f16[1,264,256]{2,1,0:T(8,128)(2,1)S(1)} %pad_maximum_fusion.1), channel_id=1, replica_groups=mesh['grp'=2,'sp'=32,'tp'=4] {'sp'}, dimensions={0}, use_global_device_ids=true | all-gather | bytes 4460544 | tf_op jit(solution)/shard_map/all_gather | solution.py:334
  97.5 0.0 copy-start.7
  97.5 0.0 copy-start.8
  97.5 0.5 multiply_convert_fusion.w_ref
  98.1 0.1 copy-done.2
  98.2 1.0 copy-done.3
  99.1 0.0 copy-done.5
  99.1 0.0 copy-done.6
  99.1 0.0 copy-done.7
  99.1 0.0 copy-done.8
  99.1 3.3 %attend.4 = (bf16[64,2048]{1,0:T(8,128)(2,1)S(1)}, f32[64,128]{1,0:T(8,128)S(1)}) custom-call(s32[3]{0:T(128)S(1)} %get-tuple-element.33.place_ref, f32[8]{0:T(128)S(1)} %copy-done.7, bf16[4,64,256]{2,1,0:T(8,128)(2,1)S(1)} %copy-done.5, bf16[4,64,256]{2,1,0:T(8,128)(2,1)S(1)} %copy-done.6, bf16[18,264,256]{2,1,0:T(8,128)(2,1)S(1)} %multiply_convert_fusion.w_ref, ...), custom_call_target="tpu_custom_call" | custom-call | flops 3000000000 | bytes 4000000 | tf_op jit(solution)/shard_map/attend/pallas_call | solution.py:168
  102.5 3.8 %collective-permute-start.1 = (bf16[64,2048]{1,0:T(8,128)(2,1)S(1)}, bf16[64,2048]{1,0:T(8,128)(2,1)}, u32[]{:S(2)}, u32[]{:S(2)}) collective-permute-start(bf16[64,2048]{1,0:T(8,128)(2,1)S(1)} %get-tuple-element.13._), channel_id=1, source_target_pairs={{0,2},{1,3},{2,0},{3,1},{4,6},{5,7},{6,4},{7,5},{8,10},{9,11},{10,... | collective-permute-start | bytes 786440 | tf_op jit(solution)/shard_map/ppermute | solution.py:23
  106.2 3.3 %attend.5 = (bf16[64,2048]{1,0:T(8,128)(2,1)S(1)}, f32[64,128]{1,0:T(8,128)S(1)}) custom-call(s32[3]{0:T(128)S(1)} %get-tuple-element.32.place_ref, f32[8]{0:T(128)S(1)} %copy-done.7, bf16[4,64,256]{2,1,0:T(8,128)(2,1)S(1)} %copy-done.5, bf16[4,64,256]{2,1,0:T(8,128)(2,1)S(1)} %copy-done.6, bf16[18,264,256]{2,1,0:T(8,128)(2,1)S(1)} %multiply_convert_fusion.w_ref, ...), custom_call_target="tpu_custom_call" | custom-call | flops 3000000000 | bytes 4000000 | tf_op jit(solution)/shard_map/attend/pallas_call | solution.py:168
  109.6 0.6 collective-permute-start
  110.2 0.1 add_add_fusion
  110.3 1.7 copy-done.4
  111.9 3.3 %attend.6 = (bf16[64,2048]{1,0:T(8,128)(2,1)S(1)}, f32[64,128]{1,0:T(8,128)S(1)}) custom-call(s32[3]{0:T(128)S(1)} %get-tuple-element.31.place_ref, f32[8]{0:T(128)S(1)} %copy-done.7, bf16[4,64,256]{2,1,0:T(8,128)(2,1)S(1)} %copy-done.5, bf16[4,64,256]{2,1,0:T(8,128)(2,1)S(1)} %copy-done.6, bf16[18,264,256]{2,1,0:T(8,128)(2,1)S(1)} %multiply_convert_fusion.w_ref, ...), custom_call_target="tpu_custom_call" | custom-call | flops 3000000000 | bytes 4000000 | tf_op jit(solution)/shard_map/attend/pallas_call | solution.py:168
  115.3 2.4 %collective-permute-start.2 = (bf16[64,2048]{1,0:T(8,128)(2,1)S(1)}, bf16[64,2048]{1,0:T(8,128)(2,1)S(1)}, u32[]{:S(2)}, u32[]{:S(2)}) collective-permute-start(bf16[64,2048]{1,0:T(8,128)(2,1)S(1)} %get-tuple-element.15._), channel_id=1, source_target_pairs={{0,3},{1,0},{2,1},{3,2},{4,7},{5,4},{6,5},{7,6},{8,11},{9,8},{10,9... | collective-permute-start | bytes 786440 | tf_op jit(solution)/shard_map/ppermute | solution.py:23
  117.7 3.3 %attend.7 = (bf16[64,2048]{1,0:T(8,128)(2,1)S(1)}, f32[64,128]{1,0:T(8,128)S(1)}) custom-call(s32[3]{0:T(128)S(1)} %get-tuple-element.30.place_ref, f32[8]{0:T(128)S(1)} %copy-done.7, bf16[4,64,256]{2,1,0:T(8,128)(2,1)S(1)} %copy-done.5, bf16[4,64,256]{2,1,0:T(8,128)(2,1)S(1)} %copy-done.6, bf16[18,264,256]{2,1,0:T(8,128)(2,1)S(1)} %multiply_convert_fusion.w_ref, ...), custom_call_target="tpu_custom_call" | custom-call | flops 3000000000 | bytes 4000000 | tf_op jit(solution)/shard_map/attend/pallas_call | solution.py:168
  121.0 0.0 copy-start
  121.0 0.0 copy-start.1
  121.0 1.9 collective-permute-done.2
  122.9 0.0 collective-permute-done
  122.9 0.0 collective-permute-done.1
  122.9 0.0 copy-done.9
  122.9 1.3 multiply_reduce_fusion
  124.2 0.0 copy-done.13
  124.2 0.1 multiply_convert_fusion.1.refs_0_
  124.4 0.4 collective-permute-start.3
  124.7 4.2 %collective-permute-start.4 = (bf16[64,2048]{1,0:T(8,128)(2,1)S(1)}, bf16[64,2048]{1,0:T(8,128)(2,1)S(1)}, u32[]{:S(2)}, u32[]{:S(2)}) collective-permute-start(bf16[64,2048]{1,0:T(8,128)(2,1)S(1)} %multiply_convert_fusion.1.refs_0_), channel_id=1, source_target_pairs={{0,2},{1,3},{2,0},{3,1},{4,6},{5,7},{6,4},{7,5},{8,10},{9,11},{10,... | collective-permute-start | bytes 786440 | tf_op jit(solution)/shard_map/ppermute | solution.py:23
  129.0 0.0 collective-permute-start.5
  129.0 6.2 %collective-permute-start.6 = (bf16[8,2048]{1,0:T(8,128)(2,1)S(1)}, bf16[8,2048]{1,0:T(8,128)(2,1)S(1)}, u32[]{:S(2)}, u32[]{:S(2)}) collective-permute-start(bf16[8,2048]{1,0:T(8,128)(2,1)S(1)} %slice.28), channel_id=1, source_target_pairs={{0,4},{4,8},{8,12},{12,16},{16,20},{20,24},{24,28},{28,32},{32,36}... | collective-permute-start | bytes 98312 | tf_op jit(solution)/shard_map/ppermute | solution.py:28
  135.2 1.1 collective-permute-done.6.refs_4_
  136.3 2.0 %collective-permute-start.7 = (bf16[8,2048]{1,0:T(8,128)(2,1)S(1)}, bf16[8,2048]{1,0:T(8,128)(2,1)S(1)}, u32[]{:S(2)}, u32[]{:S(2)}) collective-permute-start(bf16[8,2048]{1,0:T(8,128)(2,1)S(1)} %collective-permute-done.6.refs_4_), channel_id=1, source_target_pairs={{0,1},{1,2},{2,3},{3,0},{4,5},{5,6},{6,7},{7,4},{8,9},{9,10},{10,1... | collective-permute-start | bytes 98312 | tf_op jit(solution)/shard_map/ppermute | solution.py:23
  138.3 0.0 collective-permute-start.8
  138.3 3.9 %collective-permute-done.7.refs_5_ = bf16[8,2048]{1,0:T(8,128)(2,1)S(1)} collective-permute-done((bf16[8,2048]{1,0:T(8,128)(2,1)S(1)}, bf16[8,2048]{1,0:T(8,128)(2,1)S(1)}, u32[]{:S(2)}, u32[]{:S(2)}) %collective-permute-start.7) | collective-permute-done | bytes 32800 | tf_op jit(solution)/shard_map/ppermute | solution.py:23
  142.3 0.0 collective-permute-start.9
  142.3 0.4 collective-permute-done.8.refs_6_
  142.7 2.8 %collective-permute-done.9.refs_7_ = bf16[8,2048]{1,0:T(8,128)(2,1)S(1)} collective-permute-done((bf16[8,2048]{1,0:T(8,128)(2,1)S(1)}, bf16[8,2048]{1,0:T(8,128)(2,1)S(1)}, u32[]{:S(2)}, u32[]{:S(2)}) %collective-permute-start.9) | collective-permute-done | bytes 32800 | tf_op jit(solution)/shard_map/ppermute | solution.py:23
  145.4 0.0 collective-permute-done.3.refs_1_
  145.4 0.0 collective-permute-done.4.refs_2_
  145.4 0.0 collective-permute-done.5.refs_3_
  145.4 5.6 %all-gather.3.cloned.1.call-done.refs_14_ = bf16[2048,4224]{1,0:T(8,128)(2,1)} async-done(((bf16[64,4224]{1,0:T(8,128)(2,1)}), bf16[2048,4224]{1,0:T(8,128)(2,1)}) %all-gather.3.cloned.1.call-update) | async-done | bytes 17301520 | tf_op jit(solution)/shard_map/all_gather | solution.py:320
  151.1 0.0 copy-done
  151.1 8.8 %feed_forward.1 = bf16[4,64,2048]{2,1,0:T(8,128)(2,1)S(1)} custom-call(s32[1]{0:T(128)} %bitcast.12.own_ref, bf16[64,2048]{1,0:T(8,128)(2,1)S(1)} %multiply_convert_fusion.1.refs_0_, bf16[64,2048]{1,0:T(8,128)(2,1)S(1)} %collective-permute-done.3.refs_1_, bf16[64,2048]{1,0:T(8,128)(2,1)S(1)} %collective-permute-done.4.refs_2_, ...), custom_call_target="tpu_custom_call" | custom-call | tf_op jit(solution)/shard_map/feed_forward/pallas_call | solution.py:276
  159.8 18.7 %all_to_all.5 = bf16[4,64,2048]{2,1,0:T(8,128)(2,1)S(1)} all-to-all(bf16[4,64,2048]{2,1,0:T(8,128)(2,1)S(1)} %feed_forward.1), channel_id=1, replica_groups=mesh['grp'=2,'sp'=32,'tp'=4] {'tp'}, dimensions={0} | all-to-all | bytes 2097152 | tf_op jit(solution)/shard_map/all_to_all | solution.py:364
  178.6 0.2 convert_reduce_fusion
  178.8 0.8 fusion.3
  (25 shorter events, 0.2 us)
Async XLA Ops:
  6.5 4.6 %copy-start.11 = (bf16[4,64,64]{2,1,0:T(8,128)(2,1)S(1)}, bf16[4,64,64]{2,1,0:T(8,128)(2,1)}, u32[]{:S(2)}) copy-start(bf16[4,64,64]{2,1,0:T(8,128)(2,1)} %param.18) | copy-start | bytes 98308
  6.5 4.6 %copy-start.10 = (bf16[4,64,64]{2,1,0:T(8,128)(2,1)S(1)}, bf16[4,64,64]{2,1,0:T(8,128)(2,1)}, u32[]{:S(2)}) copy-start(bf16[4,64,64]{2,1,0:T(8,128)(2,1)} %param.20) | copy-start | bytes 98308
  6.6 4.3 %copy-start.12 = (bf16[4,64,128]{2,1,0:T(8,128)(2,1)S(1)}, bf16[4,64,128]{2,1,0:T(8,128)(2,1)}, u32[]{:S(2)}) copy-start(bf16[4,64,128]{2,1,0:T(8,128)(2,1)} %param.21) | copy-start | bytes 196612
  6.6 144.5 %all-gather.3.cloned.1.call-start = ((), (), s32[]{:S(2)}) async-start(), calls=%async_computation.1 | async-start | bytes 17842176 | tf_op jit(solution)/shard_map/all_gather | solution.py:320
  97.5 0.7 copy-start.2
  97.5 1.6 copy-start.3
  97.5 1.6 copy-start.5
  97.5 1.6 copy-start.6
  97.5 1.6 copy-start.7
  97.5 1.6 copy-start.8
  102.5 20.4 %collective-permute-start.1 = (bf16[64,2048]{1,0:T(8,128)(2,1)S(1)}, bf16[64,2048]{1,0:T(8,128)(2,1)}, u32[]{:S(2)}, u32[]{:S(2)}) collective-permute-start(bf16[64,2048]{1,0:T(8,128)(2,1)S(1)} %get-tuple-element.13._), channel_id=1, source_target_pairs={{0,2},{1,3},{2,0},{3,1},{4,6},{5,7},{6,4},{7,5},{8,10},{9,11},{10,... | collective-permute-start | bytes 786440 | tf_op jit(solution)/shard_map/ppermute | solution.py:23
  109.6 13.3 %collective-permute-start = (bf16[64,2048]{1,0:T(8,128)(2,1)S(1)}, bf16[64,2048]{1,0:T(8,128)(2,1)}, u32[]{:S(2)}, u32[]{:S(2)}) collective-permute-start(bf16[64,2048]{1,0:T(8,128)(2,1)S(1)} %get-tuple-element.14._), channel_id=1, source_target_pairs={{0,1},{1,2},{2,3},{3,0},{4,5},{5,6},{6,7},{7,4},{8,9},{9,10},{10,1... | collective-permute-start | bytes 786440 | tf_op jit(solution)/shard_map/ppermute | solution.py:23
  110.2 1.7 copy-start.4
  115.3 7.6 %collective-permute-start.2 = (bf16[64,2048]{1,0:T(8,128)(2,1)S(1)}, bf16[64,2048]{1,0:T(8,128)(2,1)S(1)}, u32[]{:S(2)}, u32[]{:S(2)}) collective-permute-start(bf16[64,2048]{1,0:T(8,128)(2,1)S(1)} %get-tuple-element.15._), channel_id=1, source_target_pairs={{0,3},{1,0},{2,1},{3,2},{4,7},{5,4},{6,5},{7,6},{8,11},{9,8},{10,9... | collective-permute-start | bytes 786440 | tf_op jit(solution)/shard_map/ppermute | solution.py:23
  117.6 5.2 %copy-start.9 = (bf16[1,64,2048]{2,1,0:T(8,128)(2,1)S(1)}, bf16[1,64,2048]{2,1,0:T(8,128)(2,1)}, u32[]{:S(2)}) copy-start(bf16[1,64,2048]{2,1,0:T(8,128)(2,1)} %param.16) | copy-start | bytes 786436
  117.6 6.6 %copy-start.13 = (f32[2048]{0:T(1024)S(1)}, f32[2048]{0:T(1024)}, u32[]{:S(2)}) copy-start(f32[2048]{0:T(1024)} %param.26) | copy-start | bytes 24580
  121.0 30.1 %copy-start = (f32[3,1408]{1,0:T(4,128)S(1)}, f32[3,1408]{1,0:T(4,128)}, u32[]{:S(2)}) copy-start(f32[3,1408]{1,0:T(4,128)} %refs_12_.1) | copy-start | bytes 50692
  121.0 30.1 %copy-start.1 = (f32[3,1408]{1,0:T(4,128)S(1)}, f32[3,1408]{1,0:T(4,128)}, u32[]{:S(2)}) copy-start(f32[3,1408]{1,0:T(4,128)} %refs_13_.1) | copy-start | bytes 50692
  124.4 21.1 %collective-permute-start.3 = (bf16[64,2048]{1,0:T(8,128)(2,1)S(1)}, bf16[64,2048]{1,0:T(8,128)(2,1)S(1)}, u32[]{:S(2)}, u32[]{:S(2)}) collective-permute-start(bf16[64,2048]{1,0:T(8,128)(2,1)S(1)} %multiply_convert_fusion.1.refs_0_), channel_id=1, source_target_pairs={{0,1},{1,2},{2,3},{3,0},{4,5},{5,6},{6,7},{7,4},{8,9},{9,10},{10,1... | collective-permute-start | bytes 786440 | tf_op jit(solution)/shard_map/ppermute | solution.py:23
  124.7 20.7 %collective-permute-start.4 = (bf16[64,2048]{1,0:T(8,128)(2,1)S(1)}, bf16[64,2048]{1,0:T(8,128)(2,1)S(1)}, u32[]{:S(2)}, u32[]{:S(2)}) collective-permute-start(bf16[64,2048]{1,0:T(8,128)(2,1)S(1)} %multiply_convert_fusion.1.refs_0_), channel_id=1, source_target_pairs={{0,2},{1,3},{2,0},{3,1},{4,6},{5,7},{6,4},{7,5},{8,10},{9,11},{10,... | collective-permute-start | bytes 786440 | tf_op jit(solution)/shard_map/ppermute | solution.py:23
  129.0 16.5 %collective-permute-start.5 = (bf16[64,2048]{1,0:T(8,128)(2,1)S(1)}, bf16[64,2048]{1,0:T(8,128)(2,1)S(1)}, u32[]{:S(2)}, u32[]{:S(2)}) collective-permute-start(bf16[64,2048]{1,0:T(8,128)(2,1)S(1)} %multiply_convert_fusion.1.refs_0_), channel_id=1, source_target_pairs={{0,3},{1,0},{2,1},{3,2},{4,7},{5,4},{6,5},{7,6},{8,11},{9,8},{10,9... | collective-permute-start | bytes 786440 | tf_op jit(solution)/shard_map/ppermute | solution.py:23
  129.0 7.4 %collective-permute-start.6 = (bf16[8,2048]{1,0:T(8,128)(2,1)S(1)}, bf16[8,2048]{1,0:T(8,128)(2,1)S(1)}, u32[]{:S(2)}, u32[]{:S(2)}) collective-permute-start(bf16[8,2048]{1,0:T(8,128)(2,1)S(1)} %slice.28), channel_id=1, source_target_pairs={{0,4},{4,8},{8,12},{12,16},{16,20},{20,24},{24,28},{28,32},{32,36}... | collective-permute-start | bytes 98312 | tf_op jit(solution)/shard_map/ppermute | solution.py:28
  136.3 5.9 %collective-permute-start.7 = (bf16[8,2048]{1,0:T(8,128)(2,1)S(1)}, bf16[8,2048]{1,0:T(8,128)(2,1)S(1)}, u32[]{:S(2)}, u32[]{:S(2)}) collective-permute-start(bf16[8,2048]{1,0:T(8,128)(2,1)S(1)} %collective-permute-done.6.refs_4_), channel_id=1, source_target_pairs={{0,1},{1,2},{2,3},{3,0},{4,5},{5,6},{6,7},{7,4},{8,9},{9,10},{10,1... | collective-permute-start | bytes 98312 | tf_op jit(solution)/shard_map/ppermute | solution.py:23
  138.3 4.3 %collective-permute-start.8 = (bf16[8,2048]{1,0:T(8,128)(2,1)S(1)}, bf16[8,2048]{1,0:T(8,128)(2,1)S(1)}, u32[]{:S(2)}, u32[]{:S(2)}) collective-permute-start(bf16[8,2048]{1,0:T(8,128)(2,1)S(1)} %collective-permute-done.6.refs_4_), channel_id=1, source_target_pairs={{0,2},{1,3},{2,0},{3,1},{4,6},{5,7},{6,4},{7,5},{8,10},{9,11},{10,... | collective-permute-start | bytes 98312 | tf_op jit(solution)/shard_map/ppermute | solution.py:23
  142.3 3.2 %collective-permute-start.9 = (bf16[8,2048]{1,0:T(8,128)(2,1)S(1)}, bf16[8,2048]{1,0:T(8,128)(2,1)S(1)}, u32[]{:S(2)}, u32[]{:S(2)}) collective-permute-start(bf16[8,2048]{1,0:T(8,128)(2,1)S(1)} %collective-permute-done.6.refs_4_), channel_id=1, source_target_pairs={{0,3},{1,0},{2,1},{3,2},{4,7},{5,4},{6,5},{7,6},{8,11},{9,8},{10,9... | collective-permute-start | bytes 98312 | tf_op jit(solution)/shard_map/ppermute | solution.py:23
Sparse Core Ops, SparseCore 0:
  9.2 141.8 all-gather.2

commit v7 on v5

--- a/solution.py
+++ b/solution.py
@@ -6,6 +6,7 @@
 from jax.experimental import pallas as pl
 from jax.experimental.pallas import tpu as pltpu
 from jax.sharding import PartitionSpec as P
+
 
 NORM_EPS = 1e-06
 ROPE_BASE = 500000.0
@@ -314,7 +315,6 @@
     ranks = lax.axis_size("sp")
     own = lax.axis_index("tp")
     parts = lax.axis_size("tp")
-    model = resid_in.shape[2]
 
     packed = jnp.concatenate([gate_weight, value_weight, down_weight.T], axis=1)
     weights = lax.all_gather(packed, "sp", axis=0, tiled=True)
@@ -356,12 +356,15 @@
     meansq = jnp.mean(mid * mid, axis=-1, keepdims=True)
     normed = (mid * lax.rsqrt(meansq + NORM_EPS) * norm_gain).astype(jnp.bfloat16)
     edge = from_behind(normed[rows - EDGE :], "sp")
-    blocks = [normed] + [shifted(normed, "tp", k) for k in range(1, parts)]
-    edges = [edge] + [shifted(edge, "tp", k) for k in range(1, parts)]
+    blocks, edges = [normed] * parts, [edge] * parts
+    for k in farthest_first[:-1]:
+        blocks[k] = shifted(normed, "tp", k)
+        edges[k] = shifted(edge, "tp", k)
     partial = feed_forward(blocks, edges, same, weights, conv_gate, conv_value)
     out = mid + partial[0].astype(jnp.float32)
-    for k in range(1, parts):
-        out = out + shifted(partial[k], "tp", -k).astype(jnp.float32)
+    for k in farthest_first[:-1]:
+        returned = shifted(partial[k], "tp", -k)
+        out = out + returned.astype(jnp.float32)
     return out.astype(jnp.bfloat16)[None]
 
 
@@ -384,6 +387,7 @@
         P(None, "tp"),
         P("tp", "sp"),
     )
+
     return jax.shard_map(
         per_device,
         mesh=mesh,

time: 186 us -> 183 us (0.984)
  waiting for transfers between devices: 30.1 us -> 26.7 us
    ppermute x12, waiting for transfers between devices: 23.3 us -> 19.9 us  [shifted(): lax.ppermute(array, axis, [(i, (i + by) % length) for i in range(length)])]
  transfers between devices with their start and end apart: 14 -> 14, of which waited for: 8 -> 9; matrix products, arithmetic and copies ran while one was open for 3% -> 3% of each run, Pallas kernels for 7% -> 7%
where the time goes in v7:
time: 183 us
  blocking collectives  86.1 us (47%)
  waiting for transfers between devices  26.7 us (15%)
  starting transfers between devices  24.2 us (13%)
  Pallas kernels  22 us (12%)
  between operations  13.7 us (7%)
  other arithmetic  7.07 us (4%)
  local copies, waits for them, and re-layouts  3.25 us (2%)
    all_gather x1, blocking collectives, per_device(): everyone = lax.all_gather(sent, 'sp', axis=0, tiled=False)  86.1 us
    ppermute x12, waiting for transfers between devices, shifted(): lax.ppermute(array, axis, [(i, (i + by) % length) for i in range(length)])  19.9 us
    ppermute x12, starting transfers between devices, shifted(): lax.ppermute(array, axis, [(i, (i + by) % length) for i in range(length)])  17.9 us
    pallas_call x4, Pallas kernels, attend(): pl.pallas_call(body, out_shape=(jax.ShapeDtypeStruct((rows, model), jnp.b...  13.3 us
    pallas_call x1, Pallas kernels, feed_forward(): pl.pallas_call(body, out_shape=[jax.ShapeDtypeStruct((rows, width), jnp.b...  8.75 us
    ppermute x1, starting transfers between devices, from_behind(): return lax.ppermute(array, axis, [(i, i + 1) for i in range(length - 1)])  6.32 us
    all_gather x1, waiting for transfers between devices, per_device(): weights = lax.all_gather(packed, 'sp', axis=0, tiled=True)  5.65 us
  transfers between devices with their start and end apart: 14, of which 9 were waited for; matrix products, arithmetic and copies ran while one was open for 3% of the time, Pallas kernels for 7%

profile of v7, /device:TPU:33, one launch (start us, length us, event | category | flops | bytes accessed | tf_op | source)
XLA Modules:
  0.0 183.1 jit_solution(13449219267185245277)
XLA Ops:
  6.6 0.0 all-gather.3.cloned.1.call-start
  6.6 2.0 %pad_maximum_fusion = bf16[64,4224]{1,0:T(8,128)(2,1)} fusion(bf16[64,1408]{1,0:T(8,128)(2,1)} %bitcast.26, bf16[64,1408]{1,0:T(8,128)(2,1)} %param.28, bf16[64,1408]{1,0:T(8,128)(2,1)} %param.27), kind=kLoop, calls=%fused_computation.1 | loop fusion | flops 1622016 | bytes 1081344 | tf_op jit(solution)/shard_map/concatenate | solution.py:319
  8.5 0.1 all-gather.3.cloned.1.call-update
  8.7 0.1 multiply_cosine_fusion
  8.8 0.1 copy.27.c_ref
  8.9 0.1 copy.28.s_ref
  9.0 0.7 multiply_convert_fusion.4
  9.7 0.1 tile.33
  9.8 0.1 add_add_fusion.2
  9.9 1.0 maximum_convert_fusion
  10.8 0.0 copy-done.12
  10.9 0.1 fusion.10
  11.0 0.1 fusion.11
  11.1 0.0 copy-done.11
  11.1 0.0 copy-done.10
  11.1 0.2 multiply_convert_fusion.3
  11.4 86.1 %all-gather.4 = f16[32,264,256]{2,1,0:T(8,128)(2,1)S(1)} all-gather(f16[1,264,256]{2,1,0:T(8,128)(2,1)S(1)} %pad_maximum_fusion.1), channel_id=1, replica_groups=mesh['grp'=2,'sp'=32,'tp'=4] {'sp'}, dimensions={0}, use_global_device_ids=true | all-gather | bytes 4460544 | tf_op jit(solution)/shard_map/all_gather | solution.py:334
  97.5 0.0 copy-start.7
  97.5 0.0 copy-start.8
  97.5 0.5 multiply_convert_fusion.w_ref
  98.1 0.1 copy-done.2
  98.2 1.0 copy-done.3
  99.1 0.0 copy-done.5
  99.1 0.0 copy-done.8
  99.1 3.3 %attend.4 = (bf16[64,2048]{1,0:T(8,128)(2,1)S(1)}, f32[64,128]{1,0:T(8,128)S(1)}) custom-call(s32[3]{0:T(128)S(1)} %get-tuple-element.41.place_ref, f32[8]{0:T(128)S(1)} %copy-done.7, bf16[4,64,256]{2,1,0:T(8,128)(2,1)S(1)} %copy-done.5, bf16[4,64,256]{2,1,0:T(8,128)(2,1)S(1)} %copy-done.6, bf16[18,264,256]{2,1,0:T(8,128)(2,1)S(1)} %multiply_convert_fusion.w_ref, ...), custom_call_target="tpu_custom_call" | custom-call | flops 3000000000 | bytes 4000000 | tf_op jit(solution)/shard_map/attend/pallas_call | solution.py:169
  102.5 3.7 %collective-permute-start.1 = (bf16[64,2048]{1,0:T(8,128)(2,1)S(1)}, bf16[64,2048]{1,0:T(8,128)(2,1)}, u32[]{:S(2)}, u32[]{:S(2)}) collective-permute-start(bf16[64,2048]{1,0:T(8,128)(2,1)S(1)} %get-tuple-element.17._), channel_id=1, source_target_pairs={{0,2},{1,3},{2,0},{3,1},{4,6},{5,7},{6,4},{7,5},{8,10},{9,11},{10,... | collective-permute-start | bytes 786440 | tf_op jit(solution)/shard_map/ppermute | solution.py:24
  106.2 3.3 %attend.5 = (bf16[64,2048]{1,0:T(8,128)(2,1)S(1)}, f32[64,128]{1,0:T(8,128)S(1)}) custom-call(s32[3]{0:T(128)S(1)} %get-tuple-element.40.place_ref, f32[8]{0:T(128)S(1)} %copy-done.7, bf16[4,64,256]{2,1,0:T(8,128)(2,1)S(1)} %copy-done.5, bf16[4,64,256]{2,1,0:T(8,128)(2,1)S(1)} %copy-done.6, bf16[18,264,256]{2,1,0:T(8,128)(2,1)S(1)} %multiply_convert_fusion.w_ref, ...), custom_call_target="tpu_custom_call" | custom-call | flops 3000000000 | bytes 4000000 | tf_op jit(solution)/shard_map/attend/pallas_call | solution.py:169
  109.5 0.7 collective-permute-start
  110.2 0.1 add_add_fusion
  110.3 1.7 copy-done.4
  111.9 3.3 %attend.6 = (bf16[64,2048]{1,0:T(8,128)(2,1)S(1)}, f32[64,128]{1,0:T(8,128)S(1)}) custom-call(s32[3]{0:T(128)S(1)} %get-tuple-element.39.place_ref, f32[8]{0:T(128)S(1)} %copy-done.7, bf16[4,64,256]{2,1,0:T(8,128)(2,1)S(1)} %copy-done.5, bf16[4,64,256]{2,1,0:T(8,128)(2,1)S(1)} %copy-done.6, bf16[18,264,256]{2,1,0:T(8,128)(2,1)S(1)} %multiply_convert_fusion.w_ref, ...), custom_call_target="tpu_custom_call" | custom-call | flops 3000000000 | bytes 4000000 | tf_op jit(solution)/shard_map/attend/pallas_call | solution.py:169
  115.3 2.3 %collective-permute-start.2 = (bf16[64,2048]{1,0:T(8,128)(2,1)S(1)}, bf16[64,2048]{1,0:T(8,128)(2,1)S(1)}, u32[]{:S(2)}, u32[]{:S(2)}) collective-permute-start(bf16[64,2048]{1,0:T(8,128)(2,1)S(1)} %get-tuple-element.19._), channel_id=1, source_target_pairs={{0,3},{1,0},{2,1},{3,2},{4,7},{5,4},{6,5},{7,6},{8,11},{9,8},{10,9... | collective-permute-start | bytes 786440 | tf_op jit(solution)/shard_map/ppermute | solution.py:24
  117.6 3.3 %attend.7 = (bf16[64,2048]{1,0:T(8,128)(2,1)S(1)}, f32[64,128]{1,0:T(8,128)S(1)}) custom-call(s32[3]{0:T(128)S(1)} %get-tuple-element.38.place_ref, f32[8]{0:T(128)S(1)} %copy-done.7, bf16[4,64,256]{2,1,0:T(8,128)(2,1)S(1)} %copy-done.5, bf16[4,64,256]{2,1,0:T(8,128)(2,1)S(1)} %copy-done.6, bf16[18,264,256]{2,1,0:T(8,128)(2,1)S(1)} %multiply_convert_fusion.w_ref, ...), custom_call_target="tpu_custom_call" | custom-call | flops 3000000000 | bytes 4000000 | tf_op jit(solution)/shard_map/attend/pallas_call | solution.py:169
  120.9 0.0 copy-start
  120.9 0.0 copy-start.1
  120.9 1.9 %collective-permute-done.2 = bf16[64,2048]{1,0:T(8,128)(2,1)S(1)} collective-permute-done((bf16[64,2048]{1,0:T(8,128)(2,1)S(1)}, bf16[64,2048]{1,0:T(8,128)(2,1)S(1)}, u32[]{:S(2)}, u32[]{:S(2)}) %collective-permute-start.2) | collective-permute-done | bytes 262176 | tf_op jit(solution)/shard_map/ppermute | solution.py:24
  122.9 0.0 collective-permute-done
  122.9 0.0 collective-permute-done.1
  122.9 1.3 multiply_reduce_fusion
  124.2 0.1 multiply_convert_fusion.1.refs_0_
  124.4 0.4 collective-permute-start.3
  124.7 4.2 %collective-permute-start.4 = (bf16[64,2048]{1,0:T(8,128)(2,1)S(1)}, bf16[64,2048]{1,0:T(8,128)(2,1)S(1)}, u32[]{:S(2)}, u32[]{:S(2)}) collective-permute-start(bf16[64,2048]{1,0:T(8,128)(2,1)S(1)} %multiply_convert_fusion.1.refs_0_), channel_id=1, source_target_pairs={{0,2},{1,3},{2,0},{3,1},{4,6},{5,7},{6,4},{7,5},{8,10},{9,11},{10,... | collective-permute-start | bytes 786440 | tf_op jit(solution)/shard_map/ppermute | solution.py:24
  128.9 0.0 collective-permute-start.5
  128.9 6.3 %collective-permute-start.6 = (bf16[8,2048]{1,0:T(8,128)(2,1)S(1)}, bf16[8,2048]{1,0:T(8,128)(2,1)S(1)}, u32[]{:S(2)}, u32[]{:S(2)}) collective-permute-start(bf16[8,2048]{1,0:T(8,128)(2,1)S(1)} %slice.28), channel_id=1, source_target_pairs={{0,4},{4,8},{8,12},{12,16},{16,20},{20,24},{24,28},{28,32},{32,36}... | collective-permute-start | bytes 98312 | tf_op jit(solution)/shard_map/ppermute | solution.py:29
  135.2 1.1 collective-permute-done.6.refs_4_
  136.4 2.0 %collective-permute-start.7 = (bf16[8,2048]{1,0:T(8,128)(2,1)S(1)}, bf16[8,2048]{1,0:T(8,128)(2,1)S(1)}, u32[]{:S(2)}, u32[]{:S(2)}) collective-permute-start(bf16[8,2048]{1,0:T(8,128)(2,1)S(1)} %collective-permute-done.6.refs_4_), channel_id=1, source_target_pairs={{0,1},{1,2},{2,3},{3,0},{4,5},{5,6},{6,7},{7,4},{8,9},{9,10},{10,1... | collective-permute-start | bytes 98312 | tf_op jit(solution)/shard_map/ppermute | solution.py:24
  138.3 0.0 collective-permute-start.8
  138.3 3.9 %collective-permute-done.7.refs_5_ = bf16[8,2048]{1,0:T(8,128)(2,1)S(1)} collective-permute-done((bf16[8,2048]{1,0:T(8,128)(2,1)S(1)}, bf16[8,2048]{1,0:T(8,128)(2,1)S(1)}, u32[]{:S(2)}, u32[]{:S(2)}) %collective-permute-start.7) | collective-permute-done | bytes 32800 | tf_op jit(solution)/shard_map/ppermute | solution.py:24
  142.2 0.0 collective-permute-start.9
  142.2 0.4 collective-permute-done.8.refs_6_
  142.7 2.7 %collective-permute-done.9.refs_7_ = bf16[8,2048]{1,0:T(8,128)(2,1)S(1)} collective-permute-done((bf16[8,2048]{1,0:T(8,128)(2,1)S(1)}, bf16[8,2048]{1,0:T(8,128)(2,1)S(1)}, u32[]{:S(2)}, u32[]{:S(2)}) %collective-permute-start.9) | collective-permute-done | bytes 32800 | tf_op jit(solution)/shard_map/ppermute | solution.py:24
  145.4 0.0 collective-permute-done.3.refs_1_
  145.4 0.0 collective-permute-done.4.refs_2_
  145.4 0.0 collective-permute-done.5.refs_3_
  145.4 5.6 %all-gather.3.cloned.1.call-done.refs_14_ = bf16[2048,4224]{1,0:T(8,128)(2,1)} async-done(((bf16[64,4224]{1,0:T(8,128)(2,1)}), bf16[2048,4224]{1,0:T(8,128)(2,1)}) %all-gather.3.cloned.1.call-update) | async-done | bytes 17301520 | tf_op jit(solution)/shard_map/all_gather | solution.py:320
  151.1 0.0 copy-done
  151.1 8.8 %feed_forward.1 = (bf16[64,2048]{1,0:T(8,128)(2,1)S(1)}, bf16[64,2048]{1,0:T(8,128)(2,1)S(1)}, bf16[64,2048]{1,0:T(8,128)(2,1)S(1)}, bf16[64,2048]{1,0:T(8,128)(2,1)S(1)}) custom-call(bf16[64,2048]{1,0:T(8,128)(2,1)S(1)} %multiply_convert_fusion.1.refs_0_, bf16[64,2048]{1,0:T(8,128)(2,1)S(1)} %collective-permute-done.3.refs_1_, ...), custom_call_target="tpu_custom_call" | custom-call | tf_op jit(solution)/shard_map/feed_forward/pallas_call | solution.py:277
  159.8 3.1 %collective-permute-start.10 = (bf16[64,2048]{1,0:T(8,128)(2,1)S(1)}, bf16[64,2048]{1,0:T(8,128)(2,1)S(1)}, u32[]{:S(2)}, u32[]{:S(2)}) collective-permute-start(bf16[64,2048]{1,0:T(8,128)(2,1)S(1)} %get-tuple-element.26), channel_id=1, source_target_pairs={{0,2},{1,3},{2,0},{3,1},{4,6},{5,7},{6,4},{7,5},{8,10},{9,11},{10,... | collective-permute-start | bytes 786440 | tf_op jit(solution)/shard_map/ppermute | solution.py:24
  163.0 0.7 collective-permute-start.11
  163.7 0.7 collective-permute-start.12
  164.4 4.8 %collective-permute-done.10 = bf16[64,2048]{1,0:T(8,128)(2,1)S(1)} collective-permute-done((bf16[64,2048]{1,0:T(8,128)(2,1)S(1)}, bf16[64,2048]{1,0:T(8,128)(2,1)S(1)}, u32[]{:S(2)}, u32[]{:S(2)}) %collective-permute-start.10) | collective-permute-done | bytes 262176 | tf_op jit(solution)/shard_map/ppermute | solution.py:24
  169.2 6.0 %collective-permute-done.11 = bf16[64,2048]{1,0:T(8,128)(2,1)S(1)} collective-permute-done((bf16[64,2048]{1,0:T(8,128)(2,1)S(1)}, bf16[64,2048]{1,0:T(8,128)(2,1)S(1)}, u32[]{:S(2)}, u32[]{:S(2)}) %collective-permute-start.11) | collective-permute-done | bytes 262176 | tf_op jit(solution)/shard_map/ppermute | solution.py:24
  175.2 0.2 collective-permute-done.12
  175.4 0.9 fusion.3
  (29 shorter events, 0.2 us)
Async XLA Ops:
  6.5 4.5 %copy-start.11 = (bf16[4,64,64]{2,1,0:T(8,128)(2,1)S(1)}, bf16[4,64,64]{2,1,0:T(8,128)(2,1)}, u32[]{:S(2)}) copy-start(bf16[4,64,64]{2,1,0:T(8,128)(2,1)} %param.18) | copy-start | bytes 98308
  6.5 4.6 %copy-start.10 = (bf16[4,64,64]{2,1,0:T(8,128)(2,1)S(1)}, bf16[4,64,64]{2,1,0:T(8,128)(2,1)}, u32[]{:S(2)}) copy-start(bf16[4,64,64]{2,1,0:T(8,128)(2,1)} %param.20) | copy-start | bytes 98308
  6.6 4.3 %copy-start.12 = (bf16[4,64,128]{2,1,0:T(8,128)(2,1)S(1)}, bf16[4,64,128]{2,1,0:T(8,128)(2,1)}, u32[]{:S(2)}) copy-start(bf16[4,64,128]{2,1,0:T(8,128)(2,1)} %param.21) | copy-start | bytes 196612
  6.6 144.5 %all-gather.3.cloned.1.call-start = ((), (), s32[]{:S(2)}) async-start(), calls=%async_computation | async-start | bytes 17842176 | tf_op jit(solution)/shard_map/all_gather | solution.py:320
  97.5 0.7 copy-start.2
  97.5 1.6 copy-start.3
  97.5 1.6 copy-start.5
  97.5 1.6 copy-start.6
  97.5 1.6 copy-start.7
  97.5 1.6 copy-start.8
  102.5 20.4 %collective-permute-start.1 = (bf16[64,2048]{1,0:T(8,128)(2,1)S(1)}, bf16[64,2048]{1,0:T(8,128)(2,1)}, u32[]{:S(2)}, u32[]{:S(2)}) collective-permute-start(bf16[64,2048]{1,0:T(8,128)(2,1)S(1)} %get-tuple-element.17._), channel_id=1, source_target_pairs={{0,2},{1,3},{2,0},{3,1},{4,6},{5,7},{6,4},{7,5},{8,10},{9,11},{10,... | collective-permute-start | bytes 786440 | tf_op jit(solution)/shard_map/ppermute | solution.py:24
  109.5 13.3 %collective-permute-start = (bf16[64,2048]{1,0:T(8,128)(2,1)S(1)}, bf16[64,2048]{1,0:T(8,128)(2,1)}, u32[]{:S(2)}, u32[]{:S(2)}) collective-permute-start(bf16[64,2048]{1,0:T(8,128)(2,1)S(1)} %get-tuple-element.18._), channel_id=1, source_target_pairs={{0,1},{1,2},{2,3},{3,0},{4,5},{5,6},{6,7},{7,4},{8,9},{9,10},{10,1... | collective-permute-start | bytes 786440 | tf_op jit(solution)/shard_map/ppermute | solution.py:24
  110.2 1.7 copy-start.4
  115.3 7.6 %collective-permute-start.2 = (bf16[64,2048]{1,0:T(8,128)(2,1)S(1)}, bf16[64,2048]{1,0:T(8,128)(2,1)S(1)}, u32[]{:S(2)}, u32[]{:S(2)}) collective-permute-start(bf16[64,2048]{1,0:T(8,128)(2,1)S(1)} %get-tuple-element.19._), channel_id=1, source_target_pairs={{0,3},{1,0},{2,1},{3,2},{4,7},{5,4},{6,5},{7,6},{8,11},{9,8},{10,9... | collective-permute-start | bytes 786440 | tf_op jit(solution)/shard_map/ppermute | solution.py:24
  117.6 5.3 %copy-start.9 = (bf16[1,64,2048]{2,1,0:T(8,128)(2,1)S(1)}, bf16[1,64,2048]{2,1,0:T(8,128)(2,1)}, u32[]{:S(2)}) copy-start(bf16[1,64,2048]{2,1,0:T(8,128)(2,1)} %param.16) | copy-start | bytes 786436
  117.6 6.6 %copy-start.13 = (f32[2048]{0:T(1024)S(1)}, f32[2048]{0:T(1024)}, u32[]{:S(2)}) copy-start(f32[2048]{0:T(1024)} %param.26) | copy-start | bytes 24580
  120.9 30.1 %copy-start = (f32[3,1408]{1,0:T(4,128)S(1)}, f32[3,1408]{1,0:T(4,128)}, u32[]{:S(2)}) copy-start(f32[3,1408]{1,0:T(4,128)} %refs_12_.1) | copy-start | bytes 50692
  120.9 30.1 %copy-start.1 = (f32[3,1408]{1,0:T(4,128)S(1)}, f32[3,1408]{1,0:T(4,128)}, u32[]{:S(2)}) copy-start(f32[3,1408]{1,0:T(4,128)} %refs_13_.1) | copy-start | bytes 50692
  124.4 21.1 %collective-permute-start.3 = (bf16[64,2048]{1,0:T(8,128)(2,1)S(1)}, bf16[64,2048]{1,0:T(8,128)(2,1)S(1)}, u32[]{:S(2)}, u32[]{:S(2)}) collective-permute-start(bf16[64,2048]{1,0:T(8,128)(2,1)S(1)} %multiply_convert_fusion.1.refs_0_), channel_id=1, source_target_pairs={{0,1},{1,2},{2,3},{3,0},{4,5},{5,6},{6,7},{7,4},{8,9},{9,10},{10,1... | collective-permute-start | bytes 786440 | tf_op jit(solution)/shard_map/ppermute | solution.py:24
  124.7 20.7 %collective-permute-start.4 = (bf16[64,2048]{1,0:T(8,128)(2,1)S(1)}, bf16[64,2048]{1,0:T(8,128)(2,1)S(1)}, u32[]{:S(2)}, u32[]{:S(2)}) collective-permute-start(bf16[64,2048]{1,0:T(8,128)(2,1)S(1)} %multiply_convert_fusion.1.refs_0_), channel_id=1, source_target_pairs={{0,2},{1,3},{2,0},{3,1},{4,6},{5,7},{6,4},{7,5},{8,10},{9,11},{10,... | collective-permute-start | bytes 786440 | tf_op jit(solution)/shard_map/ppermute | solution.py:24
  128.9 16.5 %collective-permute-start.5 = (bf16[64,2048]{1,0:T(8,128)(2,1)S(1)}, bf16[64,2048]{1,0:T(8,128)(2,1)S(1)}, u32[]{:S(2)}, u32[]{:S(2)}) collective-permute-start(bf16[64,2048]{1,0:T(8,128)(2,1)S(1)} %multiply_convert_fusion.1.refs_0_), channel_id=1, source_target_pairs={{0,3},{1,0},{2,1},{3,2},{4,7},{5,4},{6,5},{7,6},{8,11},{9,8},{10,9... | collective-permute-start | bytes 786440 | tf_op jit(solution)/shard_map/ppermute | solution.py:24
  128.9 7.4 %collective-permute-start.6 = (bf16[8,2048]{1,0:T(8,128)(2,1)S(1)}, bf16[8,2048]{1,0:T(8,128)(2,1)S(1)}, u32[]{:S(2)}, u32[]{:S(2)}) collective-permute-start(bf16[8,2048]{1,0:T(8,128)(2,1)S(1)} %slice.28), channel_id=1, source_target_pairs={{0,4},{4,8},{8,12},{12,16},{16,20},{20,24},{24,28},{28,32},{32,36}... | collective-permute-start | bytes 98312 | tf_op jit(solution)/shard_map/ppermute | solution.py:29
  136.4 5.9 %collective-permute-start.7 = (bf16[8,2048]{1,0:T(8,128)(2,1)S(1)}, bf16[8,2048]{1,0:T(8,128)(2,1)S(1)}, u32[]{:S(2)}, u32[]{:S(2)}) collective-permute-start(bf16[8,2048]{1,0:T(8,128)(2,1)S(1)} %collective-permute-done.6.refs_4_), channel_id=1, source_target_pairs={{0,1},{1,2},{2,3},{3,0},{4,5},{5,6},{6,7},{7,4},{8,9},{9,10},{10,1... | collective-permute-start | bytes 98312 | tf_op jit(solution)/shard_map/ppermute | solution.py:24
  138.3 4.3 %collective-permute-start.8 = (bf16[8,2048]{1,0:T(8,128)(2,1)S(1)}, bf16[8,2048]{1,0:T(8,128)(2,1)S(1)}, u32[]{:S(2)}, u32[]{:S(2)}) collective-permute-start(bf16[8,2048]{1,0:T(8,128)(2,1)S(1)} %collective-permute-done.6.refs_4_), channel_id=1, source_target_pairs={{0,2},{1,3},{2,0},{3,1},{4,6},{5,7},{6,4},{7,5},{8,10},{9,11},{10,... | collective-permute-start | bytes 98312 | tf_op jit(solution)/shard_map/ppermute | solution.py:24
  142.2 3.2 %collective-permute-start.9 = (bf16[8,2048]{1,0:T(8,128)(2,1)S(1)}, bf16[8,2048]{1,0:T(8,128)(2,1)S(1)}, u32[]{:S(2)}, u32[]{:S(2)}) collective-permute-start(bf16[8,2048]{1,0:T(8,128)(2,1)S(1)} %collective-permute-done.6.refs_4_), channel_id=1, source_target_pairs={{0,3},{1,0},{2,1},{3,2},{4,7},{5,4},{6,5},{7,6},{8,11},{9,8},{10,9... | collective-permute-start | bytes 98312 | tf_op jit(solution)/shard_map/ppermute | solution.py:24
  159.8 9.4 %collective-permute-start.10 = (bf16[64,2048]{1,0:T(8,128)(2,1)S(1)}, bf16[64,2048]{1,0:T(8,128)(2,1)S(1)}, u32[]{:S(2)}, u32[]{:S(2)}) collective-permute-start(bf16[64,2048]{1,0:T(8,128)(2,1)S(1)} %get-tuple-element.26), channel_id=1, source_target_pairs={{0,2},{1,3},{2,0},{3,1},{4,6},{5,7},{6,4},{7,5},{8,10},{9,11},{10,... | collective-permute-start | bytes 786440 | tf_op jit(solution)/shard_map/ppermute | solution.py:24
  163.0 12.2 %collective-permute-start.11 = (bf16[64,2048]{1,0:T(8,128)(2,1)S(1)}, bf16[64,2048]{1,0:T(8,128)(2,1)S(1)}, u32[]{:S(2)}, u32[]{:S(2)}) collective-permute-start(bf16[64,2048]{1,0:T(8,128)(2,1)S(1)} %get-tuple-element.27), channel_id=1, source_target_pairs={{0,3},{1,0},{2,1},{3,2},{4,7},{5,4},{6,5},{7,6},{8,11},{9,8},{10,9... | collective-permute-start | bytes 786440 | tf_op jit(solution)/shard_map/ppermute | solution.py:24
  163.7 11.7 %collective-permute-start.12 = (bf16[64,2048]{1,0:T(8,128)(2,1)S(1)}, bf16[64,2048]{1,0:T(8,128)(2,1)S(1)}, u32[]{:S(2)}, u32[]{:S(2)}) collective-permute-start(bf16[64,2048]{1,0:T(8,128)(2,1)S(1)} %get-tuple-element.28), channel_id=1, source_target_pairs={{0,1},{1,2},{2,3},{3,0},{4,5},{5,6},{6,7},{7,4},{8,9},{9,10},{10,1... | collective-permute-start | bytes 786440 | tf_op jit(solution)/shard_map/ppermute | solution.py:24
Sparse Core Ops, SparseCore 0:
  9.2 141.8 all-gather.2

commit v8 on v5

--- a/solution.py
+++ b/solution.py
@@ -6,6 +6,7 @@
 from jax.experimental import pallas as pl
 from jax.experimental.pallas import tpu as pltpu
 from jax.sharding import PartitionSpec as P
+
 
 NORM_EPS = 1e-06
 ROPE_BASE = 500000.0
@@ -314,7 +315,6 @@
     ranks = lax.axis_size("sp")
     own = lax.axis_index("tp")
     parts = lax.axis_size("tp")
-    model = resid_in.shape[2]
 
     packed = jnp.concatenate([gate_weight, value_weight, down_weight.T], axis=1)
     weights = lax.all_gather(packed, "sp", axis=0, tiled=True)
@@ -360,8 +360,9 @@
     edges = [edge] + [shifted(edge, "tp", k) for k in range(1, parts)]
     partial = feed_forward(blocks, edges, same, weights, conv_gate, conv_value)
     out = mid + partial[0].astype(jnp.float32)
-    for k in range(1, parts):
-        out = out + shifted(partial[k], "tp", -k).astype(jnp.float32)
+    for k in sorted(farthest_first[:-1], key=lambda k: (-min(k, parts - k), -k)):
+        returned = shifted(partial[k], "tp", -k)
+        out = out + returned.astype(jnp.float32)
     return out.astype(jnp.bfloat16)[None]
 
 
@@ -384,6 +385,7 @@
         P(None, "tp"),
         P("tp", "sp"),
     )
+
     return jax.shard_map(
         per_device,
         mesh=mesh,

time: 186 us -> 183 us (0.984)
  waiting for transfers between devices: 30.1 us -> 25.5 us
    ppermute x12, waiting for transfers between devices: 23.3 us -> 18.7 us  [shifted(): lax.ppermute(array, axis, [(i, (i + by) % length) for i in range(length)])]
where the time goes in v8:
time: 183 us
  blocking collectives  86.1 us (47%)
  waiting for transfers between devices  25.5 us (14%)
  starting transfers between devices  25.4 us (14%)
  Pallas kernels  22 us (12%)
  between operations  13.7 us (7%)
  other arithmetic  7.07 us (4%)
  local copies, waits for them, and re-layouts  3.25 us (2%)
    all_gather x1, blocking collectives, per_device(): everyone = lax.all_gather(sent, 'sp', axis=0, tiled=False)  86.1 us
    ppermute x12, starting transfers between devices, shifted(): lax.ppermute(array, axis, [(i, (i + by) % length) for i in range(length)])  19.1 us
    ppermute x12, waiting for transfers between devices, shifted(): lax.ppermute(array, axis, [(i, (i + by) % length) for i in range(length)])  18.7 us
    pallas_call x4, Pallas kernels, attend(): pl.pallas_call(body, out_shape=(jax.ShapeDtypeStruct((rows, model), jnp.b...  13.3 us
    pallas_call x1, Pallas kernels, feed_forward(): pl.pallas_call(body, out_shape=[jax.ShapeDtypeStruct((rows, width), jnp.b...  8.75 us
    ppermute x1, starting transfers between devices, from_behind(): return lax.ppermute(array, axis, [(i, i + 1) for i in range(length - 1)])  6.32 us
    all_gather x1, waiting for transfers between devices, per_device(): weights = lax.all_gather(packed, 'sp', axis=0, tiled=True)  5.65 us
  transfers between devices with their start and end apart: 14, of which 8 were waited for; matrix products, arithmetic and copies ran while one was open for 3% of the time, Pallas kernels for 7%

profile of v8, /device:TPU:33, one launch (start us, length us, event | category | flops | bytes accessed | tf_op | source)
XLA Modules:
  0.0 183.1 jit_solution(2802490542824777844)
XLA Ops:
  6.6 0.0 all-gather.3.cloned.1.call-start
  6.6 2.0 %pad_maximum_fusion = bf16[64,4224]{1,0:T(8,128)(2,1)} fusion(bf16[64,1408]{1,0:T(8,128)(2,1)} %bitcast.26, bf16[64,1408]{1,0:T(8,128)(2,1)} %param.28, bf16[64,1408]{1,0:T(8,128)(2,1)} %param.27), kind=kLoop, calls=%fused_computation.1 | loop fusion | flops 1622016 | bytes 1081344 | tf_op jit(solution)/shard_map/concatenate | solution.py:319
  8.5 0.1 all-gather.3.cloned.1.call-update
  8.7 0.1 multiply_cosine_fusion
  8.8 0.1 copy.27.c_ref
  8.9 0.1 copy.28.s_ref
  9.0 0.7 multiply_convert_fusion.4
  9.7 0.1 tile.33
  9.8 0.1 add_add_fusion.2
  9.9 1.0 maximum_convert_fusion
  10.8 0.0 copy-done.12
  10.9 0.1 fusion.10
  11.0 0.1 fusion.11
  11.1 0.0 copy-done.11
  11.1 0.0 copy-done.10
  11.1 0.2 multiply_convert_fusion.3
  11.4 86.1 %all-gather.4 = f16[32,264,256]{2,1,0:T(8,128)(2,1)S(1)} all-gather(f16[1,264,256]{2,1,0:T(8,128)(2,1)S(1)} %pad_maximum_fusion.1), channel_id=1, replica_groups=mesh['grp'=2,'sp'=32,'tp'=4] {'sp'}, dimensions={0}, use_global_device_ids=true | all-gather | bytes 4460544 | tf_op jit(solution)/shard_map/all_gather | solution.py:334
  97.5 0.0 copy-start.7
  97.5 0.0 copy-start.8
  97.5 0.5 multiply_convert_fusion.w_ref
  98.1 0.1 copy-done.2
  98.2 1.0 copy-done.3
  99.1 0.0 copy-done.5
  99.1 0.0 copy-done.8
  99.1 3.3 %attend.4 = (bf16[64,2048]{1,0:T(8,128)(2,1)S(1)}, f32[64,128]{1,0:T(8,128)S(1)}) custom-call(s32[3]{0:T(128)S(1)} %get-tuple-element.41.place_ref, f32[8]{0:T(128)S(1)} %copy-done.7, bf16[4,64,256]{2,1,0:T(8,128)(2,1)S(1)} %copy-done.5, bf16[4,64,256]{2,1,0:T(8,128)(2,1)S(1)} %copy-done.6, bf16[18,264,256]{2,1,0:T(8,128)(2,1)S(1)} %multiply_convert_fusion.w_ref, ...), custom_call_target="tpu_custom_call" | custom-call | flops 3000000000 | bytes 4000000 | tf_op jit(solution)/shard_map/attend/pallas_call | solution.py:169
  102.5 3.7 %collective-permute-start.1 = (bf16[64,2048]{1,0:T(8,128)(2,1)S(1)}, bf16[64,2048]{1,0:T(8,128)(2,1)}, u32[]{:S(2)}, u32[]{:S(2)}) collective-permute-start(bf16[64,2048]{1,0:T(8,128)(2,1)S(1)} %get-tuple-element.17._), channel_id=1, source_target_pairs={{0,2},{1,3},{2,0},{3,1},{4,6},{5,7},{6,4},{7,5},{8,10},{9,11},{10,... | collective-permute-start | bytes 786440 | tf_op jit(solution)/shard_map/ppermute | solution.py:24
  106.2 3.3 %attend.5 = (bf16[64,2048]{1,0:T(8,128)(2,1)S(1)}, f32[64,128]{1,0:T(8,128)S(1)}) custom-call(s32[3]{0:T(128)S(1)} %get-tuple-element.40.place_ref, f32[8]{0:T(128)S(1)} %copy-done.7, bf16[4,64,256]{2,1,0:T(8,128)(2,1)S(1)} %copy-done.5, bf16[4,64,256]{2,1,0:T(8,128)(2,1)S(1)} %copy-done.6, bf16[18,264,256]{2,1,0:T(8,128)(2,1)S(1)} %multiply_convert_fusion.w_ref, ...), custom_call_target="tpu_custom_call" | custom-call | flops 3000000000 | bytes 4000000 | tf_op jit(solution)/shard_map/attend/pallas_call | solution.py:169
  109.5 0.7 collective-permute-start
  110.2 0.1 add_add_fusion
  110.3 1.7 copy-done.4
  111.9 3.3 %attend.6 = (bf16[64,2048]{1,0:T(8,128)(2,1)S(1)}, f32[64,128]{1,0:T(8,128)S(1)}) custom-call(s32[3]{0:T(128)S(1)} %get-tuple-element.39.place_ref, f32[8]{0:T(128)S(1)} %copy-done.7, bf16[4,64,256]{2,1,0:T(8,128)(2,1)S(1)} %copy-done.5, bf16[4,64,256]{2,1,0:T(8,128)(2,1)S(1)} %copy-done.6, bf16[18,264,256]{2,1,0:T(8,128)(2,1)S(1)} %multiply_convert_fusion.w_ref, ...), custom_call_target="tpu_custom_call" | custom-call | flops 3000000000 | bytes 4000000 | tf_op jit(solution)/shard_map/attend/pallas_call | solution.py:169
  115.3 2.3 %collective-permute-start.2 = (bf16[64,2048]{1,0:T(8,128)(2,1)S(1)}, bf16[64,2048]{1,0:T(8,128)(2,1)S(1)}, u32[]{:S(2)}, u32[]{:S(2)}) collective-permute-start(bf16[64,2048]{1,0:T(8,128)(2,1)S(1)} %get-tuple-element.19._), channel_id=1, source_target_pairs={{0,3},{1,0},{2,1},{3,2},{4,7},{5,4},{6,5},{7,6},{8,11},{9,8},{10,9... | collective-permute-start | bytes 786440 | tf_op jit(solution)/shard_map/ppermute | solution.py:24
  117.6 3.3 %attend.7 = (bf16[64,2048]{1,0:T(8,128)(2,1)S(1)}, f32[64,128]{1,0:T(8,128)S(1)}) custom-call(s32[3]{0:T(128)S(1)} %get-tuple-element.38.place_ref, f32[8]{0:T(128)S(1)} %copy-done.7, bf16[4,64,256]{2,1,0:T(8,128)(2,1)S(1)} %copy-done.5, bf16[4,64,256]{2,1,0:T(8,128)(2,1)S(1)} %copy-done.6, bf16[18,264,256]{2,1,0:T(8,128)(2,1)S(1)} %multiply_convert_fusion.w_ref, ...), custom_call_target="tpu_custom_call" | custom-call | flops 3000000000 | bytes 4000000 | tf_op jit(solution)/shard_map/attend/pallas_call | solution.py:169
  120.9 0.0 copy-start
  120.9 0.0 copy-start.1
  120.9 1.9 %collective-permute-done.2 = bf16[64,2048]{1,0:T(8,128)(2,1)S(1)} collective-permute-done((bf16[64,2048]{1,0:T(8,128)(2,1)S(1)}, bf16[64,2048]{1,0:T(8,128)(2,1)S(1)}, u32[]{:S(2)}, u32[]{:S(2)}) %collective-permute-start.2) | collective-permute-done | bytes 262176 | tf_op jit(solution)/shard_map/ppermute | solution.py:24
  122.9 0.0 collective-permute-done
  122.9 0.0 collective-permute-done.1
  122.9 1.3 multiply_reduce_fusion
  124.2 0.1 multiply_convert_fusion.1.refs_0_
  124.4 0.4 collective-permute-start.3
  124.7 4.2 %collective-permute-start.4 = (bf16[64,2048]{1,0:T(8,128)(2,1)S(1)}, bf16[64,2048]{1,0:T(8,128)(2,1)S(1)}, u32[]{:S(2)}, u32[]{:S(2)}) collective-permute-start(bf16[64,2048]{1,0:T(8,128)(2,1)S(1)} %multiply_convert_fusion.1.refs_0_), channel_id=1, source_target_pairs={{0,2},{1,3},{2,0},{3,1},{4,6},{5,7},{6,4},{7,5},{8,10},{9,11},{10,... | collective-permute-start | bytes 786440 | tf_op jit(solution)/shard_map/ppermute | solution.py:24
  128.9 0.0 collective-permute-start.5
  128.9 6.3 %collective-permute-start.6 = (bf16[8,2048]{1,0:T(8,128)(2,1)S(1)}, bf16[8,2048]{1,0:T(8,128)(2,1)S(1)}, u32[]{:S(2)}, u32[]{:S(2)}) collective-permute-start(bf16[8,2048]{1,0:T(8,128)(2,1)S(1)} %slice.28), channel_id=1, source_target_pairs={{0,4},{4,8},{8,12},{12,16},{16,20},{20,24},{24,28},{28,32},{32,36}... | collective-permute-start | bytes 98312 | tf_op jit(solution)/shard_map/ppermute | solution.py:29
  135.2 1.1 collective-permute-done.6.refs_4_
  136.4 2.0 %collective-permute-start.7 = (bf16[8,2048]{1,0:T(8,128)(2,1)S(1)}, bf16[8,2048]{1,0:T(8,128)(2,1)S(1)}, u32[]{:S(2)}, u32[]{:S(2)}) collective-permute-start(bf16[8,2048]{1,0:T(8,128)(2,1)S(1)} %collective-permute-done.6.refs_4_), channel_id=1, source_target_pairs={{0,1},{1,2},{2,3},{3,0},{4,5},{5,6},{6,7},{7,4},{8,9},{9,10},{10,1... | collective-permute-start | bytes 98312 | tf_op jit(solution)/shard_map/ppermute | solution.py:24
  138.3 0.0 collective-permute-start.8
  138.3 3.9 %collective-permute-done.7.refs_5_ = bf16[8,2048]{1,0:T(8,128)(2,1)S(1)} collective-permute-done((bf16[8,2048]{1,0:T(8,128)(2,1)S(1)}, bf16[8,2048]{1,0:T(8,128)(2,1)S(1)}, u32[]{:S(2)}, u32[]{:S(2)}) %collective-permute-start.7) | collective-permute-done | bytes 32800 | tf_op jit(solution)/shard_map/ppermute | solution.py:24
  142.2 0.0 collective-permute-start.9
  142.2 0.4 collective-permute-done.8.refs_6_
  142.7 2.7 %collective-permute-done.9.refs_7_ = bf16[8,2048]{1,0:T(8,128)(2,1)S(1)} collective-permute-done((bf16[8,2048]{1,0:T(8,128)(2,1)S(1)}, bf16[8,2048]{1,0:T(8,128)(2,1)S(1)}, u32[]{:S(2)}, u32[]{:S(2)}) %collective-permute-start.9) | collective-permute-done | bytes 32800 | tf_op jit(solution)/shard_map/ppermute | solution.py:24
  145.4 0.0 collective-permute-done.3.refs_1_
  145.4 0.0 collective-permute-done.4.refs_2_
  145.4 0.0 collective-permute-done.5.refs_3_
  145.4 5.6 %all-gather.3.cloned.1.call-done.refs_14_ = bf16[2048,4224]{1,0:T(8,128)(2,1)} async-done(((bf16[64,4224]{1,0:T(8,128)(2,1)}), bf16[2048,4224]{1,0:T(8,128)(2,1)}) %all-gather.3.cloned.1.call-update) | async-done | bytes 17301520 | tf_op jit(solution)/shard_map/all_gather | solution.py:320
  151.1 0.0 copy-done
  151.1 8.8 %feed_forward.1 = (bf16[64,2048]{1,0:T(8,128)(2,1)S(1)}, bf16[64,2048]{1,0:T(8,128)(2,1)S(1)}, bf16[64,2048]{1,0:T(8,128)(2,1)S(1)}, bf16[64,2048]{1,0:T(8,128)(2,1)S(1)}) custom-call(bf16[64,2048]{1,0:T(8,128)(2,1)S(1)} %multiply_convert_fusion.1.refs_0_, bf16[64,2048]{1,0:T(8,128)(2,1)S(1)} %collective-permute-done.3.refs_1_, ...), custom_call_target="tpu_custom_call" | custom-call | tf_op jit(solution)/shard_map/feed_forward/pallas_call | solution.py:277
  159.8 3.1 %collective-permute-start.10 = (bf16[64,2048]{1,0:T(8,128)(2,1)S(1)}, bf16[64,2048]{1,0:T(8,128)(2,1)S(1)}, u32[]{:S(2)}, u32[]{:S(2)}) collective-permute-start(bf16[64,2048]{1,0:T(8,128)(2,1)S(1)} %get-tuple-element.26), channel_id=1, source_target_pairs={{0,2},{1,3},{2,0},{3,1},{4,6},{5,7},{6,4},{7,5},{8,10},{9,11},{10,... | collective-permute-start | bytes 786440 | tf_op jit(solution)/shard_map/ppermute | solution.py:24
  163.0 0.4 collective-permute-start.11
  163.4 2.2 %collective-permute-start.12 = (bf16[64,2048]{1,0:T(8,128)(2,1)S(1)}, bf16[64,2048]{1,0:T(8,128)(2,1)S(1)}, u32[]{:S(2)}, u32[]{:S(2)}) collective-permute-start(bf16[64,2048]{1,0:T(8,128)(2,1)S(1)} %get-tuple-element.28), channel_id=1, source_target_pairs={{0,3},{1,0},{2,1},{3,2},{4,7},{5,4},{6,5},{7,6},{8,11},{9,8},{10,9... | collective-permute-start | bytes 786440 | tf_op jit(solution)/shard_map/ppermute | solution.py:24
  165.7 3.6 %collective-permute-done.10 = bf16[64,2048]{1,0:T(8,128)(2,1)S(1)} collective-permute-done((bf16[64,2048]{1,0:T(8,128)(2,1)S(1)}, bf16[64,2048]{1,0:T(8,128)(2,1)S(1)}, u32[]{:S(2)}, u32[]{:S(2)}) %collective-permute-start.10) | collective-permute-done | bytes 262176 | tf_op jit(solution)/shard_map/ppermute | solution.py:24
  169.2 6.1 %collective-permute-done.11 = bf16[64,2048]{1,0:T(8,128)(2,1)S(1)} collective-permute-done((bf16[64,2048]{1,0:T(8,128)(2,1)S(1)}, bf16[64,2048]{1,0:T(8,128)(2,1)S(1)}, u32[]{:S(2)}, u32[]{:S(2)}) %collective-permute-start.11) | collective-permute-done | bytes 262176 | tf_op jit(solution)/shard_map/ppermute | solution.py:24
  175.4 0.0 collective-permute-done.12
  175.4 0.9 fusion.3
  (29 shorter events, 0.2 us)
Async XLA Ops:
  6.5 4.5 %copy-start.11 = (bf16[4,64,64]{2,1,0:T(8,128)(2,1)S(1)}, bf16[4,64,64]{2,1,0:T(8,128)(2,1)}, u32[]{:S(2)}) copy-start(bf16[4,64,64]{2,1,0:T(8,128)(2,1)} %param.18) | copy-start | bytes 98308
  6.5 4.6 %copy-start.10 = (bf16[4,64,64]{2,1,0:T(8,128)(2,1)S(1)}, bf16[4,64,64]{2,1,0:T(8,128)(2,1)}, u32[]{:S(2)}) copy-start(bf16[4,64,64]{2,1,0:T(8,128)(2,1)} %param.20) | copy-start | bytes 98308
  6.6 4.3 %copy-start.12 = (bf16[4,64,128]{2,1,0:T(8,128)(2,1)S(1)}, bf16[4,64,128]{2,1,0:T(8,128)(2,1)}, u32[]{:S(2)}) copy-start(bf16[4,64,128]{2,1,0:T(8,128)(2,1)} %param.21) | copy-start | bytes 196612
  6.6 144.5 %all-gather.3.cloned.1.call-start = ((), (), s32[]{:S(2)}) async-start(), calls=%async_computation | async-start | bytes 17842176 | tf_op jit(solution)/shard_map/all_gather | solution.py:320
  97.5 0.7 copy-start.2
  97.5 1.6 copy-start.3
  97.5 1.6 copy-start.5
  97.5 1.6 copy-start.6
  97.5 1.6 copy-start.7
  97.5 1.6 copy-start.8
  102.5 20.4 %collective-permute-start.1 = (bf16[64,2048]{1,0:T(8,128)(2,1)S(1)}, bf16[64,2048]{1,0:T(8,128)(2,1)}, u32[]{:S(2)}, u32[]{:S(2)}) collective-permute-start(bf16[64,2048]{1,0:T(8,128)(2,1)S(1)} %get-tuple-element.17._), channel_id=1, source_target_pairs={{0,2},{1,3},{2,0},{3,1},{4,6},{5,7},{6,4},{7,5},{8,10},{9,11},{10,... | collective-permute-start | bytes 786440 | tf_op jit(solution)/shard_map/ppermute | solution.py:24
  109.5 13.3 %collective-permute-start = (bf16[64,2048]{1,0:T(8,128)(2,1)S(1)}, bf16[64,2048]{1,0:T(8,128)(2,1)}, u32[]{:S(2)}, u32[]{:S(2)}) collective-permute-start(bf16[64,2048]{1,0:T(8,128)(2,1)S(1)} %get-tuple-element.18._), channel_id=1, source_target_pairs={{0,1},{1,2},{2,3},{3,0},{4,5},{5,6},{6,7},{7,4},{8,9},{9,10},{10,1... | collective-permute-start | bytes 786440 | tf_op jit(solution)/shard_map/ppermute | solution.py:24
  110.2 1.7 copy-start.4
  115.3 7.6 %collective-permute-start.2 = (bf16[64,2048]{1,0:T(8,128)(2,1)S(1)}, bf16[64,2048]{1,0:T(8,128)(2,1)S(1)}, u32[]{:S(2)}, u32[]{:S(2)}) collective-permute-start(bf16[64,2048]{1,0:T(8,128)(2,1)S(1)} %get-tuple-element.19._), channel_id=1, source_target_pairs={{0,3},{1,0},{2,1},{3,2},{4,7},{5,4},{6,5},{7,6},{8,11},{9,8},{10,9... | collective-permute-start | bytes 786440 | tf_op jit(solution)/shard_map/ppermute | solution.py:24
  117.6 5.3 %copy-start.9 = (bf16[1,64,2048]{2,1,0:T(8,128)(2,1)S(1)}, bf16[1,64,2048]{2,1,0:T(8,128)(2,1)}, u32[]{:S(2)}) copy-start(bf16[1,64,2048]{2,1,0:T(8,128)(2,1)} %param.16) | copy-start | bytes 786436
  117.6 6.6 %copy-start.13 = (f32[2048]{0:T(1024)S(1)}, f32[2048]{0:T(1024)}, u32[]{:S(2)}) copy-start(f32[2048]{0:T(1024)} %param.26) | copy-start | bytes 24580
  120.9 30.1 %copy-start = (f32[3,1408]{1,0:T(4,128)S(1)}, f32[3,1408]{1,0:T(4,128)}, u32[]{:S(2)}) copy-start(f32[3,1408]{1,0:T(4,128)} %refs_12_.1) | copy-start | bytes 50692
  120.9 30.1 %copy-start.1 = (f32[3,1408]{1,0:T(4,128)S(1)}, f32[3,1408]{1,0:T(4,128)}, u32[]{:S(2)}) copy-start(f32[3,1408]{1,0:T(4,128)} %refs_13_.1) | copy-start | bytes 50692
  124.4 21.1 %collective-permute-start.3 = (bf16[64,2048]{1,0:T(8,128)(2,1)S(1)}, bf16[64,2048]{1,0:T(8,128)(2,1)S(1)}, u32[]{:S(2)}, u32[]{:S(2)}) collective-permute-start(bf16[64,2048]{1,0:T(8,128)(2,1)S(1)} %multiply_convert_fusion.1.refs_0_), channel_id=1, source_target_pairs={{0,1},{1,2},{2,3},{3,0},{4,5},{5,6},{6,7},{7,4},{8,9},{9,10},{10,1... | collective-permute-start | bytes 786440 | tf_op jit(solution)/shard_map/ppermute | solution.py:24
  124.7 20.7 %collective-permute-start.4 = (bf16[64,2048]{1,0:T(8,128)(2,1)S(1)}, bf16[64,2048]{1,0:T(8,128)(2,1)S(1)}, u32[]{:S(2)}, u32[]{:S(2)}) collective-permute-start(bf16[64,2048]{1,0:T(8,128)(2,1)S(1)} %multiply_convert_fusion.1.refs_0_), channel_id=1, source_target_pairs={{0,2},{1,3},{2,0},{3,1},{4,6},{5,7},{6,4},{7,5},{8,10},{9,11},{10,... | collective-permute-start | bytes 786440 | tf_op jit(solution)/shard_map/ppermute | solution.py:24
  128.9 16.5 %collective-permute-start.5 = (bf16[64,2048]{1,0:T(8,128)(2,1)S(1)}, bf16[64,2048]{1,0:T(8,128)(2,1)S(1)}, u32[]{:S(2)}, u32[]{:S(2)}) collective-permute-start(bf16[64,2048]{1,0:T(8,128)(2,1)S(1)} %multiply_convert_fusion.1.refs_0_), channel_id=1, source_target_pairs={{0,3},{1,0},{2,1},{3,2},{4,7},{5,4},{6,5},{7,6},{8,11},{9,8},{10,9... | collective-permute-start | bytes 786440 | tf_op jit(solution)/shard_map/ppermute | solution.py:24
  128.9 7.4 %collective-permute-start.6 = (bf16[8,2048]{1,0:T(8,128)(2,1)S(1)}, bf16[8,2048]{1,0:T(8,128)(2,1)S(1)}, u32[]{:S(2)}, u32[]{:S(2)}) collective-permute-start(bf16[8,2048]{1,0:T(8,128)(2,1)S(1)} %slice.28), channel_id=1, source_target_pairs={{0,4},{4,8},{8,12},{12,16},{16,20},{20,24},{24,28},{28,32},{32,36}... | collective-permute-start | bytes 98312 | tf_op jit(solution)/shard_map/ppermute | solution.py:29
  136.4 5.9 %collective-permute-start.7 = (bf16[8,2048]{1,0:T(8,128)(2,1)S(1)}, bf16[8,2048]{1,0:T(8,128)(2,1)S(1)}, u32[]{:S(2)}, u32[]{:S(2)}) collective-permute-start(bf16[8,2048]{1,0:T(8,128)(2,1)S(1)} %collective-permute-done.6.refs_4_), channel_id=1, source_target_pairs={{0,1},{1,2},{2,3},{3,0},{4,5},{5,6},{6,7},{7,4},{8,9},{9,10},{10,1... | collective-permute-start | bytes 98312 | tf_op jit(solution)/shard_map/ppermute | solution.py:24
  138.3 4.3 %collective-permute-start.8 = (bf16[8,2048]{1,0:T(8,128)(2,1)S(1)}, bf16[8,2048]{1,0:T(8,128)(2,1)S(1)}, u32[]{:S(2)}, u32[]{:S(2)}) collective-permute-start(bf16[8,2048]{1,0:T(8,128)(2,1)S(1)} %collective-permute-done.6.refs_4_), channel_id=1, source_target_pairs={{0,2},{1,3},{2,0},{3,1},{4,6},{5,7},{6,4},{7,5},{8,10},{9,11},{10,... | collective-permute-start | bytes 98312 | tf_op jit(solution)/shard_map/ppermute | solution.py:24
  142.2 3.2 %collective-permute-start.9 = (bf16[8,2048]{1,0:T(8,128)(2,1)S(1)}, bf16[8,2048]{1,0:T(8,128)(2,1)S(1)}, u32[]{:S(2)}, u32[]{:S(2)}) collective-permute-start(bf16[8,2048]{1,0:T(8,128)(2,1)S(1)} %collective-permute-done.6.refs_4_), channel_id=1, source_target_pairs={{0,3},{1,0},{2,1},{3,2},{4,7},{5,4},{6,5},{7,6},{8,11},{9,8},{10,9... | collective-permute-start | bytes 98312 | tf_op jit(solution)/shard_map/ppermute | solution.py:24
  159.8 9.4 %collective-permute-start.10 = (bf16[64,2048]{1,0:T(8,128)(2,1)S(1)}, bf16[64,2048]{1,0:T(8,128)(2,1)S(1)}, u32[]{:S(2)}, u32[]{:S(2)}) collective-permute-start(bf16[64,2048]{1,0:T(8,128)(2,1)S(1)} %get-tuple-element.26), channel_id=1, source_target_pairs={{0,2},{1,3},{2,0},{3,1},{4,6},{5,7},{6,4},{7,5},{8,10},{9,11},{10,... | collective-permute-start | bytes 786440 | tf_op jit(solution)/shard_map/ppermute | solution.py:24
  163.0 12.4 %collective-permute-start.11 = (bf16[64,2048]{1,0:T(8,128)(2,1)S(1)}, bf16[64,2048]{1,0:T(8,128)(2,1)S(1)}, u32[]{:S(2)}, u32[]{:S(2)}) collective-permute-start(bf16[64,2048]{1,0:T(8,128)(2,1)S(1)} %get-tuple-element.27), channel_id=1, source_target_pairs={{0,1},{1,2},{2,3},{3,0},{4,5},{5,6},{6,7},{7,4},{8,9},{9,10},{10,1... | collective-permute-start | bytes 786440 | tf_op jit(solution)/shard_map/ppermute | solution.py:24
  163.4 12.0 %collective-permute-start.12 = (bf16[64,2048]{1,0:T(8,128)(2,1)S(1)}, bf16[64,2048]{1,0:T(8,128)(2,1)S(1)}, u32[]{:S(2)}, u32[]{:S(2)}) collective-permute-start(bf16[64,2048]{1,0:T(8,128)(2,1)S(1)} %get-tuple-element.28), channel_id=1, source_target_pairs={{0,3},{1,0},{2,1},{3,2},{4,7},{5,4},{6,5},{7,6},{8,11},{9,8},{10,9... | collective-permute-start | bytes 786440 | tf_op jit(solution)/shard_map/ppermute | solution.py:24
Sparse Core Ops, SparseCore 0:
  9.2 141.8 all-gather.2
